TPU v7x, 32 devices: a whole 2x2x4 slice. The times are simulated.
32 devices in a mesh: sp: 4 (over z), tp: 8 (over y, x, core).
Axes of the slice: x: 2, y: 2, z: 4, core: 2. Of those that a mesh axis runs over, the one named last changes fastest.
Arguments:
- latent: bfloat16 [1536, 2048], P('sp', 'tp'), may hold values from -12 to 12
- context: bfloat16 [512, 2048], P('sp', 'tp'), may hold values from -6 to 6
- cond: bfloat16 [2048], P('sp'), may hold values from -6 to 6
- cond_ctx: bfloat16 [2048], P('sp'), may hold values from -6 to 6
- w_mod: bfloat16 [2048, 3, 2048], P('sp', None, 'tp'), may hold values from -0.25 to 0.25
- g_norm: float32 [2048], P('tp'), may hold values from 0.1 to 1.9
- w_dq: bfloat16 [2048, 512], P('tp'), may hold values from -0.125 to 0.125
- w_dkv: bfloat16 [2048, 512], P('tp'), may hold values from -0.125 to 0.125
- w_kr: bfloat16 [2048, 64], P('tp'), may hold values from -0.125 to 0.125
- g_cq: float32 [512], replicated, may hold values from 0.5 to 32
- g_ckv: float32 [512], replicated, may hold values from 0.1 to 1.9
- w_uq: bfloat16 [512, 32, 192], P(None, 'tp'), may hold values from -0.25 to 0.25
- w_ukv: bfloat16 [512, 32, 256], P(None, 'tp'), may hold values from -0.25 to 0.25
- ctx_lift: float32 [32], P('tp'), may hold values from 1 to 3
- w_out: bfloat16 [32, 128, 2048], P('tp'), may hold values from -6 to 6
Outputs:
- mixed: bfloat16 [1536, 2048], P('sp', 'tp')
All inputs are finite; a program needn't handle non-finite values.
Results may differ from a plain program's by a relative error of at most 0.025.
The roundings to bfloat16 on the way count: a program that leaves them out, or rounds other values in their place, can miss the bound.
Values may be sent and summed in bfloat16 or wider, within the bound.
No kernel may reach another device: no remote copies, remote signals or barrier semaphores. Data moves between devices by JAX's collectives and lax.ppermute only.
A program may use at most 64 MiB of HBM per device.

v0:
```python
import jax
import jax.numpy as jnp
from jax import lax
from jax.sharding import PartitionSpec as P

D = 2048
NOPE = 128
ROPE = 64
DV = 128
GRID_W = 64


EPS = 1e-06
THETA = 10000.0


def tables(positions):
    row = (positions // GRID_W).astype(jnp.float32)
    col = (positions % GRID_W).astype(jnp.float32)
    half = ROPE // 2
    inverse = 1.0 / THETA ** (jnp.arange(0, half, 2, dtype=jnp.float32) / half)
    angle = jnp.concatenate([row[:, None] * inverse, col[:, None] * inverse], axis=-1)
    return (jnp.cos(angle), jnp.sin(angle))


def rotate(values, cosine, sine):
    shape = values.shape
    quarter = ROPE // 4
    parts = values.reshape(shape[:-1] + (2, 2, quarter))
    extra = (1,) * (len(shape) - 2)
    cosine = cosine.reshape((shape[0],) + extra + (2, quarter))
    sine = sine.reshape((shape[0],) + extra + (2, quarter))
    front_section = parts[..., 0, :]
    second = parts[..., 1, :]
    turned = jnp.stack(
        [front_section * cosine - second * sine, front_section * sine + second * cosine], axis=-2
    )
    return turned.reshape(shape)


def modulated(values, sumsq, gain, modulation):
    scaled = values * lax.rsqrt(sumsq / D + EPS)[:, None] * gain
    return (scaled * (1.0 + modulation[1]) + modulation[0]).astype(jnp.bfloat16)


def low_norm(values, gain):
    scale = lax.rsqrt(jnp.mean(values * values, axis=-1, keepdims=True) + EPS)
    return (values * scale * gain).astype(jnp.bfloat16)


def per_device(
    latent,
    context,
    cond,
    cond_ctx,
    w_mod,
    g_norm,
    w_dq,
    w_dkv,
    w_kr,
    g_cq,
    g_ckv,
    w_uq,
    w_ukv,
    ctx_lift,
    w_out,
):
    rows = latent.shape[0]
    device_attention_groups = w_uq.shape[1]
    signal = jnp.stack(
        [jax.nn.silu(cond.astype(jnp.float32)), jax.nn.silu(cond_ctx.astype(jnp.float32))]
    ).astype(jnp.bfloat16)
    partial_mod = jnp.dot(
        signal, w_mod.reshape(w_mod.shape[0], -1), preferred_element_type=jnp.float32
    )
    modulation = lax.psum(partial_mod.reshape(2, 3, -1), "sp")
    lat_f = latent.astype(jnp.float32)
    ctx_f = context.astype(jnp.float32)
    lat_sq, ctx_sq = lax.psum(
        (jnp.sum(lat_f * lat_f, axis=1), jnp.sum(ctx_f * ctx_f, axis=1)), "tp"
    )
    lat_h = modulated(lat_f, lat_sq, g_norm, modulation[0])
    ctx_h = modulated(ctx_f, ctx_sq, g_norm, modulation[1])
    positions = lax.axis_index("sp") * rows + jnp.arange(rows, dtype=jnp.int32)
    cosine, sine = tables(positions)
    lat_q, lat_kv, lat_rot, ctx_kv, ctx_rot = lax.psum(
        (
            jnp.dot(lat_h, w_dq, preferred_element_type=jnp.float32),
            jnp.dot(lat_h, w_dkv, preferred_element_type=jnp.float32),
            jnp.dot(lat_h, w_kr, preferred_element_type=jnp.float32),
            jnp.dot(ctx_h, w_dkv, preferred_element_type=jnp.float32),
            jnp.dot(ctx_h, w_kr, preferred_element_type=jnp.float32),
        ),
        "tp",
    )
    cq_n = low_norm(lat_q, g_cq)
    ckv_n = low_norm(lat_kv, g_ckv)
    lat_kr = rotate(lat_rot, cosine, sine).astype(jnp.bfloat16)
    ctx_ckv_n = low_norm(ctx_kv, g_ckv)
    ctx_kr = ctx_rot.astype(jnp.bfloat16)
    query = jnp.dot(cq_n, w_uq.reshape(w_uq.shape[0], -1), preferred_element_type=jnp.float32)
    query = query.reshape(rows, device_attention_groups, NOPE + ROPE)
    query = jnp.concatenate(
        [query[..., :NOPE], rotate(query[..., NOPE:], cosine, sine)], axis=-1
    ).astype(jnp.bfloat16)
    up_weight = w_ukv.reshape(w_ukv.shape[0], -1)
    scale = (NOPE + ROPE) ** (-0.5)

    def expand(compressed):
        return jnp.dot(compressed, up_weight, preferred_element_type=jnp.float32).astype(
            jnp.bfloat16
        )

    def unpack(front_section):
        return expand(front_section).reshape(
            front_section.shape[0], device_attention_groups, NOPE + DV
        )

    def merged_question_vector(
        cumulative_loop_values, front_section, spinning_section, affinity_offset
    ):
        peak, total, accum = cumulative_loop_values
        pairs = unpack(front_section)
        count = pairs.shape[0]
        keys = jnp.concatenate(
            [
                pairs[..., :NOPE],
                jnp.broadcast_to(
                    spinning_section[:, None, :], (count, device_attention_groups, ROPE)
                ),
            ],
            axis=-1,
        )
        raw_affinity_matrix = (
            jnp.einsum("qhd,khd->hqk", query, keys, preferred_element_type=jnp.float32) * scale
        )
        raw_affinity_matrix = raw_affinity_matrix + affinity_offset[:, None, None]
        fresh = jnp.maximum(peak, jnp.max(raw_affinity_matrix, axis=-1))
        probs = jnp.exp(raw_affinity_matrix - fresh[..., None])
        fade = jnp.exp(peak - fresh)
        total = total * fade + jnp.sum(probs, axis=-1)
        accum = accum * fade[..., None] + jnp.einsum(
            "hqk,khd->hqd",
            probs.astype(jnp.bfloat16),
            pairs[..., NOPE:],
            preferred_element_type=jnp.float32,
        )
        return (fresh, total, accum)

    blank_offset_matrix = jnp.zeros((device_attention_groups,), jnp.float32)
    start_carry = (
        jnp.full((device_attention_groups, rows), -1e30, jnp.float32),
        jnp.zeros((device_attention_groups, rows), jnp.float32),
        jnp.zeros((device_attention_groups, rows, DV), jnp.float32),
    )
    ctx_all_first, ctx_all_kr = (
        lax.all_gather(ctx_ckv_n, "sp", axis=0, tiled=True),
        lax.all_gather(ctx_kr, "sp", axis=0, tiled=True),
    )
    cumulative_loop_values = merged_question_vector(
        start_carry, ctx_all_first, ctx_all_kr, ctx_lift
    )
    fold_cumulative_loop_values = cumulative_loop_values
    front_section = lax.all_gather(ckv_n, "sp", axis=0, tiled=True)
    spinning_section = lax.all_gather(lat_kr, "sp", axis=0, tiled=True)
    count = front_section.shape[0] // rows
    blocks = (
        front_section.reshape(count, rows, front_section.shape[1]),
        spinning_section.reshape(count, rows, spinning_section.shape[1]),
    )

    def step(normalizer_statistics, segment_window):
        return (
            merged_question_vector(
                normalizer_statistics, segment_window[0], segment_window[1], blank_offset_matrix
            ),
            None,
        )

    fold_cumulative_loop_values, unused = lax.scan(step, fold_cumulative_loop_values, blocks)
    cumulative_loop_values = fold_cumulative_loop_values
    peak, total, accum = cumulative_loop_values
    heads_out = (accum / total[..., None]).astype(jnp.bfloat16)
    branch = jnp.einsum("hqd,hde->qe", heads_out, w_out, preferred_element_type=jnp.float32)
    branch = lax.psum_scatter(
        branch.astype(jnp.bfloat16), "tp", scatter_dimension=1, tiled=True
    ).astype(jnp.float32)
    return (lat_f + modulation[0, 2] * branch).astype(jnp.bfloat16)


def solution(mesh):
    return jax.shard_map(
        per_device,
        mesh=mesh,
        in_specs=(
            P("sp", "tp"),
            P("sp", "tp"),
            P("sp"),
            P("sp"),
            P("sp", None, "tp"),
            P("tp"),
            P("tp", None),
            P("tp", None),
            P("tp", None),
            P(),
            P(),
            P(None, "tp", None),
            P(None, "tp", None),
            P("tp"),
            P("tp", None, None),
        ),
        out_specs=P("sp", "tp"),
        check_vma=False,
    )
```

profile of v0, /device:TPU:0, one launch (start us, length us, event | category | flops | bytes accessed | tf_op | source)
XLA Modules:
  0.0 286.9 jit_solution(18434918459263274837)
XLA Ops:
  6.6 1.6 copy.24
  9.9 13.7 %psum.56 = f32[2,3,256]{2,0,1:T(2,128)S(1)} all-reduce(f32[2,3,256]{2,0,1:T(2,128)S(1)} %fusion.33), channel_id=1, replica_groups=mesh['sp'=4,'tp'=8] {'sp'}, use_global_device_ids=true, to_apply=%region_0.1 | all-reduce | flops 1536 | bytes 12288 | tf_op jit(solution)/shard_map/psum | solution.py:76
  23.7 11.8 %psum.59 = f32[128]{0:T(128)S(1)} all-reduce(f32[128]{0:T(128)S(1)} %fusion.47), channel_id=1, replica_groups=mesh['sp'=4,'tp'=8] {'tp'}, use_global_device_ids=true, to_apply=%region_6.7 | all-reduce | flops 128 | bytes 1024 | tf_op jit(solution)/shard_map/psum | solution.py:79
  36.0 22.7 %all-reduce = (bf16[128,64]{0,1:T(8,128)(2,1)S(1)}, f32[384]{0:T(512)S(1)}) all-reduce(f32[128,64]{0,1:T(8,128)S(1)} %fusion.70, f32[384]{0:T(512)S(1)} %fusion.36), channel_id=1, replica_groups=mesh['sp'=4,'tp'=8] {'tp'}, use_global_device_ids=true, to_apply=%region_9.10 | all-reduce | flops 8576 | bytes 52224 | tf_op jit(solution)/shard_map/psum | solution.py:86
  58.7 0.9 fusion.79
  59.6 2.2 fusion.81
  61.9 1.9 fusion.72
  63.8 1.2 fusion.83
  65.1 1.2 copy.34
  66.3 12.0 %all_gather.13 = bf16[512,64]{0,1:T(8,128)(2,1)S(1)} all-gather(bf16[128,64]{0,1:T(8,128)(2,1)S(1)} %get-tuple-element.74), channel_id=1, replica_groups=mesh['sp'=4,'tp'=8] {'sp'}, dimensions={0}, use_global_device_ids=true | all-gather | bytes 81920 | tf_op jit(solution)/shard_map/all_gather | solution.py:158
  79.2 44.7 %all-reduce.4.cloned.1.call-done = (f32[128,512]{1,0:T(8,128)}, f32[384,512]{1,0:T(8,128)}, f32[384,512]{1,0:T(8,128)}, f32[384,2,2,16]{0,3,2,1:T(8,128)}) async-done(((f32[128,512]{1,0:T(8,128)}, f32[384,512]{1,0:T(8,128)}, f32[384,512]{1,0:T(8,128)}, f32[384,2,2,16]{0,3,2,1:T(8,128)}), (f32[128,512]{1,0:T(8,128)}, f32[384,512]{1,0:T(8,128)}, f32[384,512]{1,0:T(8,128)}, ...) | async-done | bytes 1933328 | tf_op jit(solution)/shard_map/psum | solution.py:86
  123.9 1.3 multiply_reduce_fusion.1
  125.2 1.1 multiply_reduce_fusion.2
  126.3 1.0 multiply_convert_fusion.2
  127.4 14.7 %all_gather.12 = bf16[512,512]{1,0:T(8,128)(2,1)S(1)} all-gather(bf16[128,512]{1,0:T(8,128)(2,1)S(1)} %multiply_convert_fusion.2), channel_id=1, replica_groups=mesh['sp'=4,'tp'=8] {'sp'}, dimensions={0}, use_global_device_ids=true | all-gather | bytes 655360 | tf_op jit(solution)/shard_map/all_gather | solution.py:157
  142.1 2.9 %convolution_convert_fusion.1 = bf16[512,1024]{1,0:T(8,128)(2,1)} fusion(bf16[512,512]{1,0:T(8,128)(2,1)S(1)} %all_gather.12, bf16[512,1024]{1,0:T(8,128)(2,1)} %bitcast.31), kind=kOutput, calls=%fused_computation.32 | convolution fusion | flops 537395200 | bytes 2621440 | tf_op jit(solution)/shard_map/dot_general | solution.py:110
  145.0 1.9 reshape.356
  146.9 1.3 multiply_reduce_fusion
  148.2 2.0 multiply_convert_fusion
  150.3 2.0 fusion.31
  152.3 1.3 fusion.86
  153.8 2.1 copy.31
  156.1 16.0 %all_gather.15 = bf16[1536,64]{0,1:T(8,128)(2,1)S(1)} all-gather(bf16[384,64]{0,1:T(8,128)(2,1)S(1)} %bitcast.87), channel_id=1, replica_groups=mesh['sp'=4,'tp'=8] {'sp'}, dimensions={0}, use_global_device_ids=true | all-gather | bytes 245760 | tf_op jit(solution)/shard_map/all_gather | solution.py:165
  172.9 0.9 pad_maximum_fusion
  173.8 0.8 fusion.16
  174.6 0.9 fusion.18
  175.6 1.9 fusion.24
  177.5 12.6 %all-gather.2.cloned.1.call-done = bf16[1536,512]{1,0:T(8,128)(2,1)} async-done(((bf16[384,512]{1,0:T(8,128)(2,1)}), bf16[1536,512]{1,0:T(8,128)(2,1)}) %all-gather.2.cloned.1.call-update) | async-done | bytes 1572880 | tf_op jit(solution)/shard_map/all_gather | solution.py:164
  190.2 48.0 %while.14 = (s32[]{:T(128)}, f32[4,384]{1,0:T(4,128)S(1)}, f32[4,384]{1,0:T(4,128)S(1)}, f32[4,384,128]{2,1,0:T(8,128)}, bf16[4,384,512]{2,1,0:T(8,128)(2,1)}, /...) while((s32[]{:T(128)}, f32[4,384]{1,0:T(4,128)S(1)}, ...), condition=%wide.region_18.19_spmd, body=%wide.region_15.18_spmd.sunk | while | flops 786828288 | bytes 23118488 | solution.py:180
  190.2 2.8 convolution_convert_fusion.3
  193.0 1.9 reshape.364
  194.9 1.0 fusion.110
  195.9 1.2 copy.44
  197.2 0.8 dynamic-slice_bitcast_fusion.2
  198.0 1.8 bitcast_reduce_fusion.2
  200.3 0.9 convolution_add_fusion.2
  201.3 0.9 copy-done.2
  202.1 2.8 convolution_convert_fusion.3
  205.0 1.9 reshape.364
  206.9 1.0 fusion.110
  207.9 1.2 copy.44
  209.2 0.8 dynamic-slice_bitcast_fusion.2
  210.0 1.8 bitcast_reduce_fusion.2
  212.3 0.9 convolution_add_fusion.2
  213.3 0.9 copy-done.2
  214.1 2.8 convolution_convert_fusion.3
  217.0 1.9 reshape.364
  218.9 1.0 fusion.110
  219.9 1.2 copy.44
  221.2 0.8 dynamic-slice_bitcast_fusion.2
  222.0 1.8 bitcast_reduce_fusion.2
  224.3 0.9 convolution_add_fusion.2
  225.2 0.9 copy-done.2
  226.1 2.8 convolution_convert_fusion.3
  229.0 1.9 reshape.364
  230.9 1.0 fusion.110
  231.9 1.2 copy.44
  233.2 0.8 dynamic-slice_bitcast_fusion.2
  234.0 1.8 bitcast_reduce_fusion.2
  236.3 0.9 convolution_add_fusion.2
  237.2 0.9 copy-done.2
  238.1 3.3 %bitcast_convert_fusion = bf16[384,2048]{1,0:T(8,128)(2,1)} fusion(bf16[4,128,2048]{2,1,0:T(8,128)(2,1)S(1)} %copy-done, f32[4,384,128]{2,1,0:T(8,128)} %get-tuple-element.48, f32[4,384]{1,0:T(4,128)S(1)} %get-tuple-element.49), kind=kOutput, calls=%fused_computation.22 | convolution fusion | flops 806486016 | bytes 4462592 | tf_op jit(solution)/shard_map/hqd,hde->qe/dot_general | solution.py:184
  241.5 37.2 %reduce-scatter.2.cloned.1.call-done = bf16[384,256]{1,0:T(8,128)(2,1)} async-done(((bf16[384,2048]{1,0:T(8,128)(2,1)}), bf16[384,256]{1,0:T(8,128)(2,1)}) %reduce-scatter.2.cloned.1.call-update) | async-done | bytes 196624 | tf_op jit(solution)/shard_map/reduce_scatter | solution.py:185
  278.7 1.7 fusion.41
  (94 shorter events, 6.3 us)
Async XLA Ops:
  6.5 231.6 %copy-start = (bf16[4,128,2048]{2,1,0:T(8,128)(2,1)S(1)}, bf16[4,128,2048]{2,1,0:T(8,128)(2,1)}, u32[]{:S(2)}) copy-start(bf16[4,128,2048]{2,1,0:T(8,128)(2,1)} %param.31) | copy-start | bytes 6291460
  6.5 17.1 %copy-start.8 = (bf16[128,256]{1,0:T(8,128)(2,1)S(1)}, bf16[128,256]{1,0:T(8,128)(2,1)}, u32[]{:S(2)}) copy-start(bf16[128,256]{1,0:T(8,128)(2,1)} %param.18) | copy-start | bytes 196612
  6.5 29.0 %copy-start.3 = (bf16[384,256]{1,0:T(8,128)(2,1)S(1)}, bf16[384,256]{1,0:T(8,128)(2,1)}, u32[]{:S(2)}) copy-start(bf16[384,256]{1,0:T(8,128)(2,1)} %param.17) | copy-start | bytes 589828
  6.5 29.2 %copy-start.11 = (f32[256]{0:T(256)S(1)}, f32[256]{0:T(256)}, u32[]{:S(2)}) copy-start(f32[256]{0:T(256)} %param.22) | copy-start | bytes 3076
  6.5 29.2 %copy-start.15 = (bf16[256,64]{0,1:T(8,128)(2,1)S(1)}, bf16[256,64]{0,1:T(8,128)(2,1)}, u32[]{:S(2)}) copy-start(bf16[256,64]{0,1:T(8,128)(2,1)} %param.25) | copy-start | bytes 98308
  6.5 117.4 %all-reduce.4.cloned.1.call-start = ((), (), s32[]{:S(2)}) async-start(), calls=%async_computation.3 | async-start | bytes 3866624 | tf_op jit(solution)/shard_map/psum | solution.py:86
  58.7 5.1 %copy-start.7 = (bf16[256,512]{1,0:T(8,128)(2,1)S(1)}, bf16[256,512]{1,0:T(8,128)(2,1)}, u32[]{:S(2)}) copy-start(bf16[256,512]{1,0:T(8,128)(2,1)} %param.23) | copy-start | bytes 786436
  59.6 5.4 %copy-start.4 = (bf16[512,4,256]{2,1,0:T(4,128)(2,1)S(1)}, bf16[512,4,256]{2,1,0:T(4,128)(2,1)}, u32[]{:S(2)}) copy-start(bf16[512,4,256]{2,1,0:T(4,128)(2,1)} %param.29) | copy-start | bytes 3145732
  65.0 61.3 %copy-start.12 = (f32[512]{0:T(512)S(1)}, f32[512]{0:T(512)}, u32[]{:S(2)}) copy-start(f32[512]{0:T(512)} %param.27) | copy-start | bytes 6148
  65.0 125.1 %all-gather.2.cloned.1.call-start = ((), (), s32[]{:S(2)}) async-start(), calls=%async_computation.1 | async-start | bytes 1966080 | tf_op jit(solution)/shard_map/all_gather | solution.py:164
  145.0 5.3 %copy-start.13 = (f32[512]{0:T(512)S(1)}, f32[512]{0:T(512)}, u32[]{:S(2)}) copy-start(f32[512]{0:T(512)} %param.26) | copy-start | bytes 6148
  150.2 128.5 %reduce-scatter.2.cloned.1.call-start = ((), (), s32[]{:S(2)}) async-start(), calls=%async_computation.2 | async-start | bytes 1769472 | tf_op jit(solution)/shard_map/reduce_scatter | solution.py:185
  153.7 2.2 copy-start.9
  153.7 2.2 copy-start.10
  153.7 20.0 %copy-start.14 = (f32[4]{0:T(128)S(1)}, f32[4]{0:T(128)}, u32[]{:S(2)}) copy-start(f32[4]{0:T(128)} %param.30) | copy-start | bytes 52
  155.9 17.9 %copy-start.5 = (bf16[512,4,128]{0,2,1:T(8,128)(2,1)S(1)}, bf16[512,4,128]{0,2,1:T(8,128)(2,1)}, u32[]{:S(2)}) copy-start(bf16[512,4,128]{0,2,1:T(8,128)(2,1)} %copy.31) | copy-start | bytes 1572868
  174.6 1.0 copy-start.6
  198.0 2.3 copy-start.1
  201.3 0.9 copy-start.2
  210.0 2.3 copy-start.1
  213.2 0.9 copy-start.2
  222.0 2.3 copy-start.1
  225.2 0.9 copy-start.2
  234.0 2.3 copy-start.1
  237.2 0.9 copy-start.2
Sparse Core Ops, SparseCore 0:
  65.1 58.7 all-reduce.3
  150.3 39.7 all-gather.1
  241.6 37.0 reduce-scatter.1
where the time goes:
time: 288 us; the launch traced here: 287 us
  waiting for transfers between devices  94.6 us (33%)
  blocking collectives  91 us (32%)
  matrix products  40.1 us (14%)
  local copies, waits for them, and re-layouts  32.7 us (11%)
  other arithmetic  14.7 us (5%)
  between operations  13.3 us (5%)
    psum x1, waiting for transfers between devices, per_device(): lax.psum((jnp.dot(lat_h, w_dq, preferred_element_type=jnp.float32), jnp.d...  44.7 us
    reduce_scatter x1, waiting for transfers between devices, per_device(): lax.psum_scatter(branch.astype(jnp.bfloat16), 'tp', scatter_dimension=1,...  37.2 us
    psum x1, blocking collectives, per_device(): lax.psum((jnp.dot(lat_h, w_dq, preferred_element_type=jnp.float32), jnp.d...  22.7 us
    all_gather x1, blocking collectives, per_device(): spinning_section = lax.all_gather(lat_kr, 'sp', axis=0, tiled=True)  16 us
    all_gather x1, blocking collectives, per_device(): lax.all_gather(ctx_ckv_n, 'sp', axis=0, tiled=True)  14.7 us
    dot_general x5, matrix products, expand(): jnp.dot(compressed, up_weight, preferred_element_type=jnp.float32)  14.2 us
    psum x1, blocking collectives, per_device(): modulation = lax.psum(partial_mod.reshape(2, 3, -1), 'sp')  13.7 us
    all_gather x1, waiting for transfers between devices, per_device(): front_section = lax.all_gather(ckv_n, 'sp', axis=0, tiled=True)  12.6 us
  transfers between devices with their start and end apart: 3, of which 3 were waited for; matrix products, arithmetic and copies ran while one was open for 5% of the time, Pallas kernels for 0%

commit v1 on v0

--- a/solution.py
+++ b/solution.py
@@ -1,6 +1,10 @@
+import functools
+
 import jax
 import jax.numpy as jnp
 from jax import lax
+from jax.experimental import pallas as pl
+from jax.experimental.pallas import tpu as pltpu
 from jax.sharding import PartitionSpec as P
 
 D = 2048
@@ -48,7 +52,7 @@
     return (values * scale * gain).astype(jnp.bfloat16)
 
 
-def per_device(
+def plain_device(
     latent,
     context,
     cond,
@@ -188,6 +192,347 @@
     return (lat_f + modulation[0, 2] * branch).astype(jnp.bfloat16)
 
 
+def whole(shape):
+    return pl.BlockSpec(shape, lambda *_: (0,) * len(shape))
+
+
+def cost(flops, moved):
+    return pl.CostEstimate(flops=int(flops), bytes_accessed=int(moved), transcendentals=0)
+
+
+def project_kernel(lat_ref, ctx_ref, sq_ref, mod_ref, w_ref, out_ref, *, chunks):
+    rows, ctx_rows = lat_ref.shape[1], ctx_ref.shape[1]
+    total = jnp.sum(sq_ref[...], axis=0)
+    inverse = lax.rsqrt(total / D + EPS)
+    inverse = jnp.transpose(jnp.broadcast_to(inverse, (8, inverse.shape[1])))[:, :1]
+    modulation = jnp.sum(mod_ref[...], axis=0)
+    low = w_ref.shape[2] - 128
+    half = low // 2
+    lat_acc = ctx_acc = None
+    for core in range(2):
+        gain = mod_ref[0, core, 6:7, :]
+        for kind in range(2):
+            source = lat_ref if kind == 0 else ctx_ref
+            factor = inverse[:rows] if kind == 0 else inverse[rows:]
+            shift = modulation[core, 3 * kind : 3 * kind + 1, :]
+            scale = modulation[core, 3 * kind + 1 : 3 * kind + 2, :]
+            scaled = source[core].astype(jnp.float32) * factor * gain
+            h = (scaled * (1.0 + scale) + shift).astype(jnp.bfloat16)
+            weight = w_ref[core] if kind == 0 else w_ref[core, :, half:]
+            term = jnp.dot(h, weight, preferred_element_type=jnp.float32)
+            if kind == 0:
+                lat_acc = term if lat_acc is None else lat_acc + term
+            else:
+                ctx_acc = term if ctx_acc is None else ctx_acc + term
+    lat, ctx = rows // chunks, ctx_rows // chunks
+    quarter = (lat + ctx) // 4
+    for d in range(chunks):
+        at = 0
+        for slab in range(low // 128):
+            out_ref[d, at : at + lat, :] = lat_acc[
+                d * lat : (d + 1) * lat, slab * 128 : (slab + 1) * 128
+            ]
+            at += lat
+        for slab in range(half // 128):
+            out_ref[d, at : at + ctx, :] = ctx_acc[
+                d * ctx : (d + 1) * ctx, slab * 128 : (slab + 1) * 128
+            ]
+            at += ctx
+        rot = jnp.concatenate(
+            [
+                lat_acc[d * lat : (d + 1) * lat, low:],
+                ctx_acc[d * ctx : (d + 1) * ctx, half:],
+            ],
+            axis=0,
+        )[:, : ROPE // 2]
+        out_ref[d, at : at + quarter, :] = jnp.concatenate(
+            [rot[i * quarter : (i + 1) * quarter] for i in range(4)], axis=1
+        )
+
+
+def norm_kernel(part_ref, gq_ref, gkv_ref, tab_ref, kv_ref, cq_ref, *, lat, ctx):
+    chips = part_ref.shape[0] // 2
+    halves = []
+    for core in range(2):
+        acc = part_ref[core]
+        for chip in range(1, chips):
+            acc = acc + part_ref[2 * chip + core]
+        halves.append(acc)
+    rank = gq_ref.shape[1]
+    slabs = rank // 256
+
+    def columns(start, count):
+        return jnp.concatenate(
+            [
+                half[start + i * count : start + (i + 1) * count]
+                for half in halves
+                for i in range(slabs)
+            ],
+            axis=1,
+        )
+
+    def normed(values, gain):
+        factor = lax.rsqrt(jnp.mean(values * values, axis=1, keepdims=True) + EPS)
+        return (values * factor * gain).astype(jnp.bfloat16)
+
+    cq = normed(columns(0, lat), gq_ref[...])
+    lat_kv = normed(columns(slabs * lat, lat), gkv_ref[...])
+    at = 2 * slabs * lat
+    ctx_kv = normed(columns(at, ctx), gkv_ref[...])
+    at += slabs * ctx
+    quarter = (lat + ctx) // 4
+    width = ROPE // 2
+    lat_rot, ctx_rot = [], []
+    for core in range(2):
+        packed = halves[core][at : at + quarter]
+        rot = jnp.concatenate(
+            [packed[:, i * width : (i + 1) * width] for i in range(4)], axis=0
+        )
+        turned = rot[:lat]
+        swapped = jnp.concatenate([turned[:, width // 2 :], turned[:, : width // 2]], axis=1)
+        lat_rot.append(turned * tab_ref[0, core] + swapped * tab_ref[1, core])
+        ctx_rot.append(rot[lat:])
+    zeros = jnp.zeros((lat + ctx, 128 - ROPE), jnp.float32)
+    keys = jnp.concatenate(
+        [jnp.concatenate(lat_rot, axis=1), jnp.concatenate(ctx_rot, axis=1)], axis=0
+    )
+    keys = jnp.concatenate([keys, zeros], axis=1).astype(jnp.bfloat16)
+    compressed = jnp.concatenate([lat_kv, ctx_kv], axis=0)
+    for copy in range(kv_ref.shape[0]):
+        kv_ref[copy, :, :rank] = compressed
+        kv_ref[copy, :, rank:] = keys
+    for copy in range(cq_ref.shape[0]):
+        cq_ref[copy] = cq
+
+
+def attend_kernel(
+    side_ref,
+    lift_ref,
+    cq_own_ref,
+    cq_other_ref,
+    kv_own_ref,
+    kv_other_ref,
+    tab_ref,
+    wq_ref,
+    wkv_ref,
+    out_ref,
+    cq_ref,
+    kv_ref,
+    key_ref,
+    *,
+    lat,
+):
+    head = pl.program_id(0)
+    chips, count = cq_own_ref.shape[:2]
+    rank = cq_own_ref.shape[2]
+    block = kv_own_ref.shape[1]
+
+    @pl.when(head == 0)
+    def _():
+        first = side_ref[0] == 0
+        for chip in range(chips):
+            own, other = cq_own_ref[chip], cq_other_ref[chip]
+            cq_ref[2 * chip * count : (2 * chip + 1) * count] = jnp.where(first, own, other)
+            cq_ref[(2 * chip + 1) * count : (2 * chip + 2) * count] = jnp.where(first, other, own)
+            for side, ref in ((0, kv_own_ref), (1, kv_other_ref)):
+                at = (side * chips + chip) * block
+                kv_ref[at : at + block] = ref[chip, :, :rank]
+                key_ref[at : at + block, NOPE:] = ref[chip, :, rank:]
+
+    raw = jnp.dot(cq_ref[...], wq_ref[0], preferred_element_type=jnp.float32)
+    turned = raw[:, NOPE:] * tab_ref[...]
+    turned = turned + pltpu.roll(turned, ROPE, 1)
+    query = jnp.concatenate([raw[:, :NOPE], turned], axis=1).astype(jnp.bfloat16)
+    pairs = jnp.dot(kv_ref[...], wkv_ref[...], preferred_element_type=jnp.float32).astype(
+        jnp.bfloat16
+    )
+    key_ref[:, :NOPE] = pairs[:, :NOPE]
+    score = lax.dot_general(
+        query, key_ref[...], (((1,), (1,)), ((), ())), preferred_element_type=jnp.float32
+    )
+    period = lat[0] + lat[1]
+    position = lax.rem(lax.broadcasted_iota(jnp.int32, (1, score.shape[1]), 1), period)
+    lift = jnp.where(position >= lat[0], lift_ref[head], 0.0)
+    score = score * (NOPE + ROPE) ** -0.5 + lift
+    peak = jnp.max(score, axis=1, keepdims=True)
+    probs = jnp.exp(score - peak)
+    total = jnp.sum(probs, axis=1, keepdims=True)
+    summed = jnp.dot(
+        probs.astype(jnp.bfloat16), pairs[:, NOPE:], preferred_element_type=jnp.float32
+    )
+    out_ref[...] = (summed / total).astype(jnp.bfloat16)
+
+
+def output_kernel(heads_ref, w_ref, out_ref):
+    acc = jnp.dot(heads_ref[0], w_ref[0], preferred_element_type=jnp.float32)
+    acc = acc + jnp.dot(heads_ref[1], w_ref[1], preferred_element_type=jnp.float32)
+    out_ref[0] = acc.astype(jnp.bfloat16)
+
+
+def split_device(
+    latent,
+    context,
+    cond,
+    cond_ctx,
+    w_mod,
+    g_norm,
+    w_dq,
+    w_dkv,
+    w_kr,
+    g_cq,
+    g_ckv,
+    w_uq,
+    w_ukv,
+    ctx_lift,
+    w_out,
+):
+    f32, bf16 = jnp.float32, jnp.bfloat16
+    sp, tp = lax.axis_size("sp"), lax.axis_size("tp")
+    chips = tp // 2
+    rows, features = latent.shape
+    ctx_rows = context.shape[0]
+    heads = w_uq.shape[1]
+    rank = w_dq.shape[1]
+    lat, ctx = rows // tp, ctx_rows // tp
+    pairs = [[2 * i, 2 * i + 1] for i in range(chips)]
+    sides = [list(range(k, tp, 2)) for k in range(2)]
+    columns = [[s * tp + 2 * c + k for s in range(sp) for k in range(2)] for c in range(chips)]
+    me, side = lax.axis_index("tp"), lax.rem(lax.axis_index("tp"), 2)
+    across = [(i, i ^ 1) for i in range(tp)]
+
+    lat_f, ctx_f = latent.astype(f32), context.astype(f32)
+    sums = jnp.concatenate([jnp.sum(lat_f * lat_f, axis=1), jnp.sum(ctx_f * ctx_f, axis=1)])
+    sums = jnp.broadcast_to(sums[None, None], (tp, 1, sums.shape[0]))
+    sums = lax.all_to_all(sums, "tp", 0, 0)
+    signal = jnp.stack([jax.nn.silu(cond.astype(f32)), jax.nn.silu(cond_ctx.astype(f32))])
+    partial = jnp.dot(
+        signal.astype(bf16), w_mod.reshape(w_mod.shape[0], -1), preferred_element_type=f32
+    ).reshape(6, features)
+    partial = jnp.concatenate([partial, g_norm[None], jnp.zeros((1, features), f32)])
+    partial = jnp.broadcast_to(partial[None], (2 * sp,) + partial.shape)
+    partial = lax.all_to_all(partial, ("sp", "tp"), 0, 0, axis_index_groups=columns)
+    partial = partial.reshape(sp, 2, 8, features)
+
+    lat_pair = lax.all_gather(latent, "tp", axis_index_groups=pairs)
+    ctx_pair = lax.all_gather(context, "tp", axis_index_groups=pairs)
+    half = rank // 2
+    w_down = jnp.stack(
+        [
+            jnp.concatenate(
+                [
+                    w_dq[:, k * half : (k + 1) * half],
+                    w_dkv[:, k * half : (k + 1) * half],
+                    w_kr[:, k * ROPE // 2 : (k + 1) * ROPE // 2],
+                    jnp.zeros((features, 128 - ROPE // 2), bf16),
+                ],
+                axis=1,
+            )
+            for k in range(2)
+        ]
+    )
+    w_down = lax.all_to_all(w_down, "tp", 0, 0, axis_index_groups=pairs)
+    w_up = w_out.reshape(heads * DV, chips, 2, features).transpose(2, 0, 1, 3)
+    w_up = w_up.reshape(2, heads * DV, chips * features)
+    w_up = lax.all_to_all(w_up, "tp", 0, 0, axis_index_groups=pairs)
+
+    height = 2 * half // 128 * lat + half // 128 * ctx + (lat + ctx) // 4
+    part = pl.pallas_call(
+        functools.partial(project_kernel, chunks=tp),
+        out_shape=jax.ShapeDtypeStruct((tp, height, 128), f32),
+        cost_estimate=cost(4 * (rows + ctx_rows) * features * (rank + 128), 4e6),
+        name="project",
+    )(lat_pair, ctx_pair, sums, partial, w_down)
+    part = lax.all_to_all(part, "tp", 0, 0)
+
+    positions = lax.axis_index("sp") * rows + jnp.arange(rows, dtype=jnp.int32)
+    cosine, sine = tables(positions)
+    quarter = ROPE // 4
+    c0, c1, s0, s1 = cosine[:, :quarter], cosine[:, quarter:], sine[:, :quarter], sine[:, quarter:]
+    q_tab = jnp.concatenate([c0, c0, c1, c1, -s0, s0, -s1, s1], axis=1)
+    k_tab = lax.dynamic_slice_in_dim(q_tab, me * lat, lat, 0)
+    k_tab = k_tab.reshape(lat, 2, 2, ROPE // 2).transpose(1, 2, 0, 3)
+    kv, cq = pl.pallas_call(
+        functools.partial(norm_kernel, lat=lat, ctx=ctx),
+        out_shape=(
+            jax.ShapeDtypeStruct((sp, lat + ctx, rank + 128), bf16),
+            jax.ShapeDtypeStruct((chips, lat, rank), bf16),
+        ),
+        cost_estimate=cost(1e7, 2e6),
+        name="norm",
+    )(part, g_cq[None], g_ckv[None], k_tab)
+
+    cq_own = lax.all_to_all(cq, "tp", 0, 0, axis_index_groups=sides)
+    cq_other = lax.ppermute(cq_own, "tp", across)
+    kv = lax.all_to_all(kv, "sp", 0, 0).reshape(1, sp * (lat + ctx), rank + 128)
+    kv = jnp.broadcast_to(kv, (chips,) + kv.shape[1:])
+    kv_own = lax.all_to_all(kv, "tp", 0, 0, axis_index_groups=sides)
+    kv_other = lax.ppermute(kv_own, "tp", across)
+
+    w_q = jnp.transpose(w_uq, (1, 0, 2))
+    turn = w_q[..., NOPE:].reshape(heads, rank, 2, 2, quarter)[:, :, :, ::-1]
+    w_q = jnp.concatenate([w_q, turn.reshape(heads, rank, ROPE)], axis=2)
+    keys = sp * (rows + ctx_rows)
+    heads_out = pl.pallas_call(
+        functools.partial(attend_kernel, lat=(lat, ctx)),
+        grid=(heads,),
+        in_specs=[
+            pl.BlockSpec(memory_space=pltpu.SMEM),
+            pl.BlockSpec(memory_space=pltpu.SMEM),
+            whole(cq_own.shape),
+            whole(cq_own.shape),
+            whole(kv_own.shape),
+            whole(kv_own.shape),
+            whole(q_tab.shape),
+            pl.BlockSpec((1, rank, 2 * NOPE), lambda h: (h, 0, 0)),
+            pl.BlockSpec((rank, NOPE + DV), lambda h: (0, h)),
+        ],
+        out_specs=pl.BlockSpec((rows, DV), lambda h: (0, h)),
+        out_shape=jax.ShapeDtypeStruct((rows, heads * DV), bf16),
+        scratch_shapes=[
+            pltpu.VMEM((rows, rank), bf16),
+            pltpu.VMEM((keys, rank), bf16),
+            pltpu.VMEM((keys, 2 * NOPE), bf16),
+        ],
+        cost_estimate=cost(heads * 2 * keys * (rows * 384 + rank * 256), 8e6),
+        compiler_params=pltpu.CompilerParams(vmem_limit_bytes=48 << 20),
+        name="attend",
+    )(
+        side[None],
+        ctx_lift,
+        cq_own,
+        cq_other,
+        kv_own,
+        kv_other,
+        q_tab,
+        w_q,
+        w_ukv.reshape(rank, heads * (NOPE + DV)),
+    )
+
+    heads_out = lax.all_gather(heads_out, "tp", axis_index_groups=pairs)
+    branch = pl.pallas_call(
+        output_kernel,
+        grid=(chips,),
+        in_specs=[
+            whole(heads_out.shape),
+            pl.BlockSpec((2, heads * DV, features), lambda c: (0, 0, c)),
+        ],
+        out_specs=pl.BlockSpec((1, rows, features), lambda c: (c, 0, 0)),
+        out_shape=jax.ShapeDtypeStruct((chips, rows, features), bf16),
+        cost_estimate=cost(4 * rows * heads * DV * chips * features, 4e6),
+        name="project_out",
+    )(heads_out, w_up)
+    branch = lax.all_to_all(branch, "tp", 0, 0, axis_index_groups=sides)
+    gate = jnp.sum(partial, axis=0)[side, 2]
+    return (lat_f + gate * jnp.sum(branch.astype(f32), axis=0)).astype(bf16)
+
+
+def per_device(*arrays):
+    rows, ctx_rows, features = arrays[0].shape[0], arrays[1].shape[0], arrays[0].shape[1]
+    tp = lax.axis_size("tp")
+    aligned = rows % (16 * tp) == 0 and ctx_rows % (16 * tp) == 0 and features % 128 == 0
+    return (split_device if tp % 2 == 0 and aligned else plain_device)(*arrays)
+
+
 def solution(mesh):
     return jax.shard_map(
         per_device,

time: 288 us -> 164 us (0.57)
  waiting for transfers between devices: 94.6 us -> 30.7 us
  blocking collectives: 91 us -> 47.3 us
  matrix products: 40.1 us -> 0.29 us
  starting transfers between devices: 0.12 us -> 25.6 us
  Pallas kernels: 0 us -> 23.5 us
  between operations: 13.3 us -> 0.36 us
  other arithmetic: 14.7 us -> 2.8 us
    psum x3 -> x0, blocking collectives: 48.3 us -> none  [the longest x1 22.7 us: per_device(): lax.psum((jnp.dot(lat_h, w_dq, preferred_element_type=jnp.float32), jnp.d...]
    psum x1 -> x0, waiting for transfers between devices: 44.7 us -> none  [per_device(): lax.psum((jnp.dot(lat_h, w_dq, preferred_element_type=jnp.float32), jnp.d...]
    all_to_all x0 -> x3, blocking collectives: none -> 40.3 us  [the longest x1 20.4 us: split_device(): kv_own = lax.all_to_all(kv, 'tp', 0, 0, axis_index_groups=sides)]
    dot_general x23 -> x1, matrix products: 40.1 us -> 0.29 us  [split_device(): jnp.dot(signal.astype(bf16), w_mod.reshape(w_mod.shape[0], -1), preferred...]
    reduce_scatter x1 -> x0, waiting for transfers between devices: 37.2 us -> none  [per_device(): lax.psum_scatter(branch.astype(jnp.bfloat16), 'tp', scatter_dimension=1,...]
    all_gather x3, blocking collectives: 42.7 us -> 6.99 us  [the longest x1 2.61 us: split_device(): heads_out = lax.all_gather(heads_out, 'tp', axis_index_groups=pairs)]
    all_to_all x0 -> x6, waiting for transfers between devices: none -> 30.7 us  [the longest x1 12.3 us: split_device(): part = lax.all_to_all(part, 'tp', 0, 0)]
    all_to_all x0 -> x6, starting transfers between devices: none -> 25.6 us  [the longest x1 5.2 us: split_device(): sums = lax.all_to_all(sums, 'tp', 0, 0)]
  transfers between devices with their start and end apart: 3 -> 8, of which waited for: 3 -> 5; matrix products, arithmetic and copies ran while one was open for 5% -> 17% of each run, Pallas kernels for 0% -> 8%
where the time goes in v1:
time: 164 us; the launch traced here: 162 us
  blocking collectives  47.3 us (29%)
  local copies, waits for them, and re-layouts  31.9 us (19%)
  waiting for transfers between devices  30.7 us (19%)
  starting transfers between devices  25.6 us (16%)
  Pallas kernels  23.5 us (14%)
  other arithmetic  2.8 us (2%)
    all_to_all x1, blocking collectives, split_device(): kv_own = lax.all_to_all(kv, 'tp', 0, 0, axis_index_groups=sides)  20.4 us
    pallas_call x1, Pallas kernels, split_device(): pl.pallas_call(functools.partial(attend_kernel, lat=(lat, ctx)), grid=(he...  13.7 us
    all_to_all x1, waiting for transfers between devices, split_device(): part = lax.all_to_all(part, 'tp', 0, 0)  12.3 us
    all_to_all x1, waiting for transfers between devices, split_device(): branch = lax.all_to_all(branch, 'tp', 0, 0, axis_index_groups=sides)  11.6 us
    all_to_all x1, blocking collectives, split_device(): kv = lax.all_to_all(kv, 'sp', 0, 0).reshape(1, sp * (lat + ctx), rank + 128)  11.4 us
    all_to_all x1, blocking collectives, split_device(): cq_own = lax.all_to_all(cq, 'tp', 0, 0, axis_index_groups=sides)  8.49 us
    reshape x2, local copies, waits for them, and re-layouts, split_device(): w_up = w_out.reshape(heads * DV, chips, 2, features).transpose(2, 0, 1, 3)  8.25 us
    unnamed x35, local copies, waits for them, and re-layouts  6.08 us
  transfers between devices with their start and end apart: 8, of which 5 were waited for; matrix products, arithmetic and copies ran while one was open for 17% of the time, Pallas kernels for 8%

profile of v1, /device:TPU:0, one launch (start us, length us, event | category | flops | bytes accessed | tf_op | source)
XLA Modules:
  0.0 162.5 jit_solution(9309504358717832943)
XLA Ops:
  0.0 0.7 fusion.23
  0.7 0.1 copy.40
  0.9 0.1 copy.41
  1.0 0.1 pad.13.clone
  1.1 1.1 fusion.18
  2.2 0.0 copy-start.9
  2.2 0.0 copy-start.13
  2.2 0.0 copy-start.14
  2.2 0.0 copy-start.5
  2.3 0.1 maximum_bitcast_fusion
  2.4 0.9 pad_maximum_fusion.1
  3.3 3.6 %all-to-all-start.2 = ((bf16[2,256,640]{2,1,0:T(8,128)(2,1)}), bf16[2,256,640]{2,1,0:T(8,128)(2,1)S(1)}, u32[]{:S(2)}, u32[]{:S(2)}) async-start(bf16[2,256,640]{2,1,0:T(8,128)(2,1)} %pad_maximum_fusion.1), calls=%async_computation.2 | async-start | bytes 1310720 | tf_op jit(solution)/shard_map/all_to_all | solution.py:433
  7.0 0.1 multiply_reduce_fusion
  7.2 0.1 fusion
  7.4 0.3 copy.29
  7.7 0.3 fusion.10
  8.0 0.1 pad.18.clone
  8.1 0.1 broadcast_multiply_fusion.1
  8.1 0.7 all-to-all-done.2.w_ref
  8.8 0.7 broadcast_in_dim.42
  9.5 5.2 %all-to-all-start.1 = ((f32[8,1,512]{2,1,0:T(1,128)}), f32[8,1,512]{2,1,0:T(1,128)S(1)}, u32[]{:S(2)}, u32[]{:S(2)}) async-start(f32[8,1,512]{2,1,0:T(1,128)} %broadcast_in_dim.42), calls=%async_computation.1 | async-start | bytes 32768 | tf_op jit(solution)/shard_map/all_to_all | solution.py:406
  14.7 0.1 maximum_maximum_fusion
  14.7 4.7 %all-to-all-done.1.sq_ref = f32[8,1,512]{2,1,0:T(1,128)S(1)} async-done(((f32[8,1,512]{2,1,0:T(1,128)}), f32[8,1,512]{2,1,0:T(1,128)S(1)}, u32[]{:S(2)}, u32[]{:S(2)}) %all-to-all-start.1) | async-done | bytes 16416 | tf_op jit(solution)/shard_map/all_to_all | solution.py:406
  19.4 0.6 broadcast_in_dim.40
  20.1 4.9 %all-to-all-start = ((f32[8,8,256]{2,1,0:T(8,128)}), f32[8,8,256]{2,1,0:T(8,128)S(1)}, u32[]{:S(2)}, u32[]{:S(2)}) async-start(f32[8,8,256]{2,1,0:T(8,128)} %broadcast_in_dim.40), calls=%async_computation | async-start | bytes 131072 | tf_op jit(solution)/shard_map/all_to_all | solution.py:413
  24.9 2.2 %all-gather.1 = bf16[256,256]{1,0:T(8,128)(2,1)} all-gather(bf16[128,256]{1,0:T(8,128)(2,1)S(1)} %copy-done.9), channel_id=3, replica_groups={{0,1},{2,3},{4,5},{6,7},{8,9},{10,11},{12,13},{14,15},{16,17},{18,19},{..., dimensions={0}, use_global_device_ids=true | all-gather | bytes 196608 | tf_op jit(solution)/shard_map/all_gather | solution.py:417
  27.1 2.2 %all-gather = bf16[768,256]{1,0:T(8,128)(2,1)} all-gather(bf16[384,256]{1,0:T(8,128)(2,1)S(1)} %copy-done.5), channel_id=2, replica_groups={{0,1},{2,3},{4,5},{6,7},{8,9},{10,11},{12,13},{14,15},{16,17},{18,19},{..., dimensions={0}, use_global_device_ids=true | all-gather | bytes 589824 | tf_op jit(solution)/shard_map/all_gather | solution.py:416
  29.3 1.5 all-to-all-done
  30.9 0.6 copy-done.7
  31.5 3.1 %project.1 = f32[8,240,128]{2,1,0:T(8,128)} custom-call(bf16[2,384,256]{2,1,0:T(8,128)(2,1)} %bitcast.33, bf16[2,128,256]{2,1,0:T(8,128)(2,1)} %bitcast.40, f32[8,1,512]{2,1,0:T(1,128)} %copy-done.11, f32[4,2,8,256]{3,2,1,0:T(8,128)} %bitcast.38, bf16[2,256,640]{2,1,0:T(8,128)(2,1)} %copy-done.3), custom_call_target="tpu_custom_call" | custom-call | flops 335544320 | bytes 4000000 | tf_op jit(solution)/shard_map/project/pallas_call | solution.py:439
  34.6 3.6 %all-to-all-start.3 = ((f32[8,240,128]{2,1,0:T(8,128)}), f32[8,240,128]{2,1,0:T(8,128)S(1)}, u32[]{:S(2)}, u32[]{:S(2)}) async-start(f32[8,240,128]{2,1,0:T(8,128)} %project.1), calls=%async_computation.3 | async-start | bytes 1966080 | tf_op jit(solution)/shard_map/all_to_all | solution.py:445
  38.2 0.1 copy.32
  38.3 0.7 fusion.21
  39.0 0.1 fusion.22
  39.1 0.1 fusion.20
  39.3 0.4 concatenate.26.tab_ref
  39.7 0.1 copy.34
  39.8 0.7 copy.35
  40.5 12.3 %all-to-all-done.3.part_ref = f32[8,240,128]{2,1,0:T(8,128)S(1)} async-done(((f32[8,240,128]{2,1,0:T(8,128)}), f32[8,240,128]{2,1,0:T(8,128)S(1)}, u32[]{:S(2)}, u32[]{:S(2)}) %all-to-all-start.3) | async-done | bytes 983072 | tf_op jit(solution)/shard_map/all_to_all | solution.py:445
  52.8 1.0 copy-done.2
  53.8 2.2 %norm.1 = (bf16[4,64,640]{2,1,0:T(8,128)(2,1)}, bf16[4,48,512]{2,1,0:T(8,128)(2,1)}) custom-call(f32[8,240,128]{2,1,0:T(8,128)} %copy-done.2, f32[1,512]{1,0:T(1,128)} %bitcast.44, f32[1,512]{1,0:T(1,128)} %bitcast.45, f32[2,2,48,32]{3,2,1,0:T(8,128)} %bitcast.41), custom_call_target="tpu_custom_call" | custom-call | flops 10000000 | bytes 2000000 | tf_op jit(solution)/shard_map/norm/pallas_call | solution.py:454
  56.0 11.4 %all_to_all.45 = bf16[4,64,640]{2,1,0:T(8,128)(2,1)S(1)} all-to-all(bf16[4,64,640]{2,1,0:T(8,128)(2,1)} %get-tuple-element.8), channel_id=1, replica_groups=mesh['sp'=4,'tp'=8] {'sp'}, dimensions={0} | all-to-all | bytes 655360 | tf_op jit(solution)/shard_map/all_to_all | solution.py:466
  67.4 0.1 broadcast_in_dim.46
  67.5 20.4 %all_to_all.46.kv_own_ref = bf16[4,256,640]{2,1,0:T(8,128)(2,1)S(1)} all-to-all(bf16[4,256,640]{2,1,0:T(8,128)(2,1)S(1)} %broadcast_in_dim.46), channel_id=1, replica_groups={{0,2,4,6},{1,3,5,7},{8,10,12,14},{9,11,13,15},{16,18,20,22},{17,19,21,2..., dimensions={0} | all-to-all | bytes 2621440 | tf_op jit(solution)/shard_map/all_to_all | solution.py:468
  87.9 8.5 %all_to_all.47.cq_own_ref = bf16[4,48,512]{2,1,0:T(8,128)(2,1)S(1)} all-to-all(bf16[4,48,512]{2,1,0:T(8,128)(2,1)S(1)} %copy-done.10), channel_id=1, replica_groups={{0,2,4,6},{1,3,5,7},{8,10,12,14},{9,11,13,15},{16,18,20,22},{17,19,21,2..., dimensions={0} | all-to-all | bytes 393216 | tf_op jit(solution)/shard_map/all_to_all | solution.py:464
  96.4 4.5 %reshape.81 = bf16[512,4,2,256]{3,2,1,0:T(2,128)(2,1)} reshape(bf16[4,128,2048]{2,1,0:T(8,128)(2,1)} %param.29) | data formatting | bytes 4194304 | tf_op jit(solution)/shard_map/reshape | solution.py:434
  100.9 3.8 %copy.44 = bf16[512,4,2,256]{3,1,0,2:T(4,128)(2,1)} copy(bf16[512,4,2,256]{3,2,1,0:T(2,128)(2,1)} %reshape.81) | data formatting | bytes 4194304 | tf_op jit(solution)/shard_map/reshape | solution.py:434
  104.6 4.5 %reshape.82 = bf16[2,512,1024]{2,1,0:T(8,128)(2,1)} reshape(bf16[2,512,4,256]{3,2,1,0:T(4,128)(2,1)} %bitcast.28) | data formatting | bytes 4194304 | tf_op jit(solution)/shard_map/reshape | solution.py:435
  109.1 4.8 %all-to-all-start.7 = ((bf16[2,512,1024]{2,1,0:T(8,128)(2,1)}), bf16[2,512,1024]{2,1,0:T(8,128)(2,1)}, u32[]{:S(2)}, u32[]{:S(2)}) async-start(bf16[2,512,1024]{2,1,0:T(8,128)(2,1)} %reshape.82), calls=%async_computation.7 | async-start | bytes 4194304 | tf_op jit(solution)/shard_map/all_to_all | solution.py:436
  113.9 2.2 %copy.36 = bf16[512,4,192]{2,0,1:T(8,128)(2,1)} copy(bf16[512,4,192]{0,2,1:T(8,128)(2,1)} %param.26) | data formatting | bytes 1572864 | tf_op args[11]
  116.2 1.9 %slice.49 = bf16[4,512,64]{2,1,0:T(8,128)(2,1)} slice(bf16[4,512,192]{2,1,0:T(8,128)(2,1)} %bitcast.29), slice={[0:4], [0:512], [128:192]} | slice | bytes 524288 | tf_op jit(solution)/shard_map/slice | solution.py:472
  118.0 1.9 %copy.37 = bf16[4,512,64]{1,2,0:T(8,128)(2,1)} copy(bf16[4,512,64]{2,1,0:T(8,128)(2,1)} %slice.49) | data formatting | bytes 524288 | tf_op jit(solution)/shard_map/slice | solution.py:472
  120.0 1.7 %rev.3 = bf16[4,512,2,2,16]{1,4,3,2,0:T(8,128)(2,1)} reverse(bf16[4,512,2,2,16]{1,4,3,2,0:T(8,128)(2,1)} %bitcast.35), dimensions={3} | reverse | bytes 524288 | tf_op jit(solution)/shard_map/rev | solution.py:472
  121.7 2.0 %copy.38 = bf16[4,512,64]{2,1,0:T(8,128)(2,1)} copy(bf16[4,512,64]{1,2,0:T(8,128)(2,1)} %bitcast.36) | data formatting | bytes 524288 | tf_op jit(solution)/shard_map/reshape | solution.py:473
  123.6 1.6 copy.42
  125.2 0.1 copy-done.4
  125.3 0.3 pad_maximum_fusion.wq_ref
  125.7 13.7 %attend.1 = bf16[384,512]{1,0:T(8,128)(2,1)S(1)} custom-call(s32[1]{0:T(128)} %bitcast.4.side_ref, f32[4]{0:T(128)S(1)} %copy-done, bf16[4,48,512]{2,1,0:T(8,128)(2,1)S(1)} %all_to_all.47.cq_own_ref, bf16[4,48,512]{2,1,0:T(8,128)(2,1)S(1)} %collective-permute-done.cq_other_ref, bf16[4,256,640]{2,1,0:T(8,128)(2,1)S(1)} %all_to_all.46.kv_own_ref, ...), custom_call_target="tpu_custom_call" | custom-call | flops 4563402752 | bytes 8000000 | tf_op jit(solution)/shard_map/attend/pallas_call | solution.py:475
  139.4 2.6 %all-gather.2 = bf16[768,512]{1,0:T(8,128)(2,1)} all-gather(bf16[384,512]{1,0:T(8,128)(2,1)S(1)} %attend.1), channel_id=4, replica_groups={{0,1},{2,3},{4,5},{6,7},{8,9},{10,11},{12,13},{14,15},{16,17},{18,19},{..., dimensions={0}, use_global_device_ids=true | all-gather | bytes 1179648 | tf_op jit(solution)/shard_map/all_gather | solution.py:511
  142.0 4.5 %project_out.1 = bf16[4,384,256]{2,1,0:T(8,128)(2,1)} custom-call(bf16[2,384,512]{2,1,0:T(8,128)(2,1)} %bitcast.31, bf16[2,512,1024]{2,1,0:T(8,128)(2,1)} %all-to-all-done.7.w_ref), custom_call_target="tpu_custom_call" | custom-call | flops 805306368 | bytes 4000000 | tf_op jit(solution)/shard_map/project_out/pallas_call | solution.py:512
  146.5 3.5 %all-to-all-start.8 = ((bf16[4,384,256]{2,1,0:T(8,128)(2,1)}), bf16[4,384,256]{2,1,0:T(8,128)(2,1)S(1)}, u32[]{:S(2)}, u32[]{:S(2)}) async-start(bf16[4,384,256]{2,1,0:T(8,128)(2,1)} %project_out.1), calls=%async_computation.8 | async-start | bytes 1572864 | tf_op jit(solution)/shard_map/all_to_all | solution.py:524
  150.1 11.6 %all-to-all-done.8 = bf16[4,384,256]{2,1,0:T(8,128)(2,1)S(1)} async-done(((bf16[4,384,256]{2,1,0:T(8,128)(2,1)}), bf16[4,384,256]{2,1,0:T(8,128)(2,1)S(1)}, u32[]{:S(2)}, u32[]{:S(2)}) %all-to-all-start.8) | async-done | bytes 786464 | tf_op jit(solution)/shard_map/all_to_all | solution.py:524
  161.6 0.1 convert_reduce_fusion
  161.7 0.7 fusion.1
  (41 shorter events, 0.2 us)
Async XLA Ops:
  2.2 4.8 %copy-start.9 = (bf16[128,256]{1,0:T(8,128)(2,1)S(1)}, bf16[128,256]{1,0:T(8,128)(2,1)}, u32[]{:S(2)}) copy-start(bf16[128,256]{1,0:T(8,128)(2,1)} %param.16) | copy-start | bytes 196612
  2.2 4.9 %copy-start.13 = (bf16[512]{0:T(512)(128)(2,1)S(1)}, bf16[512]{0:T(512)(128)(2,1)}, u32[]{:S(2)}) copy-start(bf16[512]{0:T(512)(128)(2,1)} %param.17) | copy-start | bytes 3076
  2.2 4.9 %copy-start.14 = (bf16[512]{0:T(512)(128)(2,1)S(1)}, bf16[512]{0:T(512)(128)(2,1)}, u32[]{:S(2)}) copy-start(bf16[512]{0:T(512)(128)(2,1)} %param.18) | copy-start | bytes 3076
  2.2 5.0 %copy-start.5 = (bf16[384,256]{1,0:T(8,128)(2,1)S(1)}, bf16[384,256]{1,0:T(8,128)(2,1)}, u32[]{:S(2)}) copy-start(bf16[384,256]{1,0:T(8,128)(2,1)} %param.15) | copy-start | bytes 589828
  2.2 5.1 %copy-start.6 = (bf16[512,3,256]{2,0,1:T(8,128)(2,1)S(1)}, bf16[512,3,256]{2,0,1:T(8,128)(2,1)}, u32[]{:S(2)}) copy-start(bf16[512,3,256]{2,0,1:T(8,128)(2,1)} %param.19) | copy-start | bytes 2359300
  3.3 11.3 %copy-start.12 = (f32[256]{0:T(256)S(1)}, f32[256]{0:T(256)}, u32[]{:S(2)}) copy-start(f32[256]{0:T(256)} %param.20) | copy-start | bytes 3076
  3.3 5.5 %all-to-all-start.2 = ((bf16[2,256,640]{2,1,0:T(8,128)(2,1)}), bf16[2,256,640]{2,1,0:T(8,128)(2,1)S(1)}, u32[]{:S(2)}, u32[]{:S(2)}) async-start(bf16[2,256,640]{2,1,0:T(8,128)(2,1)} %pad_maximum_fusion.1), calls=%async_computation.2 | async-start | bytes 1310720 | tf_op jit(solution)/shard_map/all_to_all | solution.py:433
  8.8 22.1 %copy-start.3 = (bf16[2,256,640]{2,1,0:T(8,128)(2,1)}, bf16[2,256,640]{2,1,0:T(8,128)(2,1)S(1)}, u32[]{:S(2)}) copy-start(bf16[2,256,640]{2,1,0:T(8,128)(2,1)S(1)} %all-to-all-done.2.w_ref) | copy-start | bytes 1966084
  9.5 10.0 %all-to-all-start.1 = ((f32[8,1,512]{2,1,0:T(1,128)}), f32[8,1,512]{2,1,0:T(1,128)S(1)}, u32[]{:S(2)}, u32[]{:S(2)}) async-start(f32[8,1,512]{2,1,0:T(1,128)} %broadcast_in_dim.42), calls=%async_computation.1 | async-start | bytes 32768 | tf_op jit(solution)/shard_map/all_to_all | solution.py:406
  19.4 11.4 %copy-start.11 = (f32[8,1,512]{2,1,0:T(1,128)}, f32[8,1,512]{2,1,0:T(1,128)S(1)}, u32[]{:S(2)}) copy-start(f32[8,1,512]{2,1,0:T(1,128)S(1)} %all-to-all-done.1.sq_ref) | copy-start | bytes 49156
  20.1 10.8 %all-to-all-start = ((f32[8,8,256]{2,1,0:T(8,128)}), f32[8,8,256]{2,1,0:T(8,128)S(1)}, u32[]{:S(2)}, u32[]{:S(2)}) async-start(f32[8,8,256]{2,1,0:T(8,128)} %broadcast_in_dim.40), calls=%async_computation | async-start | bytes 131072 | tf_op jit(solution)/shard_map/all_to_all | solution.py:413
  30.8 0.6 copy-start.7
  34.6 18.2 %all-to-all-start.3 = ((f32[8,240,128]{2,1,0:T(8,128)}), f32[8,240,128]{2,1,0:T(8,128)S(1)}, u32[]{:S(2)}, u32[]{:S(2)}) async-start(f32[8,240,128]{2,1,0:T(8,128)} %project.1), calls=%async_computation.3 | async-start | bytes 1966080 | tf_op jit(solution)/shard_map/all_to_all | solution.py:445
  52.8 1.0 copy-start.2
  67.4 20.5 %copy-start.10 = (bf16[4,48,512]{2,1,0:T(8,128)(2,1)S(1)}, bf16[4,48,512]{2,1,0:T(8,128)(2,1)}, u32[]{:S(2)}) copy-start(bf16[4,48,512]{2,1,0:T(8,128)(2,1)} %get-tuple-element.7) | copy-start | bytes 589828
  87.9 37.8 %collective-permute-start.1 = (bf16[4,256,640]{2,1,0:T(8,128)(2,1)S(1)}, bf16[4,256,640]{2,1,0:T(8,128)(2,1)S(1)}, u32[]{:S(2)}, u32[]{:S(2)}) collective-permute-start(bf16[4,256,640]{2,1,0:T(8,128)(2,1)S(1)} %all_to_all.46.kv_own_ref), channel_id=1, source_target_pairs={{0,1},{1,0},{2,3},{3,2},{4,5},{5,4},{6,7},{7,6},{8,9},{9,8},{10,11... | collective-permute-start | bytes 3932168 | tf_op jit(solution)/shard_map/ppermute | solution.py:469
  96.4 29.3 %collective-permute-start = (bf16[4,48,512]{2,1,0:T(8,128)(2,1)S(1)}, bf16[4,48,512]{2,1,0:T(8,128)(2,1)S(1)}, u32[]{:S(2)}, u32[]{:S(2)}) collective-permute-start(bf16[4,48,512]{2,1,0:T(8,128)(2,1)S(1)} %all_to_all.47.cq_own_ref), channel_id=1, source_target_pairs={{0,1},{1,0},{2,3},{3,2},{4,5},{5,4},{6,7},{7,6},{8,9},{9,8},{10,11... | collective-permute-start | bytes 589832 | tf_op jit(solution)/shard_map/ppermute | solution.py:465
  109.1 32.9 %all-to-all-start.7 = ((bf16[2,512,1024]{2,1,0:T(8,128)(2,1)}), bf16[2,512,1024]{2,1,0:T(8,128)(2,1)}, u32[]{:S(2)}, u32[]{:S(2)}) async-start(bf16[2,512,1024]{2,1,0:T(8,128)(2,1)} %reshape.82), calls=%async_computation.7 | async-start | bytes 4194304 | tf_op jit(solution)/shard_map/all_to_all | solution.py:436
  123.6 1.6 copy-start.1
  123.6 1.7 %copy-start.4 = (bf16[4,512,64]{2,1,0:T(8,128)(2,1)S(1)}, bf16[4,512,64]{2,1,0:T(8,128)(2,1)}, u32[]{:S(2)}) copy-start(bf16[4,512,64]{2,1,0:T(8,128)(2,1)} %copy.38) | copy-start | bytes 786436
  123.6 2.0 %copy-start = (f32[4]{0:T(128)S(1)}, f32[4]{0:T(128)}, u32[]{:S(2)}) copy-start(f32[4]{0:T(128)} %lift_ref.1) | copy-start | bytes 52
  142.0 8.0 %copy-start.8 = (f32[8,8,256]{2,1,0:T(8,128)S(1)}, f32[8,8,256]{2,1,0:T(8,128)}, u32[]{:S(2)}) copy-start(f32[8,8,256]{2,1,0:T(8,128)} %copy-done.7) | copy-start | bytes 196612
  146.5 15.1 %all-to-all-start.8 = ((bf16[4,384,256]{2,1,0:T(8,128)(2,1)}), bf16[4,384,256]{2,1,0:T(8,128)(2,1)S(1)}, u32[]{:S(2)}, u32[]{:S(2)}) async-start(bf16[4,384,256]{2,1,0:T(8,128)(2,1)} %project_out.1), calls=%async_computation.8 | async-start | bytes 1572864 | tf_op jit(solution)/shard_map/all_to_all | solution.py:524

commit v2 on v0

--- a/solution.py
+++ b/solution.py
@@ -1,6 +1,10 @@
+import functools
+
 import jax
 import jax.numpy as jnp
 from jax import lax
+from jax.experimental import pallas as pl
+from jax.experimental.pallas import tpu as pltpu
 from jax.sharding import PartitionSpec as P
 
 D = 2048
@@ -48,7 +52,7 @@
     return (values * scale * gain).astype(jnp.bfloat16)
 
 
-def per_device(
+def plain_device(
     latent,
     context,
     cond,
@@ -188,6 +192,477 @@
     return (lat_f + modulation[0, 2] * branch).astype(jnp.bfloat16)
 
 
+def call(kernel, outs, *args, flops=1e6, scratch=(), limit=8, name=None, held=True, kept=True):
+    single = not isinstance(outs, tuple)
+    vmem = pl.BlockSpec(memory_space=pltpu.VMEM)
+    outs = (outs,) if single else outs
+    if kept:
+        outs = tuple(pltpu.VMEM(o.shape, o.dtype) for o in outs)
+    if held:
+        args = tuple(pltpu.with_memory_space_constraint(a, pltpu.VMEM) for a in args)
+    result = pl.pallas_call(
+        kernel,
+        in_specs=[vmem] * len(args),
+        out_specs=(vmem,) * len(outs),
+        out_shape=outs,
+        scratch_shapes=scratch,
+        cost_estimate=pl.CostEstimate(
+            flops=int(flops), bytes_accessed=int(1e5), transcendentals=0
+        ),
+        compiler_params=pltpu.CompilerParams(vmem_limit_bytes=limit << 20),
+        name=name,
+    )(*args)
+    return result[0] if single else result
+
+
+def place():
+    me = lax.axis_index("tp")
+    return lax.axis_index("sp") * lax.axis_size("tp"), me // 2, lax.rem(me, 2), me
+
+
+def dot_t(left, right, **options):
+    return lax.dot_general(
+        left, right, (((1,), (1,)), ((), ())), preferred_element_type=jnp.float32, **options
+    )
+
+
+def share_kernel(wq_ref, wkv_ref, wr_ref, own_ref, other_ref):
+    features, rank = wq_ref.shape
+    half, width = rank // 2, ROPE // 2
+    side = place()[2]
+    for which, ref in ((side, own_ref), (1 - side, other_ref)):
+        start = pl.multiple_of(which * half, half)
+        ref[:features, :half] = wq_ref[:, pl.ds(start, half)]
+        ref[:features, half:] = wkv_ref[:, pl.ds(start, half)]
+        low = pl.multiple_of(which * width, width)
+        rot = wr_ref[pl.ds(low, width), :]
+        count = width * features // rank
+        for i in range(rank // features):
+            ref[features:, i * features : (i + 1) * features] = rot[i * count : (i + 1) * count]
+
+
+def stats_kernel(lat_ref, ctx_ref, cond_ref, cond_ctx_ref, w_ref, g_ref, out_ref, rows_ref, *, sp, tp):
+    chip = place()[1]
+    features = lat_ref.shape[1]
+    size = out_ref.shape[2]
+    rows_ref[: lat_ref.shape[0]] = lat_ref[...]
+    rows_ref[lat_ref.shape[0] :] = ctx_ref[...]
+    ones = jnp.ones((8, features), jnp.float32)
+    sums = []
+    for ref in (lat_ref, ctx_ref):
+        values = ref[...].astype(jnp.float32)
+        sums.append(dot_t(ones, values * values, precision=lax.Precision.HIGHEST)[:1])
+    sums.append(jnp.zeros((1, size - lat_ref.shape[0] - ctx_ref.shape[0]), jnp.float32))
+    sums = jnp.concatenate(sums, axis=1)
+    lat_c = jax.nn.silu(cond_ref[...].astype(jnp.float32))
+    ctx_c = jax.nn.silu(cond_ctx_ref[...].astype(jnp.float32))
+    row = lax.broadcasted_iota(jnp.int32, (16, lat_c.shape[1]), 0)
+    signal = jnp.where(row < 8, lat_c, ctx_c).astype(jnp.bfloat16)
+    parts = [jnp.dot(signal, w_ref[j], preferred_element_type=jnp.float32) for j in range(3)]
+    gain = g_ref[...]
+    gains = parts[1] * gain + gain * (1.0 / sp)
+    modulation = jnp.concatenate(
+        [
+            parts[0][:1],
+            gains[:1],
+            parts[0][8:9],
+            gains[8:9],
+            parts[2][:1],
+            jnp.zeros((1, size - 5 * features), jnp.float32),
+        ][: 5 if size == 5 * features else 6],
+        axis=1,
+    )
+    for d in range(sp * tp):
+        out_ref[d] = jnp.where((d % tp) // 2 == chip, modulation, sums)
+
+
+def project_kernel(
+    own_ref, other_ref, stat_ref, w_own_ref, w_other_ref, out_ref, gate_ref, *, sp, tp, rows
+):
+    count, features = own_ref.shape
+    ctx_rows = count - rows
+    rank = w_own_ref.shape[1]
+    half, width = rank // 2, ROPE // 2
+    base, chip, side, me = place()
+    apart = jnp.zeros((1, count), jnp.float32)
+    for t in range(tp):
+        term = stat_ref[base + t][:, :count]
+        apart = apart + jnp.where(chip == t // 2, jnp.zeros_like(term), term)
+    apart = jnp.transpose(jnp.broadcast_to(apart, (8, count)))[:, :1]
+    mine, partner = stat_ref[me], stat_ref[me + 1 - 2 * side]
+    for s in range(1, sp):
+        mine = mine + stat_ref[s * tp + me]
+        partner = partner + stat_ref[s * tp + me + 1 - 2 * side]
+    gate_ref[...] = mine[:, 4 * features : 5 * features]
+
+    def split(ref):
+        packed = ref[features:]
+        rot = [packed[:, i * features : (i + 1) * features] for i in range(rank // features)]
+        return ref[:features, :half], ref[:features, half:], jnp.concatenate(rot, axis=0)
+
+    w_own, w_other = split(w_own_ref), split(w_other_ref)
+
+    def rows_of(part, apart, kind):
+        own, other = own_ref[part].astype(jnp.float32), other_ref[part].astype(jnp.float32)
+        total = jnp.sum(own * own + other * other, axis=1, keepdims=True) + apart
+        inverse = lax.rsqrt(total / D + EPS)
+        first = second = rot = None
+        for values, vectors, weights in ((own, mine, w_own), (other, partner, w_other)):
+            shift = vectors[:, 2 * kind * features : (2 * kind + 1) * features]
+            gain = vectors[:, (2 * kind + 1) * features : (2 * kind + 2) * features]
+            h = (values * inverse * gain + shift).astype(jnp.bfloat16)
+            terms = [None if kind else jnp.dot(h, weights[0], preferred_element_type=jnp.float32)]
+            terms.append(jnp.dot(h, weights[1], preferred_element_type=jnp.float32))
+            terms.append(dot_t(h, weights[2]))
+            if second is None:
+                first, second, rot = terms
+            else:
+                first = None if kind else first + terms[0]
+                second, rot = second + terms[1], rot + terms[2]
+        return first, second, rot
+
+    lat_q, lat_kv, lat_rot = rows_of(slice(0, rows), apart[:rows], 0)
+    unused, ctx_kv, ctx_rot = rows_of(slice(rows, count), apart[rows:], 1)
+    lat, ctx = rows // tp, ctx_rows // tp
+    quarter = (lat + ctx) // 4
+    for d in range(tp):
+        at = 0
+        for source, size in ((lat_q, lat), (lat_kv, lat), (ctx_kv, ctx)):
+            for slab in range(half // 128):
+                out_ref[d, at : at + size, :] = source[
+                    d * size : (d + 1) * size, slab * 128 : (slab + 1) * 128
+                ]
+                at += size
+        rot = jnp.concatenate(
+            [lat_rot[d * lat : (d + 1) * lat], ctx_rot[d * ctx : (d + 1) * ctx]], axis=0
+        )
+        out_ref[d, at : at + quarter, :] = jnp.concatenate(
+            [rot[i * quarter : (i + 1) * quarter] for i in range(4)], axis=1
+        )
+
+
+def norm_kernel(part_ref, gq_ref, gkv_ref, tab_ref, kv_ref, cq_ref, *, lat, ctx):
+    chips = part_ref.shape[0] // 2
+    halves = []
+    for core in range(2):
+        acc = part_ref[core]
+        for chip in range(1, chips):
+            acc = acc + part_ref[2 * chip + core]
+        halves.append(acc)
+    rank = gq_ref.shape[1]
+    slabs = rank // 256
+
+    def columns(start, count):
+        return jnp.concatenate(
+            [
+                half[start + i * count : start + (i + 1) * count]
+                for half in halves
+                for i in range(slabs)
+            ],
+            axis=1,
+        )
+
+    def normed(values, gain):
+        factor = lax.rsqrt(jnp.mean(values * values, axis=1, keepdims=True) + EPS)
+        return (values * factor * gain).astype(jnp.bfloat16)
+
+    cq = normed(columns(0, lat), gq_ref[...])
+    lat_kv = normed(columns(slabs * lat, lat), gkv_ref[...])
+    at = 2 * slabs * lat
+    ctx_kv = normed(columns(at, ctx), gkv_ref[...])
+    at += slabs * ctx
+    quarter = (lat + ctx) // 4
+    width = ROPE // 2
+    lat_rot, ctx_rot = [], []
+    for core in range(2):
+        packed = halves[core][at : at + quarter]
+        rot = jnp.concatenate(
+            [packed[:, i * width : (i + 1) * width] for i in range(4)], axis=0
+        )
+        turned = rot[:lat]
+        swapped = jnp.concatenate([turned[:, width // 2 :], turned[:, : width // 2]], axis=1)
+        lat_rot.append(turned * tab_ref[0, core] + swapped * tab_ref[1, core])
+        ctx_rot.append(rot[lat:])
+    zeros = jnp.zeros((lat + ctx, 128 - ROPE), jnp.float32)
+    keys = jnp.concatenate(
+        [jnp.concatenate(lat_rot, axis=1), jnp.concatenate(ctx_rot, axis=1)], axis=0
+    )
+    keys = jnp.concatenate([keys, zeros], axis=1).astype(jnp.bfloat16)
+    compressed = jnp.concatenate([lat_kv, ctx_kv], axis=0)
+    for copy in range(kv_ref.shape[0]):
+        kv_ref[copy, :, :rank] = compressed
+        kv_ref[copy, :, rank:] = keys
+    cq_ref[...] = cq
+
+
+def query_kernel(own_ref, other_ref, tab_ref, w_ref, out_ref, cq_ref):
+    chips, count = own_ref.shape[:2]
+    unused, here, side, unused = place()
+    first = side == 0
+    for chip in range(chips):
+        own, other = own_ref[chip ^ here], other_ref[chip ^ here]
+        at = 2 * chip * count
+        cq_ref[at : at + count] = jnp.where(first, own, other)
+        cq_ref[at + count : at + 2 * count] = jnp.where(first, other, own)
+    quarter = ROPE // 4
+    for head in range(w_ref.shape[0]):
+        pieces = [w_ref[head]]
+        for block in (1, 0, 3, 2):
+            pieces.append(w_ref[head, NOPE + block * quarter : NOPE + (block + 1) * quarter])
+        raw = dot_t(cq_ref[...], jnp.concatenate(pieces, axis=0))
+        turned = raw[:, NOPE:] * tab_ref[...]
+        turned = turned + pltpu.roll(turned, ROPE, 1)
+        out_ref[head] = jnp.concatenate([raw[:, :NOPE], turned], axis=1).astype(jnp.bfloat16)
+
+
+def expand_kernel(kv_ref, w_ref, out_ref):
+    rank = w_ref.shape[0]
+    values = kv_ref[...].reshape(out_ref.shape[1], kv_ref.shape[2])[:, :rank]
+    for head in range(out_ref.shape[0]):
+        weight = w_ref[:, head * (NOPE + DV) : (head + 1) * (NOPE + DV)]
+        out_ref[head] = jnp.dot(values, weight, preferred_element_type=jnp.float32).astype(
+            jnp.bfloat16
+        )
+
+
+def attend_kernel(
+    lift_ref, query_ref, pairs_ref, own_ref, other_ref, w_ref, out_ref, key_ref, value_ref, *, lat
+):
+    rank = w_ref.shape[0]
+    heads, count = pairs_ref.shape[:2]
+    for at, ref in ((0, own_ref), (count, other_ref)):
+        key_ref[at : at + count, NOPE:] = ref[:, :, rank:].reshape(count, 128)
+    position = lax.broadcasted_iota(jnp.int32, (1, 2 * count), 1)
+    context = lax.rem(position, lat[0] + lat[1]) >= lat[0]
+
+    @pl.loop(0, heads)
+    def _(head):
+        other = other_ref[...].reshape(count, other_ref.shape[2])[:, :rank]
+        width = NOPE + DV
+        weight = w_ref[:, pl.ds(pl.multiple_of(head * width, width), width)]
+        pairs = jnp.dot(other, weight, preferred_element_type=jnp.float32).astype(jnp.bfloat16)
+        key_ref[:count, :NOPE] = pairs_ref[head, :, :NOPE]
+        key_ref[count:, :NOPE] = pairs[:, :NOPE]
+        value_ref[:count] = pairs_ref[head, :, NOPE:]
+        value_ref[count:] = pairs[:, NOPE:]
+        score = dot_t(query_ref[head], key_ref[...])
+        lift = lift_ref[pl.ds(head, 1), :1]
+        score = score * (NOPE + ROPE) ** -0.5 + jnp.where(context, lift, 0.0)
+        peak = jnp.max(score, axis=1, keepdims=True)
+        probs = jnp.exp(score - peak)
+        total = jnp.sum(probs, axis=1, keepdims=True)
+        summed = jnp.dot(
+            probs.astype(jnp.bfloat16), value_ref[...], preferred_element_type=jnp.float32
+        )
+        out_ref[:, pl.ds(pl.multiple_of(head * DV, DV), DV)] = (summed / total).astype(jnp.bfloat16)
+
+
+def share_out_kernel(w_ref, out_ref):
+    chips, unused, features = out_ref.shape
+    side = place()[2]
+    for chip in range(chips):
+        start = pl.multiple_of((2 * chip + 1 - side) * features, features)
+        out_ref[chip] = w_ref[:, pl.ds(start, features)]
+
+
+def output_own_kernel(heads_ref, w_ref, out_ref):
+    chips, unused, features = out_ref.shape
+    side = place()[2]
+    for chip in range(chips):
+        start = pl.multiple_of((2 * chip + side) * features, features)
+        out_ref[chip] = jnp.dot(
+            heads_ref[...], w_ref[:, pl.ds(start, features)], preferred_element_type=jnp.float32
+        )
+
+
+def output_kernel(heads_ref, w_ref, acc_ref, out_ref):
+    for chip in range(out_ref.shape[0]):
+        acc = acc_ref[chip] + jnp.dot(
+            heads_ref[...], w_ref[chip], preferred_element_type=jnp.float32
+        )
+        out_ref[chip] = acc.astype(jnp.bfloat16)
+
+
+def mix_kernel(latent_ref, gate_ref, branch_ref, out_ref):
+    branch = branch_ref[0].astype(jnp.float32)
+    for chip in range(1, branch_ref.shape[0]):
+        branch = branch + branch_ref[chip].astype(jnp.float32)
+    out_ref[...] = (latent_ref[...].astype(jnp.float32) + gate_ref[...] * branch).astype(
+        jnp.bfloat16
+    )
+
+
+def split_device(
+    latent,
+    context,
+    cond,
+    cond_ctx,
+    w_mod,
+    g_norm,
+    w_dq,
+    w_dkv,
+    w_kr,
+    g_cq,
+    g_ckv,
+    w_uq,
+    w_ukv,
+    ctx_lift,
+    w_out,
+):
+    f32, bf16 = jnp.float32, jnp.bfloat16
+    sp, tp = lax.axis_size("sp"), lax.axis_size("tp")
+    chips = tp // 2
+    rows, features = latent.shape
+    ctx_rows = context.shape[0]
+    heads = w_uq.shape[1]
+    rank = w_dq.shape[1]
+    lat, ctx = rows // tp, ctx_rows // tp
+    half = rank // 2
+    sides = [list(range(k, tp, 2)) for k in range(2)]
+    across = [(i, i ^ 1) for i in range(tp)]
+    me = lax.axis_index("tp")
+
+    def array(shape, dtype=bf16):
+        return jax.ShapeDtypeStruct(shape, dtype)
+
+    size = max(5 * features, rows + ctx_rows)
+    stat, tokens = call(
+        functools.partial(stats_kernel, sp=sp, tp=tp),
+        (array((sp * tp, 1, size), f32), array((rows + ctx_rows, features))),
+        latent,
+        context,
+        cond[None],
+        cond_ctx[None],
+        jnp.transpose(w_mod, (1, 0, 2)),
+        g_norm[None],
+        name="stats",
+        held=False,
+    )
+    stat = lax.all_to_all(stat, ("sp", "tp"), 0, 0)
+
+    share = array((features + ROPE // 2 * features // rank, rank))
+    w_own, w_other = call(share_kernel, (share, share), w_dq, w_dkv, w_kr.T, name="share", held=False)
+    tokens_other = lax.ppermute(tokens, "tp", across)
+    w_other = lax.ppermute(w_other, "tp", across)
+    w_up = w_out.reshape(heads * DV, 2 * chips * features)
+    w_up_share = call(
+        share_out_kernel, array((chips, heads * DV, features)), w_up, flops=1e9, name="share_out"
+    )
+    stat, w_up_share = lax.optimization_barrier((stat, w_up_share))
+    w_up_other = lax.ppermute(w_up_share, "tp", across)
+
+    height = half // 128 * (2 * lat + ctx) + (lat + ctx) // 4
+    part, gate = call(
+        functools.partial(project_kernel, sp=sp, tp=tp, rows=rows),
+        (array((tp, height, 128), f32), array((1, features), f32)),
+        tokens,
+        tokens_other,
+        stat,
+        w_own,
+        w_other,
+        flops=4 * (rows + ctx_rows) * features * (rank + 128),
+        limit=16,
+        name="project",
+    )
+    part, w_kv, zero = lax.optimization_barrier((part, w_ukv, jnp.int32(0)))
+    part = lax.all_to_all(part, "tp", 0, 0)
+
+    positions = zero + lax.axis_index("sp") * rows + jnp.arange(rows, dtype=jnp.int32)
+    cosine, sine = tables(positions)
+    quarter = ROPE // 4
+    c0, c1, s0, s1 = cosine[:, :quarter], cosine[:, quarter:], sine[:, :quarter], sine[:, quarter:]
+    q_tab = jnp.concatenate([c0, c0, c1, c1, -s0, s0, -s1, s1], axis=1)
+    k_tab = lax.dynamic_slice_in_dim(q_tab, me * lat, lat, 0)
+    k_tab = k_tab.reshape(lat, 2, 2, ROPE // 2).transpose(1, 2, 0, 3)
+    w_kv = w_kv.reshape(rank, heads * (NOPE + DV))
+    part, q_tab, w_up_other, w_kv = lax.optimization_barrier((part, q_tab, w_up_other, w_kv))
+
+    kv, cq = call(
+        functools.partial(norm_kernel, lat=lat, ctx=ctx),
+        (array((sp, lat + ctx, rank + 128)), array((lat, rank))),
+        part,
+        g_cq[None],
+        g_ckv[None],
+        k_tab,
+        name="norm",
+    )
+
+    kv = lax.all_to_all(kv, "sp", 0, 0).reshape(1, sp * (lat + ctx), rank + 128)
+    near = [cq]
+    for hop in range(1, chips):
+        swap = [(i, i ^ (2 * hop)) for i in range(tp)]
+        near.append(lax.ppermute(cq, "tp", swap))
+    cq_own, kv = lax.optimization_barrier((jnp.stack(near), kv))
+    cq_other = lax.ppermute(cq_own, "tp", across)
+    kv = jnp.broadcast_to(kv, (chips,) + kv.shape[1:])
+    kv_own = lax.all_to_all(kv, "tp", 0, 0, axis_index_groups=sides)
+    kv_other = lax.ppermute(kv_own, "tp", across)
+
+    keys = sp * (rows + ctx_rows)
+    query = call(
+        query_kernel,
+        array((heads, rows, 2 * NOPE)),
+        cq_own,
+        cq_other,
+        q_tab,
+        jnp.transpose(w_uq, (1, 2, 0)),
+        scratch=[pltpu.VMEM((rows, rank), bf16)],
+        flops=2 * rows * rank * 256 * heads,
+        name="query",
+    )
+    pairs = call(
+        expand_kernel,
+        array((heads, keys // 2, NOPE + DV)),
+        kv_own,
+        w_kv,
+        flops=keys * rank * 256 * heads,
+        name="expand",
+    )
+    heads_out = call(
+        functools.partial(attend_kernel, lat=(lat, ctx)),
+        array((rows, heads * DV)),
+        jnp.broadcast_to(ctx_lift[:, None], (heads, 128)),
+        query,
+        pairs,
+        kv_own,
+        kv_other,
+        w_kv,
+        scratch=[pltpu.VMEM((keys, 2 * NOPE), bf16), pltpu.VMEM((keys, DV), bf16)],
+        flops=heads * keys * (2 * rows * 384 + rank * 256),
+        limit=24,
+        name="attend",
+    )
+
+    heads_other = lax.ppermute(heads_out, "tp", across)
+    flops = 2 * rows * heads * DV * chips * features
+    branch = call(
+        output_own_kernel,
+        array((chips, rows, features), f32),
+        heads_out,
+        w_up,
+        flops=flops,
+        name="output_own",
+    )
+    branch = call(
+        output_kernel,
+        array((chips, rows, features)),
+        heads_other,
+        w_up_other,
+        branch,
+        flops=flops,
+        name="output",
+    )
+    branch = lax.all_to_all(branch, "tp", 0, 0, axis_index_groups=sides)
+    return call(mix_kernel, array(latent.shape), latent, gate, branch, name="mix", kept=False)
+
+
+def per_device(*arrays):
+    rows, ctx_rows, features = arrays[0].shape[0], arrays[1].shape[0], arrays[0].shape[1]
+    tp = lax.axis_size("tp")
+    aligned = rows % (16 * tp) == 0 and ctx_rows % (16 * tp) == 0 and features % 128 == 0 and arrays[6].shape[1] % features == 0
+    return (split_device if tp in (2, 4, 8, 16) and aligned else plain_device)(*arrays)
+
+
 def solution(mesh):
     return jax.shard_map(
         per_device,

time: 288 us -> 109 us (0.38)
  waiting for transfers between devices: 94.6 us -> 19.6 us
  blocking collectives: 91 us -> 34.8 us
  matrix products: 40.1 us -> 0 us
  starting transfers between devices: 0.12 us -> 19.6 us
  Pallas kernels: 0 us -> 19.3 us
  local copies, waits for them, and re-layouts: 32.7 us -> 14.6 us
  other arithmetic: 14.7 us -> 0.24 us
  between operations: 13.3 us -> 0.23 us
    psum x3 -> x0, blocking collectives: 48.3 us -> none  [the longest x1 22.7 us: per_device(): lax.psum((jnp.dot(lat_h, w_dq, preferred_element_type=jnp.float32), jnp.d...]
    psum x1 -> x0, waiting for transfers between devices: 44.7 us -> none  [per_device(): lax.psum((jnp.dot(lat_h, w_dq, preferred_element_type=jnp.float32), jnp.d...]
    all_gather x3 -> x0, blocking collectives: 42.7 us -> none  [the longest x1 16 us: per_device(): spinning_section = lax.all_gather(lat_kr, 'sp', axis=0, tiled=True)]
    dot_general x23 -> x0, matrix products: 40.1 us -> none  [the longest x5 14.2 us: expand(): jnp.dot(compressed, up_weight, preferred_element_type=jnp.float32)]
    reduce_scatter x1 -> x0, waiting for transfers between devices: 37.2 us -> none  [per_device(): lax.psum_scatter(branch.astype(jnp.bfloat16), 'tp', scatter_dimension=1,...]
    all_to_all x0 -> x2, blocking collectives: none -> 34.8 us  [the longest x1 20.3 us: split_device(): kv_own = lax.all_to_all(kv, 'tp', 0, 0, axis_index_groups=sides)]
    pallas_call x0 -> x11, Pallas kernels: none -> 19.3 us  [call(): pl.pallas_call(kernel, in_specs=[vmem] * len(args), out_specs=(vmem,) * l...]
    all_to_all x0 -> x3, starting transfers between devices: none -> 14.3 us  [the longest x1 7.33 us: split_device(): stat = lax.all_to_all(stat, ('sp', 'tp'), 0, 0)]
  transfers between devices with their start and end apart: 3 -> 12, of which waited for: 3 -> 8; matrix products, arithmetic and copies ran while one was open for 5% -> 4% of each run, Pallas kernels for 0% -> 3%
where the time goes in v2:
time: 109 us; the launch traced here: 108 us
  blocking collectives  34.8 us (32%)
  starting transfers between devices  19.6 us (18%)
  waiting for transfers between devices  19.6 us (18%)
  Pallas kernels  19.3 us (18%)
  local copies, waits for them, and re-layouts  14.6 us (13%)
    all_to_all x1, blocking collectives, split_device(): kv_own = lax.all_to_all(kv, 'tp', 0, 0, axis_index_groups=sides)  20.3 us
    pallas_call x11, Pallas kernels, call(): pl.pallas_call(kernel, in_specs=[vmem] * len(args), out_specs=(vmem,) * l...  19.3 us
    all_to_all x1, blocking collectives, split_device(): branch = lax.all_to_all(branch, 'tp', 0, 0, axis_index_groups=sides)  14.5 us
    unnamed x31, local copies, waits for them, and re-layouts  10 us
    all_to_all x1, waiting for transfers between devices, split_device(): part = lax.all_to_all(part, 'tp', 0, 0)  9.43 us
    all_to_all x1, starting transfers between devices, split_device(): stat = lax.all_to_all(stat, ('sp', 'tp'), 0, 0)  7.33 us
    all_to_all x1, starting transfers between devices, split_device(): part = lax.all_to_all(part, 'tp', 0, 0)  3.57 us
    ppermute x3, starting transfers between devices, split_device(): near.append(lax.ppermute(cq, 'tp', swap))  3.55 us
  transfers between devices with their start and end apart: 12, of which 8 were waited for; matrix products, arithmetic and copies ran while one was open for 4% of the time, Pallas kernels for 3%

profile of v2, /device:TPU:0, one launch (start us, length us, event | category | flops | bytes accessed | tf_op | source)
XLA Modules:
  0.0 108.3 jit_solution(2533177474160781198)
XLA Ops:
  0.0 0.7 broadcast_in_dim.32.cond_ref
  0.7 0.7 broadcast_in_dim.33.cond_ctx_ref
  1.4 1.1 %copy-done.2 = bf16[512,3,256]{2,0,1:T(8,128)(2,1)S(1)} copy-done((bf16[512,3,256]{2,0,1:T(8,128)(2,1)S(1)}, bf16[512,3,256]{2,0,1:T(8,128)(2,1)}, u32[]{:S(2)}) %copy-start.2) | copy-done | bytes 786456
  2.5 0.9 copy-done.4
  3.4 0.8 copy-done.9
  4.3 0.7 copy-done.13
  4.9 1.3 %stats.1 = (f32[32,1,1280]{2,1,0:T(1,128)}, bf16[512,256]{1,0:T(8,128)(2,1)S(1)}) custom-call(bf16[384,256]{1,0:T(8,128)(2,1)S(1)} %copy-done.4, bf16[128,256]{1,0:T(8,128)(2,1)S(1)} %copy-done.9, bf16[1,512]{1,0:T(2,128)(2,1)S(1)} %broadcast_in_dim.32.cond_ref, bf16[1,512]{1,0:T(2,128)(2,1)S(1)} %broadcast_in_dim.33.cond_ctx_ref, ...), custom_call_target="tpu_custom_call" | custom-call | flops 1000000 | bytes 100000 | tf_op jit(solution)/shard_map/stats/pallas_call | solution.py:203
  6.3 7.3 %all-to-all-start = ((f32[32,1,1280]{2,1,0:T(1,128)}), f32[32,1,1280]{2,1,0:T(1,128)S(1)}, u32[]{:S(2)}, u32[]{:S(2)}) async-start(f32[32,1,1280]{2,1,0:T(1,128)} %get-tuple-element.25), calls=%async_computation | async-start | bytes 327680 | tf_op jit(solution)/shard_map/all_to_all | solution.py:541
  13.6 0.0 copy-start.7
  13.6 0.9 copy-done.7
  14.6 0.9 copy-done.8
  15.5 0.8 copy-done.10
  16.3 0.3 collective-permute-start.1
  16.6 0.3 collective-permute-start
  16.9 1.6 %copy-done = bf16[4,128,2048]{2,1,0:T(8,128)(2,1)S(1)} copy-done((bf16[4,128,2048]{2,1,0:T(8,128)(2,1)S(1)}, bf16[4,128,2048]{2,1,0:T(8,128)(2,1)}, u32[]{:S(2)}) %copy-start) | copy-done | bytes 2097176
  18.5 1.1 %share_out.1 = bf16[4,512,256]{2,1,0:T(8,128)(2,1)} custom-call(bf16[512,2048]{1,0:T(8,128)(2,1)S(1)} %bitcast.19), custom_call_target="tpu_custom_call" | custom-call | flops 1000000000 | bytes 100000 | tf_op jit(solution)/shard_map/share_out/pallas_call | solution.py:203
  19.6 2.6 %all-to-all-done.stat_ref = f32[32,1,1280]{2,1,0:T(1,128)S(1)} async-done(((f32[32,1,1280]{2,1,0:T(1,128)}), f32[32,1,1280]{2,1,0:T(1,128)S(1)}, u32[]{:S(2)}, u32[]{:S(2)}) %all-to-all-start) | async-done | bytes 163872 | tf_op jit(solution)/shard_map/all_to_all | solution.py:541
  22.2 0.0 collective-permute-done.other_ref
  22.2 0.0 collective-permute-done.1.w_other_ref
  22.2 1.9 %project.1 = (f32[8,240,128]{2,1,0:T(8,128)}, f32[1,256]{1,0:T(1,128)S(1)}) custom-call(bf16[512,256]{1,0:T(8,128)(2,1)S(1)} %get-tuple-element.24.own_ref, bf16[512,256]{1,0:T(8,128)(2,1)S(1)} %collective-permute-done.other_ref, f32[32,1,1280]{2,1,0:T(1,128)S(1)} %all-to-all-done.stat_ref, bf16[272,512]{1,0:T(8,128)(2,1)S(1)} %get-tuple-element.27.w_own_ref, ...), custom_call_target="tpu_custom_call" | custom-call | flops 335544320 | bytes 100000 | tf_op jit(solution)/shard_map/project/pallas_call | solution.py:203
  24.2 3.6 %all-to-all-start.1 = ((f32[8,240,128]{2,1,0:T(8,128)}), f32[8,240,128]{2,1,0:T(8,128)S(1)}, u32[]{:S(2)}, u32[]{:S(2)}) async-start(f32[8,240,128]{2,1,0:T(8,128)} %get-tuple-element.31), calls=%async_computation.1 | async-start | bytes 1966080 | tf_op jit(solution)/shard_map/all_to_all | solution.py:568
  27.7 0.4 collective-permute-start.2
  28.1 0.1 broadcast_multiply_fusion.1
  28.2 0.1 copy.18
  28.4 0.7 fusion.6
  29.0 0.7 fusion.7
  29.8 0.1 fusion.5
  29.9 1.3 %concatenate.8.tab_ref = f32[384,128]{1,0:T(8,128)S(1)} concatenate(f32[384,16]{1,0:T(8,128)} %get-tuple-element.50, f32[384,32]{1,0:T(8,128)S(1)} %get-tuple-element.48, f32[384,16]{1,0:T(8,128)S(1)} %get-tuple-element.49, f32[384,16]{1,0:T(8,128)S(1)} %get-tuple-element.44, f32[384,16]{1,0:T(8,128)S(1)} %get-tuple-element.46, f32[384,16]{1,0:T(8,128)S(1)} %get-tuple-element.45, ...), dimensions={1} | concatenate | bytes 393216 | tf_op jit(solution)/shard_map/concatenate | solution.py:574
  31.2 0.0 copy-start.11
  31.2 0.0 copy-start.12
  31.3 0.1 copy.20
  31.4 0.1 copy.21
  31.5 1.4 %copy.22 = bf16[64,8,4,256]{3,1,2,0:T(8,128)(2,1)S(1)} copy(bf16[64,8,4,256]{3,2,1,0:T(4,128)(2,1)} %bitcast.30) | data formatting | bytes 2097152
  32.9 9.4 %all-to-all-done.1.part_ref = f32[8,240,128]{2,1,0:T(8,128)S(1)} async-done(((f32[8,240,128]{2,1,0:T(8,128)}), f32[8,240,128]{2,1,0:T(8,128)S(1)}, u32[]{:S(2)}, u32[]{:S(2)}) %all-to-all-start.1) | async-done | bytes 983072 | tf_op jit(solution)/shard_map/all_to_all | solution.py:568
  42.3 0.0 collective-permute-done.2.w_ref
  42.4 0.2 norm.1
  42.6 0.7 copy-done.6
  43.3 3.5 %all-to-all-start.2 = ((bf16[4,64,640]{2,1,0:T(8,128)(2,1)}), bf16[4,64,640]{2,1,0:T(8,128)(2,1)S(1)}, u32[]{:S(2)}, u32[]{:S(2)}) async-start(bf16[4,64,640]{2,1,0:T(8,128)(2,1)} %copy-done.6), calls=%async_computation.2 | async-start | bytes 655360 | tf_op jit(solution)/shard_map/all_to_all | solution.py:590
  46.8 0.7 collective-permute-start.5
  47.4 1.4 %collective-permute-start.4 = (bf16[48,512]{1,0:T(8,128)(2,1)S(1)}, bf16[48,512]{1,0:T(8,128)(2,1)S(1)}, u32[]{:S(2)}, u32[]{:S(2)}) collective-permute-start(bf16[48,512]{1,0:T(8,128)(2,1)S(1)} %get-tuple-element.36), channel_id=1, source_target_pairs={{0,4},{1,5},{2,6},{3,7},{4,0},{5,1},{6,2},{7,3},{8,12},{9,13},{10,... | collective-permute-start | bytes 147464 | tf_op jit(solution)/shard_map/ppermute | solution.py:594
  48.8 1.5 %collective-permute-start.3 = (bf16[48,512]{1,0:T(8,128)(2,1)S(1)}, bf16[48,512]{1,0:T(8,128)(2,1)S(1)}, u32[]{:S(2)}, u32[]{:S(2)}) collective-permute-start(bf16[48,512]{1,0:T(8,128)(2,1)S(1)} %get-tuple-element.36), channel_id=1, source_target_pairs={{0,2},{1,3},{2,0},{3,1},{4,6},{5,7},{6,4},{7,5},{8,10},{9,11},{10,... | collective-permute-start | bytes 147464 | tf_op jit(solution)/shard_map/ppermute | solution.py:594
  50.3 1.6 %collective-permute-done.5 = bf16[48,512]{1,0:T(8,128)(2,1)S(1)} collective-permute-done((bf16[48,512]{1,0:T(8,128)(2,1)S(1)}, bf16[48,512]{1,0:T(8,128)(2,1)S(1)}, u32[]{:S(2)}, u32[]{:S(2)}) %collective-permute-start.5) | collective-permute-done | bytes 49184 | tf_op jit(solution)/shard_map/ppermute | solution.py:594
  51.9 0.1 collective-permute-done.4
  52.0 0.8 collective-permute-done.3
  52.9 1.1 %all-to-all-done.2 = bf16[4,64,640]{2,1,0:T(8,128)(2,1)S(1)} async-done(((bf16[4,64,640]{2,1,0:T(8,128)(2,1)}), bf16[4,64,640]{2,1,0:T(8,128)(2,1)S(1)}, u32[]{:S(2)}, u32[]{:S(2)}) %all-to-all-start.2) | async-done | bytes 327712 | tf_op jit(solution)/shard_map/all_to_all | solution.py:590
  54.0 0.1 broadcast_in_dim.39
  54.1 0.0 copy-start.3
  54.2 20.3 %all_to_all.25.kv_ref.own_ref = bf16[4,256,640]{2,1,0:T(8,128)(2,1)S(1)} all-to-all(bf16[4,256,640]{2,1,0:T(8,128)(2,1)S(1)} %broadcast_in_dim.39), channel_id=1, replica_groups={{0,2,4,6},{1,3,5,7},{8,10,12,14},{9,11,13,15},{16,18,20,22},{17,19,21,2..., dimensions={0} | all-to-all | bytes 2621440 | tf_op jit(solution)/shard_map/all_to_all | solution.py:598
  74.5 0.0 collective-permute-start.7
  74.5 0.5 collective-permute-start.6
  75.0 2.8 %collective-permute-done.6.other_ref = bf16[4,48,512]{2,1,0:T(8,128)(2,1)S(1)} collective-permute-done((bf16[4,48,512]{2,1,0:T(8,128)(2,1)S(1)}, bf16[4,48,512]{2,1,0:T(8,128)(2,1)S(1)}, u32[]{:S(2)}, u32[]{:S(2)}) %collective-permute-start.6) | collective-permute-done | bytes 196640 | tf_op jit(solution)/shard_map/ppermute | solution.py:596
  77.8 0.7 query.1.query_ref
  78.5 0.0 copy-start.14
  78.5 1.3 %expand.1.pairs_ref = bf16[4,1024,256]{2,1,0:T(8,128)(2,1)S(1)} custom-call(bf16[4,256,640]{2,1,0:T(8,128)(2,1)S(1)} %all_to_all.25.kv_ref.own_ref, bf16[512,1024]{1,0:T(8,128)(2,1)S(1)} %bitcast.17), custom_call_target="tpu_custom_call" | custom-call | flops 1073741824 | bytes 100000 | tf_op jit(solution)/shard_map/expand/pallas_call | solution.py:203
  79.7 0.0 collective-permute-done.7.other_ref
  79.8 0.1 broadcast_in_dim.35.lift_ref
  79.8 10.8 %attend.1.heads_ref = bf16[384,512]{1,0:T(8,128)(2,1)S(1)} custom-call(f32[4,128]{1,0:T(4,128)S(1)} %broadcast_in_dim.35.lift_ref, bf16[4,384,256]{2,1,0:T(8,128)(2,1)S(1)} %query.1.query_ref, bf16[4,1024,256]{2,1,0:T(8,128)(2,1)S(1)} %expand.1.pairs_ref, bf16[4,256,640]{2,1,0:T(8,128)(2,1)S(1)} %all_to_all.25.kv_ref.own_ref, ...), custom_call_target="tpu_custom_call" | custom-call | flops 3489660928 | bytes 100000 | tf_op jit(solution)/shard_map/attend/pallas_call | solution.py:203
  90.6 0.2 collective-permute-start.8
  90.8 0.6 output_own.1.acc_ref
  91.4 1.0 collective-permute-done.8.heads_ref
  92.4 0.6 output.1
  93.0 0.0 copy-start.5
  93.0 14.5 %all_to_all.26.branch_ref = bf16[4,384,256]{2,1,0:T(8,128)(2,1)S(1)} all-to-all(bf16[4,384,256]{2,1,0:T(8,128)(2,1)S(1)} %output.1), channel_id=1, replica_groups={{0,2,4,6},{1,3,5,7},{8,10,12,14},{9,11,13,15},{16,18,20,22},{17,19,21,2..., dimensions={0} | all-to-all | bytes 1572864 | tf_op jit(solution)/shard_map/all_to_all | solution.py:655
  107.4 0.8 mix.1
  (21 shorter events, 0.1 us)
Async XLA Ops:
  1.4 1.1 %copy-start.2 = (bf16[512,3,256]{2,0,1:T(8,128)(2,1)S(1)}, bf16[512,3,256]{2,0,1:T(8,128)(2,1)}, u32[]{:S(2)}) copy-start(bf16[512,3,256]{2,0,1:T(8,128)(2,1)} %param.19) | copy-start | bytes 2359300
  2.5 0.9 copy-start.4
  3.4 0.8 copy-start.9
  4.3 0.7 copy-start.13
  6.3 16.0 %all-to-all-start = ((f32[32,1,1280]{2,1,0:T(1,128)}), f32[32,1,1280]{2,1,0:T(1,128)S(1)}, u32[]{:S(2)}, u32[]{:S(2)}) async-start(f32[32,1,1280]{2,1,0:T(1,128)} %get-tuple-element.25), calls=%async_computation | async-start | bytes 327680 | tf_op jit(solution)/shard_map/all_to_all | solution.py:541
  13.6 1.0 copy-start.7
  14.6 0.9 copy-start.8
  15.5 0.8 copy-start.10
  16.3 5.9 %collective-permute-start.1 = (bf16[272,512]{1,0:T(8,128)(2,1)S(1)}, bf16[272,512]{1,0:T(8,128)(2,1)S(1)}, u32[]{:S(2)}, u32[]{:S(2)}) collective-permute-start(bf16[272,512]{1,0:T(8,128)(2,1)S(1)} %get-tuple-element.28), channel_id=1, source_target_pairs={{0,1},{1,0},{2,3},{3,2},{4,5},{5,4},{6,7},{7,6},{8,9},{9,8},{10,11... | collective-permute-start | bytes 835592 | tf_op jit(solution)/shard_map/ppermute | solution.py:546
  16.6 5.6 %collective-permute-start = (bf16[512,256]{1,0:T(8,128)(2,1)S(1)}, bf16[512,256]{1,0:T(8,128)(2,1)S(1)}, u32[]{:S(2)}, u32[]{:S(2)}) collective-permute-start(bf16[512,256]{1,0:T(8,128)(2,1)S(1)} %get-tuple-element.24.own_ref), channel_id=1, source_target_pairs={{0,1},{1,0},{2,3},{3,2},{4,5},{5,4},{6,7},{7,6},{8,9},{9,8},{10,11... | collective-permute-start | bytes 786440 | tf_op jit(solution)/shard_map/ppermute | solution.py:545
  16.9 1.6 %copy-start = (bf16[4,128,2048]{2,1,0:T(8,128)(2,1)S(1)}, bf16[4,128,2048]{2,1,0:T(8,128)(2,1)}, u32[]{:S(2)}) copy-start(bf16[4,128,2048]{2,1,0:T(8,128)(2,1)} %param.29) | copy-start | bytes 6291460
  24.2 18.2 %all-to-all-start.1 = ((f32[8,240,128]{2,1,0:T(8,128)}), f32[8,240,128]{2,1,0:T(8,128)S(1)}, u32[]{:S(2)}, u32[]{:S(2)}) async-start(f32[8,240,128]{2,1,0:T(8,128)} %get-tuple-element.31), calls=%async_computation.1 | async-start | bytes 1966080 | tf_op jit(solution)/shard_map/all_to_all | solution.py:568
  27.7 14.6 %collective-permute-start.2 = (bf16[4,512,256]{2,1,0:T(8,128)(2,1)}, bf16[4,512,256]{2,1,0:T(8,128)(2,1)S(1)}, u32[]{:S(2)}, u32[]{:S(2)}) collective-permute-start(bf16[4,512,256]{2,1,0:T(8,128)(2,1)} %share_out.1), channel_id=1, source_target_pairs={{0,1},{1,0},{2,3},{3,2},{4,5},{5,4},{6,7},{7,6},{8,9},{9,8},{10,11... | collective-permute-start | bytes 3145736 | tf_op jit(solution)/shard_map/ppermute | solution.py:552
  31.2 11.1 %copy-start.11 = (f32[512]{0:T(512)S(1)}, f32[512]{0:T(512)}, u32[]{:S(2)}) copy-start(f32[512]{0:T(512)} %param.24) | copy-start | bytes 6148
  31.2 11.1 %copy-start.12 = (f32[512]{0:T(512)S(1)}, f32[512]{0:T(512)}, u32[]{:S(2)}) copy-start(f32[512]{0:T(512)} %param.25) | copy-start | bytes 6148
  42.6 0.7 copy-start.6
  43.3 10.7 %all-to-all-start.2 = ((bf16[4,64,640]{2,1,0:T(8,128)(2,1)}), bf16[4,64,640]{2,1,0:T(8,128)(2,1)S(1)}, u32[]{:S(2)}, u32[]{:S(2)}) async-start(bf16[4,64,640]{2,1,0:T(8,128)(2,1)} %copy-done.6), calls=%async_computation.2 | async-start | bytes 655360 | tf_op jit(solution)/shard_map/all_to_all | solution.py:590
  46.8 5.2 %collective-permute-start.5 = (bf16[48,512]{1,0:T(8,128)(2,1)S(1)}, bf16[48,512]{1,0:T(8,128)(2,1)S(1)}, u32[]{:S(2)}, u32[]{:S(2)}) collective-permute-start(bf16[48,512]{1,0:T(8,128)(2,1)S(1)} %get-tuple-element.36), channel_id=1, source_target_pairs={{0,6},{1,7},{2,4},{3,5},{4,2},{5,3},{6,0},{7,1},{8,14},{9,15},{10,... | collective-permute-start | bytes 147464 | tf_op jit(solution)/shard_map/ppermute | solution.py:594
  47.4 4.6 %collective-permute-start.4 = (bf16[48,512]{1,0:T(8,128)(2,1)S(1)}, bf16[48,512]{1,0:T(8,128)(2,1)S(1)}, u32[]{:S(2)}, u32[]{:S(2)}) collective-permute-start(bf16[48,512]{1,0:T(8,128)(2,1)S(1)} %get-tuple-element.36), channel_id=1, source_target_pairs={{0,4},{1,5},{2,6},{3,7},{4,0},{5,1},{6,2},{7,3},{8,12},{9,13},{10,... | collective-permute-start | bytes 147464 | tf_op jit(solution)/shard_map/ppermute | solution.py:594
  48.8 4.1 %collective-permute-start.3 = (bf16[48,512]{1,0:T(8,128)(2,1)S(1)}, bf16[48,512]{1,0:T(8,128)(2,1)S(1)}, u32[]{:S(2)}, u32[]{:S(2)}) collective-permute-start(bf16[48,512]{1,0:T(8,128)(2,1)S(1)} %get-tuple-element.36), channel_id=1, source_target_pairs={{0,2},{1,3},{2,0},{3,1},{4,6},{5,7},{6,4},{7,5},{8,10},{9,11},{10,... | collective-permute-start | bytes 147464 | tf_op jit(solution)/shard_map/ppermute | solution.py:594
  54.1 23.6 %copy-start.3 = (bf16[512,4,192]{0,2,1:T(8,128)(2,1)S(1)}, bf16[512,4,192]{0,2,1:T(8,128)(2,1)}, u32[]{:S(2)}) copy-start(bf16[512,4,192]{0,2,1:T(8,128)(2,1)} %param.26) | copy-start | bytes 2359300
  74.5 5.3 %collective-permute-start.7 = (bf16[4,256,640]{2,1,0:T(8,128)(2,1)S(1)}, bf16[4,256,640]{2,1,0:T(8,128)(2,1)S(1)}, u32[]{:S(2)}, u32[]{:S(2)}) collective-permute-start(bf16[4,256,640]{2,1,0:T(8,128)(2,1)S(1)} %all_to_all.25.kv_ref.own_ref), channel_id=1, source_target_pairs={{0,1},{1,0},{2,3},{3,2},{4,5},{5,4},{6,7},{7,6},{8,9},{9,8},{10,11... | collective-permute-start | bytes 3932168 | tf_op jit(solution)/shard_map/ppermute | solution.py:599
  74.5 3.3 %collective-permute-start.6 = (bf16[4,48,512]{2,1,0:T(8,128)(2,1)S(1)}, bf16[4,48,512]{2,1,0:T(8,128)(2,1)S(1)}, u32[]{:S(2)}, u32[]{:S(2)}) collective-permute-start(bf16[4,48,512]{2,1,0:T(8,128)(2,1)S(1)} %pad_maximum_fusion.own_ref), channel_id=1, source_target_pairs={{0,1},{1,0},{2,3},{3,2},{4,5},{5,4},{6,7},{7,6},{8,9},{9,8},{10,11... | collective-permute-start | bytes 589832 | tf_op jit(solution)/shard_map/ppermute | solution.py:596
  78.5 1.3 %copy-start.14 = (f32[4]{0:T(128)S(1)}, f32[4]{0:T(128)}, u32[]{:S(2)}) copy-start(f32[4]{0:T(128)} %param.28) | copy-start | bytes 52
  79.8 11.0 %copy-start.1 = (bf16[4,128,2048]{2,1,0:T(8,128)(2,1)S(1)}, bf16[4,128,2048]{2,1,0:T(8,128)(2,1)}, u32[]{:S(2)}) copy-start(bf16[4,128,2048]{2,1,0:T(8,128)(2,1)} %param.29) | copy-start | bytes 6291460
  90.6 1.8 %collective-permute-start.8 = (bf16[384,512]{1,0:T(8,128)(2,1)S(1)}, bf16[384,512]{1,0:T(8,128)(2,1)S(1)}, u32[]{:S(2)}, u32[]{:S(2)}) collective-permute-start(bf16[384,512]{1,0:T(8,128)(2,1)S(1)} %attend.1.heads_ref), channel_id=1, source_target_pairs={{0,1},{1,0},{2,3},{3,2},{4,5},{5,4},{6,7},{7,6},{8,9},{9,8},{10,11... | collective-permute-start | bytes 1179656 | tf_op jit(solution)/shard_map/ppermute | solution.py:636
  93.0 14.5 %copy-start.5 = (bf16[384,256]{1,0:T(8,128)(2,1)S(1)}, bf16[384,256]{1,0:T(8,128)(2,1)}, u32[]{:S(2)}) copy-start(bf16[384,256]{1,0:T(8,128)(2,1)} %latent_ref.1) | copy-start | bytes 589828

commit v3 on v2

--- a/solution.py
+++ b/solution.py
@@ -16,6 +16,7 @@
 
 EPS = 1e-06
 THETA = 10000.0
+LOG2E = 1.4426950408889634
 
 
 def tables(positions):
@@ -181,9 +182,9 @@
             None,
         )
 
-    fold_cumulative_loop_values, unused = lax.scan(step, fold_cumulative_loop_values, blocks)
+    fold_cumulative_loop_values, _ = lax.scan(step, fold_cumulative_loop_values, blocks)
     cumulative_loop_values = fold_cumulative_loop_values
-    peak, total, accum = cumulative_loop_values
+    _, total, accum = cumulative_loop_values
     heads_out = (accum / total[..., None]).astype(jnp.bfloat16)
     branch = jnp.einsum("hqd,hde->qe", heads_out, w_out, preferred_element_type=jnp.float32)
     branch = lax.psum_scatter(
@@ -192,14 +193,14 @@
     return (lat_f + modulation[0, 2] * branch).astype(jnp.bfloat16)
 
 
-def call(kernel, outs, *args, flops=1e6, scratch=(), limit=8, name=None, held=True, kept=True):
+def call(kernel, outs, *args, flops=1e6, scratch=(), limit=8, held=pltpu.VMEM, kept=True):
     single = not isinstance(outs, tuple)
     vmem = pl.BlockSpec(memory_space=pltpu.VMEM)
     outs = (outs,) if single else outs
     if kept:
         outs = tuple(pltpu.VMEM(o.shape, o.dtype) for o in outs)
-    if held:
-        args = tuple(pltpu.with_memory_space_constraint(a, pltpu.VMEM) for a in args)
+    if held is not None:
+        args = tuple(pltpu.with_memory_space_constraint(a, held) for a in args)
     result = pl.pallas_call(
         kernel,
         in_specs=[vmem] * len(args),
@@ -210,7 +211,6 @@
             flops=int(flops), bytes_accessed=int(1e5), transcendentals=0
         ),
         compiler_params=pltpu.CompilerParams(vmem_limit_bytes=limit << 20),
-        name=name,
     )(*args)
     return result[0] if single else result
 
@@ -241,59 +241,52 @@
             ref[features:, i * features : (i + 1) * features] = rot[i * count : (i + 1) * count]
 
 
-def stats_kernel(lat_ref, ctx_ref, cond_ref, cond_ctx_ref, w_ref, g_ref, out_ref, rows_ref, *, sp, tp):
-    chip = place()[1]
-    features = lat_ref.shape[1]
-    size = out_ref.shape[2]
+def stats_kernel(lat_ref, ctx_ref, cond_ref, cond_ctx_ref, w_ref, g_ref, out_ref, rows_ref, *, sp):
     rows_ref[: lat_ref.shape[0]] = lat_ref[...]
     rows_ref[lat_ref.shape[0] :] = ctx_ref[...]
-    ones = jnp.ones((8, features), jnp.float32)
-    sums = []
-    for ref in (lat_ref, ctx_ref):
-        values = ref[...].astype(jnp.float32)
-        sums.append(dot_t(ones, values * values, precision=lax.Precision.HIGHEST)[:1])
-    sums.append(jnp.zeros((1, size - lat_ref.shape[0] - ctx_ref.shape[0]), jnp.float32))
-    sums = jnp.concatenate(sums, axis=1)
-    lat_c = jax.nn.silu(cond_ref[...].astype(jnp.float32))
-    ctx_c = jax.nn.silu(cond_ctx_ref[...].astype(jnp.float32))
-    row = lax.broadcasted_iota(jnp.int32, (16, lat_c.shape[1]), 0)
+    inner = cond_ref.shape[0]
+    lat_c = jax.nn.silu(cond_ref[...].astype(jnp.float32).reshape(1, inner))
+    ctx_c = jax.nn.silu(cond_ctx_ref[...].astype(jnp.float32).reshape(1, inner))
+    row = lax.broadcasted_iota(jnp.int32, (16, inner), 0)
     signal = jnp.where(row < 8, lat_c, ctx_c).astype(jnp.bfloat16)
     parts = [jnp.dot(signal, w_ref[j], preferred_element_type=jnp.float32) for j in range(3)]
-    gain = g_ref[...]
+    gain = g_ref[...].reshape(1, g_ref.shape[0])
     gains = parts[1] * gain + gain * (1.0 / sp)
     modulation = jnp.concatenate(
-        [
-            parts[0][:1],
-            gains[:1],
-            parts[0][8:9],
-            gains[8:9],
-            parts[2][:1],
-            jnp.zeros((1, size - 5 * features), jnp.float32),
-        ][: 5 if size == 5 * features else 6],
-        axis=1,
-    )
-    for d in range(sp * tp):
-        out_ref[d] = jnp.where((d % tp) // 2 == chip, modulation, sums)
+        [parts[0][:1], gains[:1], parts[0][8:9], gains[8:9], parts[2][:1]], axis=1
+    )
+    for d in range(out_ref.shape[0]):
+        out_ref[d] = modulation
+
+
+def square_kernel(own_ref, other_ref, out_ref):
+    ones = jnp.ones((8, own_ref.shape[1]), jnp.float32)
+    total = None
+    for ref in (own_ref, other_ref):
+        values = ref[...].astype(jnp.float32)
+        term = dot_t(ones, values * values, precision=lax.Precision.HIGHEST)
+        total = term if total is None else total + term
+    out_ref[...] = total
 
 
 def project_kernel(
-    own_ref, other_ref, stat_ref, w_own_ref, w_other_ref, out_ref, gate_ref, *, sp, tp, rows
+    own_ref, other_ref, mod_ref, w_own_ref, w_other_ref, sq_ref, *refs, sp, tp, rows
 ):
+    out_ref, gate_ref = refs[-2:]
     count, features = own_ref.shape
     ctx_rows = count - rows
     rank = w_own_ref.shape[1]
-    half, width = rank // 2, ROPE // 2
-    base, chip, side, me = place()
-    apart = jnp.zeros((1, count), jnp.float32)
-    for t in range(tp):
-        term = stat_ref[base + t][:, :count]
-        apart = apart + jnp.where(chip == t // 2, jnp.zeros_like(term), term)
-    apart = jnp.transpose(jnp.broadcast_to(apart, (8, count)))[:, :1]
-    mine, partner = stat_ref[me], stat_ref[me + 1 - 2 * side]
+    half = rank // 2
+    side = place()[2]
+    total = sq_ref[...]
+    for ref in refs[:-2]:
+        total = total + ref[...]
+    total = jnp.transpose(total)[:, :1]
+    mine, partner = mod_ref[side], mod_ref[1 - side]
     for s in range(1, sp):
-        mine = mine + stat_ref[s * tp + me]
-        partner = partner + stat_ref[s * tp + me + 1 - 2 * side]
-    gate_ref[...] = mine[:, 4 * features : 5 * features]
+        mine = mine + mod_ref[2 * s + side]
+        partner = partner + mod_ref[2 * s + 1 - side]
+    gate_ref[...] = mine[:, 4 * features :]
 
     def split(ref):
         packed = ref[features:]
@@ -302,10 +295,9 @@
 
     w_own, w_other = split(w_own_ref), split(w_other_ref)
 
-    def rows_of(part, apart, kind):
+    def rows_of(part, kind):
         own, other = own_ref[part].astype(jnp.float32), other_ref[part].astype(jnp.float32)
-        total = jnp.sum(own * own + other * other, axis=1, keepdims=True) + apart
-        inverse = lax.rsqrt(total / D + EPS)
+        inverse = lax.rsqrt(total[part] / D + EPS)
         first = second = rot = None
         for values, vectors, weights in ((own, mine, w_own), (other, partner, w_other)):
             shift = vectors[:, 2 * kind * features : (2 * kind + 1) * features]
@@ -321,8 +313,8 @@
                 second, rot = second + terms[1], rot + terms[2]
         return first, second, rot
 
-    lat_q, lat_kv, lat_rot = rows_of(slice(0, rows), apart[:rows], 0)
-    unused, ctx_kv, ctx_rot = rows_of(slice(rows, count), apart[rows:], 1)
+    lat_q, lat_kv, lat_rot = rows_of(slice(0, rows), 0)
+    _, ctx_kv, ctx_rot = rows_of(slice(rows, count), 1)
     lat, ctx = rows // tp, ctx_rows // tp
     quarter = (lat + ctx) // 4
     for d in range(tp):
@@ -341,7 +333,7 @@
         )
 
 
-def norm_kernel(part_ref, gq_ref, gkv_ref, tab_ref, kv_ref, cq_ref, *, lat, ctx):
+def norm_kernel(part_ref, gq_ref, gkv_ref, tab_ref, kv_ref, near_ref, *, lat, ctx):
     chips = part_ref.shape[0] // 2
     halves = []
     for core in range(2):
@@ -383,111 +375,165 @@
         swapped = jnp.concatenate([turned[:, width // 2 :], turned[:, : width // 2]], axis=1)
         lat_rot.append(turned * tab_ref[0, core] + swapped * tab_ref[1, core])
         ctx_rot.append(rot[lat:])
-    zeros = jnp.zeros((lat + ctx, 128 - ROPE), jnp.float32)
     keys = jnp.concatenate(
         [jnp.concatenate(lat_rot, axis=1), jnp.concatenate(ctx_rot, axis=1)], axis=0
     )
-    keys = jnp.concatenate([keys, zeros], axis=1).astype(jnp.bfloat16)
+    pieces = rank // ROPE
+    low = (lat + ctx) // pieces
+    keys = jnp.concatenate(
+        [keys[i * low : (i + 1) * low] for i in range(pieces)], axis=1
+    ).astype(jnp.bfloat16)
     compressed = jnp.concatenate([lat_kv, ctx_kv], axis=0)
-    for copy in range(kv_ref.shape[0]):
-        kv_ref[copy, :, :rank] = compressed
-        kv_ref[copy, :, rank:] = keys
-    cq_ref[...] = cq
-
-
-def query_kernel(own_ref, other_ref, tab_ref, w_ref, out_ref, cq_ref):
-    chips, count = own_ref.shape[:2]
+    for ref in [kv_ref.at[copy] for copy in range(kv_ref.shape[0])] + [near_ref]:
+        ref[: lat + ctx] = compressed
+        ref[lat + ctx : lat + ctx + low] = keys
+    near_ref[lat + ctx + low :] = cq
+
+
+def gather_kernel(kv_ref, out_ref):
+    planes, size = kv_ref.shape[:2]
+    here = lax.axis_index("sp")
+    for i in range(planes - 1):
+        out_ref[i * size : (i + 1) * size] = kv_ref[lax.rem(here + 1 + i, planes)]
+
+
+def unpack(chunks, kv_ref, key_ref, lat, ctx):
+    count = lat + ctx
+    rank = kv_ref.shape[1]
+    row = lax.broadcasted_iota(jnp.int32, (count, 128 - ROPE), 0)
+    lane = lax.broadcasted_iota(jnp.int32, (count, 128 - ROPE), 1)
+    flags = jnp.where((row >= lat) & (lane < 3), 1.0, 0.0)
+    for i, (ref, at) in enumerate(chunks):
+        kv_ref[i * count : (i + 1) * count] = ref[at : at + count]
+        low = count * ROPE // rank
+        packed = ref[at + count : at + count + low].astype(jnp.float32)
+        rot = [packed[:, j * ROPE : (j + 1) * ROPE] for j in range(rank // ROPE)]
+        rot = jnp.concatenate([jnp.concatenate(rot, axis=0), flags], axis=1)
+        key_ref[i * count : (i + 1) * count] = rot.astype(jnp.bfloat16)
+
+
+def expanded(kv_ref, w_ref, head):
+    weight = w_ref[:, head * (NOPE + DV) : (head + 1) * (NOPE + DV)]
+    return jnp.dot(kv_ref[...], weight, preferred_element_type=jnp.float32).astype(jnp.bfloat16)
+
+
+def weighted(query, keys, values):
+    score = dot_t(query, keys)
+    peak = jnp.max(score, axis=1, keepdims=True)
+    probs = jnp.exp2((score - peak) * ((NOPE + ROPE) ** -0.5 * LOG2E))
+    total = jnp.sum(probs, axis=1, keepdims=True)
+    summed = jnp.dot(probs.astype(jnp.bfloat16), values, preferred_element_type=jnp.float32)
+    return peak, total, summed
+
+
+def near_kernel(tab_ref, lift_ref, wq_ref, wkv_ref, *refs, lat, ctx, chips):
+    own_refs, other_refs = refs[:chips], refs[chips : 2 * chips]
+    query_ref, stat_ref, sum_ref, cq_ref, kv_ref, key_ref = refs[-6:]
+    size = own_refs[0].shape[0]
     unused, here, side, unused = place()
-    first = side == 0
-    for chip in range(chips):
-        own, other = own_ref[chip ^ here], other_ref[chip ^ here]
-        at = 2 * chip * count
-        cq_ref[at : at + count] = jnp.where(first, own, other)
-        cq_ref[at + count : at + 2 * count] = jnp.where(first, other, own)
+    for hop in range(chips):
+        own, other = own_refs[hop][size - lat :], other_refs[hop][size - lat :]
+        at = pl.multiple_of(2 * (here ^ hop) * lat, 16)
+        cq_ref[pl.ds(at, lat)] = jnp.where(side == 0, own, other)
+        cq_ref[pl.ds(at + lat, lat)] = jnp.where(side == 0, other, own)
+    chunks = [(ref, 0) for ref in own_refs + other_refs]
+    chunks += chunks_of(refs[2 * chips : -6], size - lat)
+    unpack(chunks, kv_ref, key_ref, lat, ctx)
+    stats = jnp.zeros(stat_ref.shape, jnp.float32)
+    spot = lax.broadcasted_iota(jnp.int32, stat_ref.shape, 1)
+    heads = wq_ref.shape[0]
     quarter = ROPE // 4
-    for head in range(w_ref.shape[0]):
-        pieces = [w_ref[head]]
+    lane = lax.broadcasted_iota(jnp.int32, (1, 2 * ROPE), 1)
+    for head in range(wq_ref.shape[0]):
+        pieces = [wq_ref[head]]
         for block in (1, 0, 3, 2):
-            pieces.append(w_ref[head, NOPE + block * quarter : NOPE + (block + 1) * quarter])
+            pieces.append(wq_ref[head, NOPE + block * quarter : NOPE + (block + 1) * quarter])
         raw = dot_t(cq_ref[...], jnp.concatenate(pieces, axis=0))
         turned = raw[:, NOPE:] * tab_ref[...]
         turned = turned + pltpu.roll(turned, ROPE, 1)
-        out_ref[head] = jnp.concatenate([raw[:, :NOPE], turned], axis=1).astype(jnp.bfloat16)
-
-
-def expand_kernel(kv_ref, w_ref, out_ref):
-    rank = w_ref.shape[0]
-    values = kv_ref[...].reshape(out_ref.shape[1], kv_ref.shape[2])[:, :rank]
-    for head in range(out_ref.shape[0]):
-        weight = w_ref[:, head * (NOPE + DV) : (head + 1) * (NOPE + DV)]
-        out_ref[head] = jnp.dot(values, weight, preferred_element_type=jnp.float32).astype(
-            jnp.bfloat16
-        )
-
-
-def attend_kernel(
-    lift_ref, query_ref, pairs_ref, own_ref, other_ref, w_ref, out_ref, key_ref, value_ref, *, lat
-):
-    rank = w_ref.shape[0]
-    heads, count = pairs_ref.shape[:2]
-    for at, ref in ((0, own_ref), (count, other_ref)):
-        key_ref[at : at + count, NOPE:] = ref[:, :, rank:].reshape(count, 128)
-    position = lax.broadcasted_iota(jnp.int32, (1, 2 * count), 1)
-    context = lax.rem(position, lat[0] + lat[1]) >= lat[0]
-
-    @pl.loop(0, heads)
-    def _(head):
-        other = other_ref[...].reshape(count, other_ref.shape[2])[:, :rank]
-        width = NOPE + DV
-        weight = w_ref[:, pl.ds(pl.multiple_of(head * width, width), width)]
-        pairs = jnp.dot(other, weight, preferred_element_type=jnp.float32).astype(jnp.bfloat16)
-        key_ref[:count, :NOPE] = pairs_ref[head, :, :NOPE]
-        key_ref[count:, :NOPE] = pairs[:, :NOPE]
-        value_ref[:count] = pairs_ref[head, :, NOPE:]
-        value_ref[count:] = pairs[:, NOPE:]
-        score = dot_t(query_ref[head], key_ref[...])
-        lift = lift_ref[pl.ds(head, 1), :1]
-        score = score * (NOPE + ROPE) ** -0.5 + jnp.where(context, lift, 0.0)
-        peak = jnp.max(score, axis=1, keepdims=True)
-        probs = jnp.exp(score - peak)
-        total = jnp.sum(probs, axis=1, keepdims=True)
-        summed = jnp.dot(
-            probs.astype(jnp.bfloat16), value_ref[...], preferred_element_type=jnp.float32
-        )
-        out_ref[:, pl.ds(pl.multiple_of(head * DV, DV), DV)] = (summed / total).astype(jnp.bfloat16)
+        lift = lift_ref[head : head + 1] * (NOPE + ROPE) ** 0.5
+        first = lift.astype(jnp.bfloat16).astype(jnp.float32)
+        second = (lift - first).astype(jnp.bfloat16).astype(jnp.float32)
+        third = lift - first - second
+        lifts = jnp.where(lane == ROPE, first, jnp.where(lane == ROPE + 1, second, third))
+        lifts = jnp.where(lane < ROPE + 3, lifts, 0.0)
+        turned = jnp.where(lane < ROPE, turned, lifts)
+        query = jnp.concatenate([raw[:, :NOPE], turned], axis=1).astype(jnp.bfloat16)
+        query_ref[head] = query
+        pairs = expanded(kv_ref, wkv_ref, head)
+        keys = jnp.concatenate([pairs[:, :NOPE], key_ref[...]], axis=1)
+        peak, total, summed = weighted(query, keys, pairs[:, NOPE:])
+        stats = jnp.where(spot == head, peak, jnp.where(spot == heads + head, total, stats))
+        sum_ref[head] = summed
+    stat_ref[...] = stats
+
+
+def chunks_of(refs, step):
+    return [(ref, at) for ref in refs for at in range(0, refs[0].shape[0], step)]
+
+
+def expand_kernel(w_ref, *refs, lat, ctx):
+    key_ref, value_ref, kv_ref, rot_ref = refs[-4:]
+    step = lat + ctx + (lat + ctx) * ROPE // w_ref.shape[0]
+    unpack(chunks_of(refs[:-4], step), kv_ref, rot_ref, lat, ctx)
+    for head in range(key_ref.shape[0]):
+        pairs = expanded(kv_ref, w_ref, head)
+        key_ref[head, :, :NOPE] = pairs[:, :NOPE]
+        key_ref[head, :, NOPE:] = rot_ref[...]
+        value_ref[head] = pairs[:, NOPE:]
+
+
+def far_kernel(query_ref, stat_ref, sum_ref, key_ref, value_ref, w_ref, *refs, lat, ctx):
+    out_ref, kv_ref, rot_ref = refs[-3:]
+    step = lat + ctx + (lat + ctx) * ROPE // w_ref.shape[0]
+    unpack(chunks_of(refs[:-3], step), kv_ref, rot_ref, lat, ctx)
+    heads = query_ref.shape[0]
+    factor = (NOPE + ROPE) ** -0.5 * LOG2E
+    for head in range(query_ref.shape[0]):
+        pairs = expanded(kv_ref, w_ref, head)
+        keys = jnp.concatenate([pairs[:, :NOPE], rot_ref[...]], axis=1)
+        keys = jnp.concatenate([key_ref[head], keys], axis=0)
+        values = jnp.concatenate([value_ref[head], pairs[:, NOPE:]], axis=0)
+        peak, total, summed = weighted(query_ref[head], keys, values)
+        near = stat_ref[:, head : head + 1]
+        top = jnp.maximum(peak, near)
+        new, old = jnp.exp2((peak - top) * factor), jnp.exp2((near - top) * factor)
+        total = total * new + stat_ref[:, heads + head : heads + head + 1] * old
+        summed = summed * new + sum_ref[head] * old
+        out_ref[:, head * DV : (head + 1) * DV] = (summed / total).astype(jnp.bfloat16)
 
 
 def share_out_kernel(w_ref, out_ref):
     chips, unused, features = out_ref.shape
-    side = place()[2]
-    for chip in range(chips):
-        start = pl.multiple_of((2 * chip + 1 - side) * features, features)
-        out_ref[chip] = w_ref[:, pl.ds(start, features)]
+    unused, here, side, unused = place()
+    for hop in range(chips):
+        start = pl.multiple_of((2 * (here ^ hop) + 1 - side) * features, features)
+        out_ref[hop] = w_ref[:, pl.ds(start, features)]
 
 
 def output_own_kernel(heads_ref, w_ref, out_ref):
     chips, unused, features = out_ref.shape
-    side = place()[2]
-    for chip in range(chips):
-        start = pl.multiple_of((2 * chip + side) * features, features)
-        out_ref[chip] = jnp.dot(
+    unused, here, side, unused = place()
+    for hop in range(chips):
+        start = pl.multiple_of((2 * (here ^ hop) + side) * features, features)
+        out_ref[hop] = jnp.dot(
             heads_ref[...], w_ref[:, pl.ds(start, features)], preferred_element_type=jnp.float32
         )
 
 
-def output_kernel(heads_ref, w_ref, acc_ref, out_ref):
-    for chip in range(out_ref.shape[0]):
-        acc = acc_ref[chip] + jnp.dot(
-            heads_ref[...], w_ref[chip], preferred_element_type=jnp.float32
-        )
-        out_ref[chip] = acc.astype(jnp.bfloat16)
-
-
-def mix_kernel(latent_ref, gate_ref, branch_ref, out_ref):
-    branch = branch_ref[0].astype(jnp.float32)
-    for chip in range(1, branch_ref.shape[0]):
-        branch = branch + branch_ref[chip].astype(jnp.float32)
-    out_ref[...] = (latent_ref[...].astype(jnp.float32) + gate_ref[...] * branch).astype(
+def output_kernel(heads_ref, w_ref, acc_ref, *out_refs):
+    for hop in reversed(range(len(out_refs))):
+        acc = acc_ref[hop] + jnp.dot(
+            heads_ref[...], w_ref[hop], preferred_element_type=jnp.float32
+        )
+        out_refs[hop][...] = acc.astype(out_refs[hop].dtype)
+
+
+def mix_kernel(latent_ref, gate_ref, *refs):
+    branch = refs[0][...]
+    for ref in refs[1:-1]:
+        branch = branch + ref[...].astype(jnp.float32)
+    refs[-1][...] = (latent_ref[...].astype(jnp.float32) + gate_ref[...] * branch).astype(
         jnp.bfloat16
     )
 
@@ -518,37 +564,41 @@
     rank = w_dq.shape[1]
     lat, ctx = rows // tp, ctx_rows // tp
     half = rank // 2
-    sides = [list(range(k, tp, 2)) for k in range(2)]
     across = [(i, i ^ 1) for i in range(tp)]
     me = lax.axis_index("tp")
 
     def array(shape, dtype=bf16):
         return jax.ShapeDtypeStruct(shape, dtype)
 
-    size = max(5 * features, rows + ctx_rows)
-    stat, tokens = call(
-        functools.partial(stats_kernel, sp=sp, tp=tp),
-        (array((sp * tp, 1, size), f32), array((rows + ctx_rows, features))),
+    def hopped(value):
+        return [value] + [
+            lax.ppermute(value, "tp", [(i, i ^ (2 * hop)) for i in range(tp)])
+            for hop in range(1, chips)
+        ]
+
+    modulation, tokens = call(
+        functools.partial(stats_kernel, sp=sp),
+        (array((2 * sp, 1, 5 * features), f32), array((rows + ctx_rows, features))),
         latent,
         context,
-        cond[None],
-        cond_ctx[None],
+        cond,
+        cond_ctx,
         jnp.transpose(w_mod, (1, 0, 2)),
-        g_norm[None],
-        name="stats",
-        held=False,
-    )
-    stat = lax.all_to_all(stat, ("sp", "tp"), 0, 0)
+        g_norm,
+        held=pltpu.HBM,
+    )
+    tokens_other = lax.ppermute(tokens, "tp", across)
+    columns = [[s * tp + 2 * c + k for s in range(sp) for k in range(2)] for c in range(chips)]
+    modulation = lax.all_to_all(modulation, ("sp", "tp"), 0, 0, axis_index_groups=columns)
+    squares = call(square_kernel, array((8, rows + ctx_rows), f32), tokens, tokens_other)
+    squares = hopped(squares)
 
     share = array((features + ROPE // 2 * features // rank, rank))
-    w_own, w_other = call(share_kernel, (share, share), w_dq, w_dkv, w_kr.T, name="share", held=False)
-    tokens_other = lax.ppermute(tokens, "tp", across)
+    w_own, w_other = call(share_kernel, (share, share), w_dq, w_dkv, w_kr.T, held=pltpu.HBM)
     w_other = lax.ppermute(w_other, "tp", across)
     w_up = w_out.reshape(heads * DV, 2 * chips * features)
-    w_up_share = call(
-        share_out_kernel, array((chips, heads * DV, features)), w_up, flops=1e9, name="share_out"
-    )
-    stat, w_up_share = lax.optimization_barrier((stat, w_up_share))
+    w_up_share = call(share_out_kernel, array((chips, heads * DV, features)), w_up, flops=1e9)
+    modulation, w_up_share = lax.optimization_barrier((modulation, w_up_share))
     w_up_other = lax.ppermute(w_up_share, "tp", across)
 
     height = half // 128 * (2 * lat + ctx) + (lat + ctx) // 4
@@ -557,12 +607,12 @@
         (array((tp, height, 128), f32), array((1, features), f32)),
         tokens,
         tokens_other,
-        stat,
+        modulation,
         w_own,
         w_other,
+        *squares,
         flops=4 * (rows + ctx_rows) * features * (rank + 128),
         limit=16,
-        name="project",
     )
     part, w_kv, zero = lax.optimization_barrier((part, w_ukv, jnp.int32(0)))
     part = lax.all_to_all(part, "tp", 0, 0)
@@ -577,86 +627,96 @@
     w_kv = w_kv.reshape(rank, heads * (NOPE + DV))
     part, q_tab, w_up_other, w_kv = lax.optimization_barrier((part, q_tab, w_up_other, w_kv))
 
-    kv, cq = call(
+    count = lat + ctx
+    step = count + count * ROPE // rank
+    kv, near = call(
         functools.partial(norm_kernel, lat=lat, ctx=ctx),
-        (array((sp, lat + ctx, rank + 128)), array((lat, rank))),
+        (array((sp, step, rank)), array((step + lat, rank))),
         part,
         g_cq[None],
         g_ckv[None],
         k_tab,
-        name="norm",
-    )
-
-    kv = lax.all_to_all(kv, "sp", 0, 0).reshape(1, sp * (lat + ctx), rank + 128)
-    near = [cq]
-    for hop in range(1, chips):
-        swap = [(i, i ^ (2 * hop)) for i in range(tp)]
-        near.append(lax.ppermute(cq, "tp", swap))
-    cq_own, kv = lax.optimization_barrier((jnp.stack(near), kv))
-    cq_other = lax.ppermute(cq_own, "tp", across)
-    kv = jnp.broadcast_to(kv, (chips,) + kv.shape[1:])
-    kv_own = lax.all_to_all(kv, "tp", 0, 0, axis_index_groups=sides)
-    kv_other = lax.ppermute(kv_own, "tp", across)
-
-    keys = sp * (rows + ctx_rows)
-    query = call(
-        query_kernel,
-        array((heads, rows, 2 * NOPE)),
-        cq_own,
-        cq_other,
+    )
+
+    kv = lax.all_to_all(kv, "sp", 0, 0)
+    near_own = hopped(near)
+    *near_own, kv = lax.optimization_barrier((*near_own, kv))
+    near_other = [lax.ppermute(n, "tp", across) for n in near_own]
+    far = call(gather_kernel, array(((sp - 1) * step, rank)), kv)
+    far_own = hopped(far)
+    far_other = [lax.ppermute(f, "tp", across) for f in far_own]
+
+    keys = (tp + 2 * (sp - 1)) * count
+    query, stats, summed = call(
+        functools.partial(near_kernel, lat=lat, ctx=ctx, chips=chips),
+        (
+            array((heads, rows, 2 * NOPE)),
+            array((rows, 128), f32),
+            array((heads, rows, DV), f32),
+        ),
         q_tab,
+        jnp.broadcast_to(ctx_lift[:, None], (heads, 128)),
         jnp.transpose(w_uq, (1, 2, 0)),
-        scratch=[pltpu.VMEM((rows, rank), bf16)],
-        flops=2 * rows * rank * 256 * heads,
-        name="query",
-    )
-    pairs = call(
-        expand_kernel,
-        array((heads, keys // 2, NOPE + DV)),
-        kv_own,
         w_kv,
-        flops=keys * rank * 256 * heads,
-        name="expand",
+        *near_own,
+        *near_other,
+        far_own[0],
+        far_other[0],
+        scratch=[
+            pltpu.VMEM((rows, rank), bf16),
+            pltpu.VMEM((keys, rank), bf16),
+            pltpu.VMEM((keys, 128), bf16),
+        ],
+        flops=heads * rows * (2 * rank * 256 + 2 * keys * 384),
+        limit=16,
+    )
+    keys = (chips - 1) * (sp - 1) * count
+    scratch = [pltpu.VMEM((keys, rank), bf16), pltpu.VMEM((keys, 128), bf16)]
+    far_keys, far_values = call(
+        functools.partial(expand_kernel, lat=lat, ctx=ctx),
+        (array((heads, keys, 2 * NOPE)), array((heads, keys, DV))),
+        w_kv,
+        *far_own[1:],
+        scratch=scratch,
+        flops=2 * keys * rank * 256 * heads,
     )
     heads_out = call(
-        functools.partial(attend_kernel, lat=(lat, ctx)),
+        functools.partial(far_kernel, lat=lat, ctx=ctx),
         array((rows, heads * DV)),
-        jnp.broadcast_to(ctx_lift[:, None], (heads, 128)),
         query,
-        pairs,
-        kv_own,
-        kv_other,
+        stats,
+        summed,
+        far_keys,
+        far_values,
         w_kv,
-        scratch=[pltpu.VMEM((keys, 2 * NOPE), bf16), pltpu.VMEM((keys, DV), bf16)],
-        flops=heads * keys * (2 * rows * 384 + rank * 256),
-        limit=24,
-        name="attend",
+        *far_other[1:],
+        scratch=scratch,
+        flops=2 * heads * keys * (2 * rows * 384 + rank * 256),
+        limit=28,
     )
 
     heads_other = lax.ppermute(heads_out, "tp", across)
     flops = 2 * rows * heads * DV * chips * features
     branch = call(
-        output_own_kernel,
-        array((chips, rows, features), f32),
-        heads_out,
-        w_up,
-        flops=flops,
-        name="output_own",
-    )
-    branch = call(
+        output_own_kernel, array((chips, rows, features), f32), heads_out, w_up, flops=flops
+    )
+    block = array((rows, features))
+    branch, *apart = call(
         output_kernel,
-        array((chips, rows, features)),
+        (array((rows, features), f32),) + (block,) * (chips - 1),
         heads_other,
         w_up_other,
         branch,
         flops=flops,
-        name="output",
-    )
-    branch = lax.all_to_all(branch, "tp", 0, 0, axis_index_groups=sides)
-    return call(mix_kernel, array(latent.shape), latent, gate, branch, name="mix", kept=False)
-
-
-def per_device(*arrays):
+    )
+    apart = [
+        lax.ppermute(a, "tp", [(i, i ^ (2 * hop + 2)) for i in range(tp)])
+        for hop, a in enumerate(apart)
+    ]
+    return call(mix_kernel, array(latent.shape), latent, gate, branch, *apart, kept=False)
+
+
+def chosen(*arrays):
     rows, ctx_rows, features = arrays[0].shape[0], arrays[1].shape[0], arrays[0].shape[1]
     tp = lax.axis_size("tp")
     aligned = rows % (16 * tp) == 0 and ctx_rows % (16 * tp) == 0 and features % 128 == 0 and arrays[6].shape[1] % features == 0
@@ -665,7 +725,7 @@
 
 def solution(mesh):
     return jax.shard_map(
-        per_device,
+        chosen,
         mesh=mesh,
         in_specs=(
             P("sp", "tp"),

time: 109 us -> 101 us (0.927)
  blocking collectives: 34.8 us -> 0 us
  waiting for transfers between devices: 19.6 us -> 32.5 us
  starting transfers between devices: 19.6 us -> 31.6 us
  Pallas kernels: 19.3 us -> 22.8 us
  local copies, waits for them, and re-layouts: 14.6 us -> 11.9 us
    all_to_all x2 -> x0, blocking collectives: 34.8 us -> none  [the longest x1 20.3 us: split_device(): kv_own = lax.all_to_all(kv, 'tp', 0, 0, axis_index_groups=sides)]
    ppermute x5 -> x20, waiting for transfers between devices: 5.37 us -> 24.5 us  [the longest x9 15.7 us: hopped(): lax.ppermute(value, 'tp', [(i, i ^ 2 * hop) for i in range(tp)])]
    ppermute x5 -> x20, starting transfers between devices: 4.06 us -> 15.8 us  [the longest x9 10.5 us: hopped(): lax.ppermute(value, 'tp', [(i, i ^ 2 * hop) for i in range(tp)])]
    all_to_all x2, waiting for transfers between devices: 3.75 us -> 0.2 us  [the longest x1 0.2 us: split_device(): lax.all_to_all(modulation, ('sp', 'tp'), 0, 0, axis_index_groups=columns)]
    pallas_call x11 -> x13, Pallas kernels: 19.3 us -> 22.8 us  [call(): pl.pallas_call(kernel, in_specs=[vmem] * len(args), out_specs=(vmem,) * l...]
    all_to_all x1, waiting for transfers between devices: 9.43 us -> 6.71 us  [split_device(): part = lax.all_to_all(part, 'tp', 0, 0)]
    unnamed x31 -> x35, local copies, waits for them, and re-layouts: 10 us -> 7.52 us
    broadcast_in_dim x3 -> x0, local copies, waits for them, and re-layouts: 1.47 us -> none  [the longest x1 0.68 us: split_device(): cond[None]]
  transfers between devices with their start and end apart: 12 -> 27, of which waited for: 8 -> 12; matrix products, arithmetic and copies ran while one was open for 4% -> 8% of each run, Pallas kernels for 3% -> 11%
where the time goes in v3:
time: 101 us; the launch traced here: 100 us
  waiting for transfers between devices  32.5 us (32%)
  starting transfers between devices  31.6 us (31%)
  Pallas kernels  22.8 us (23%)
  local copies, waits for them, and re-layouts  11.9 us (12%)
  other arithmetic  1.08 us (1%)
    pallas_call x13, Pallas kernels, call(): pl.pallas_call(kernel, in_specs=[vmem] * len(args), out_specs=(vmem,) * l...  22.8 us
    ppermute x9, waiting for transfers between devices, hopped(): lax.ppermute(value, 'tp', [(i, i ^ 2 * hop) for i in range(tp)])  15.7 us
    ppermute x9, starting transfers between devices, hopped(): lax.ppermute(value, 'tp', [(i, i ^ 2 * hop) for i in range(tp)])  10.5 us
    ppermute x3, waiting for transfers between devices, split_device(): lax.ppermute(a, 'tp', [(i, i ^ 2 * hop + 2) for i in range(tp)])  7.75 us
    unnamed x35, local copies, waits for them, and re-layouts  7.52 us
    all_to_all x1, waiting for transfers between devices, split_device(): part = lax.all_to_all(part, 'tp', 0, 0)  6.71 us
    all_to_all x1, starting transfers between devices, split_device(): lax.all_to_all(modulation, ('sp', 'tp'), 0, 0, axis_index_groups=columns)  6.35 us
    all_to_all x1, starting transfers between devices, split_device(): kv = lax.all_to_all(kv, 'sp', 0, 0)  5.22 us
  transfers between devices with their start and end apart: 27, of which 12 were waited for; matrix products, arithmetic and copies ran while one was open for 8% of the time, Pallas kernels for 11%

profile of v3, /device:TPU:0, one launch (start us, length us, event | category | flops | bytes accessed | tf_op | source)
XLA Modules:
  0.0 100.2 jit_solution(4767792153081093913)
XLA Ops:
  0.0 2.3 %shard_map.145 = (f32[8,1,1280]{2,1,0:T(1,128)}, bf16[512,256]{1,0:T(8,128)(2,1)S(1)}) custom-call(bf16[384,256]{1,0:T(8,128)(2,1)} %latent_ref.1, bf16[128,256]{1,0:T(8,128)(2,1)} %ctx_ref.1, bf16[512]{0:T(512)(128)(2,1)} %cond_ref.1, bf16[512]{0:T(512)(128)(2,1)} %cond_ctx_ref.1, bf16[3,512,256]{2,1,0:T(8,128)(2,1)} %bitcast.20, f32[256]{0:T(256)} %g_ref.1), custom_call_target="tpu_custom_call" | custom-call | flops 1000000 | bytes 100000 | tf_op jit(solution)/shard_map/pallas_call | solution.py:204
  2.3 0.5 collective-permute-start
  2.8 1.1 %shard_map.147 = (bf16[272,512]{1,0:T(8,128)(2,1)S(1)}, bf16[272,512]{1,0:T(8,128)(2,1)S(1)}) custom-call(bf16[256,512]{1,0:T(8,128)(2,1)} %wq_ref.1, bf16[256,512]{1,0:T(8,128)(2,1)} %wkv_ref.1, bf16[64,256]{1,0:T(8,128)(2,1)} %bitcast.22), custom_call_target="tpu_custom_call" | custom-call | flops 1000000 | bytes 100000 | tf_op jit(solution)/shard_map/pallas_call | solution.py:204
  3.9 0.1 collective-permute-start.1
  4.0 6.4 %all-to-all-start = ((f32[8,1,1280]{2,1,0:T(1,128)}), f32[8,1,1280]{2,1,0:T(1,128)S(1)}, u32[]{:S(2)}, u32[]{:S(2)}) async-start(f32[8,1,1280]{2,1,0:T(1,128)} %get-tuple-element.37), calls=%async_computation | async-start | bytes 81920 | tf_op jit(solution)/shard_map/all_to_all | solution.py:592
  10.3 0.9 shard_map.148.sq_ref
  11.3 1.5 %collective-permute-start.2 = (f32[8,512]{1,0:T(8,128)S(1)}, f32[8,512]{1,0:T(8,128)S(1)}, u32[]{:S(2)}, u32[]{:S(2)}) collective-permute-start(f32[8,512]{1,0:T(8,128)S(1)} %shard_map.148.sq_ref), channel_id=1, source_target_pairs={{0,2},{1,3},{2,0},{3,1},{4,6},{5,7},{6,4},{7,5},{8,10},{9,11},{10,... | collective-permute-start | bytes 49160 | tf_op jit(solution)/shard_map/ppermute | solution.py:575
  12.8 1.5 %collective-permute-start.3 = (f32[8,512]{1,0:T(8,128)S(1)}, f32[8,512]{1,0:T(8,128)S(1)}, u32[]{:S(2)}, u32[]{:S(2)}) collective-permute-start(f32[8,512]{1,0:T(8,128)S(1)} %shard_map.148.sq_ref), channel_id=1, source_target_pairs={{0,4},{1,5},{2,6},{3,7},{4,0},{5,1},{6,2},{7,3},{8,12},{9,13},{10,... | collective-permute-start | bytes 49160 | tf_op jit(solution)/shard_map/ppermute | solution.py:575
  14.3 0.5 collective-permute-start.4
  14.8 0.1 shard_map.146
  14.9 1.0 copy-done.8
  15.9 0.2 all-to-all-done.mod_ref
  16.1 0.0 collective-permute-done.2.refs_0_
  16.1 0.4 collective-permute-done.3.refs_1_
  16.5 2.5 %collective-permute-done.4.refs_2_ = f32[8,512]{1,0:T(8,128)} collective-permute-done((f32[8,512]{1,0:T(8,128)S(1)}, f32[8,512]{1,0:T(8,128)}, u32[]{:S(2)}, u32[]{:S(2)}) %collective-permute-start.4) | collective-permute-done | bytes 16416 | tf_op jit(solution)/shard_map/ppermute | solution.py:575
  19.0 1.5 %shard_map.149 = (f32[8,240,128]{2,1,0:T(8,128)S(1)}, f32[1,256]{1,0:T(1,128)S(1)}) custom-call(bf16[512,256]{1,0:T(8,128)(2,1)S(1)} %get-tuple-element.36.own_ref, bf16[512,256]{1,0:T(8,128)(2,1)S(1)} %collective-permute-done.other_ref, f32[8,1,1280]{2,1,0:T(1,128)S(1)} %all-to-all-done.mod_ref, bf16[272,512]{1,0:T(8,128)(2,1)S(1)} %get-tuple-element.39.w_own_ref, ...), custom_call_target="tpu_custom_call" | custom-call | flops 335544320 | bytes 100000 | tf_op jit(solution)/shard_map/pallas_call | solution.py:204
  20.6 0.9 copy-done.4
  21.5 3.6 %all-to-all-start.1 = ((f32[8,240,128]{2,1,0:T(8,128)}), f32[8,240,128]{2,1,0:T(8,128)S(1)}, u32[]{:S(2)}, u32[]{:S(2)}) async-start(f32[8,240,128]{2,1,0:T(8,128)} %copy-done.4), calls=%async_computation.1 | async-start | bytes 1966080 | tf_op jit(solution)/shard_map/all_to_all | solution.py:618
  25.1 0.1 broadcast_multiply_fusion.1
  25.2 0.8 copy.18
  26.0 2.5 %copy.22 = bf16[64,8,4,256]{3,1,2,0:T(8,128)(2,1)} copy(bf16[64,8,4,256]{3,2,1,0:T(4,128)(2,1)} %bitcast.19) | data formatting | bytes 2097152
  28.4 0.7 fusion.6
  29.1 0.8 fusion.7
  30.0 1.0 fusion.5
  30.9 1.8 %concatenate.8.tab_ref = f32[384,128]{1,0:T(8,128)S(1)} concatenate(f32[384,16]{1,0:T(8,128)} %get-tuple-element.74, f32[384,32]{1,0:T(8,128)} %copy-done.14, f32[384,16]{1,0:T(8,128)} %get-tuple-element.73, f32[384,16]{1,0:T(8,128)} %get-tuple-element.68, f32[384,16]{1,0:T(8,128)} %get-tuple-element.70, f32[384,16]{1,0:T(8,128)} %get-tuple-element.69, f32[384,16]{1,0:T(8,128)} %get-tuple-element.67), dimensions={1} | concatenate | bytes 393216 | tf_op jit(solution)/shard_map/concatenate | solution.py:624
  32.8 0.1 copy.20
  32.9 0.1 copy.21
  33.0 6.7 %all-to-all-done.1.part_ref = f32[8,240,128]{2,1,0:T(8,128)S(1)} async-done(((f32[8,240,128]{2,1,0:T(8,128)}), f32[8,240,128]{2,1,0:T(8,128)S(1)}, u32[]{:S(2)}, u32[]{:S(2)}) %all-to-all-start.1) | async-done | bytes 983072 | tf_op jit(solution)/shard_map/all_to_all | solution.py:618
  39.7 1.0 %shard_map.150 = (bf16[4,72,512]{2,1,0:T(8,128)(2,1)}, bf16[120,512]{1,0:T(8,128)(2,1)S(1)}) custom-call(f32[8,240,128]{2,1,0:T(8,128)S(1)} %all-to-all-done.1.part_ref, f32[1,512]{1,0:T(1,128)S(1)} %bitcast.16, f32[1,512]{1,0:T(1,128)S(1)} %bitcast.17, f32[2,2,48,32]{3,2,1,0:T(8,128)S(1)} %bitcast.15), custom_call_target="tpu_custom_call" | custom-call | flops 1000000 | bytes 100000 | tf_op jit(solution)/shard_map/pallas_call | solution.py:204
  40.7 5.2 %all-to-all-start.2 = ((bf16[4,72,512]{2,1,0:T(8,128)(2,1)}), bf16[4,72,512]{2,1,0:T(8,128)(2,1)S(1)}, u32[]{:S(2)}, u32[]{:S(2)}) async-start(bf16[4,72,512]{2,1,0:T(8,128)(2,1)} %get-tuple-element.51), calls=%async_computation.2 | async-start | bytes 589824 | tf_op jit(solution)/shard_map/all_to_all | solution.py:641
  45.9 0.5 collective-permute-start.6
  46.4 0.7 collective-permute-start.7
  47.1 2.3 %collective-permute-start.8 = (bf16[120,512]{1,0:T(8,128)(2,1)S(1)}, bf16[120,512]{1,0:T(8,128)(2,1)}, u32[]{:S(2)}, u32[]{:S(2)}) collective-permute-start(bf16[120,512]{1,0:T(8,128)(2,1)S(1)} %get-tuple-element.52.refs_0_), channel_id=1, source_target_pairs={{0,6},{1,7},{2,4},{3,5},{4,2},{5,3},{6,0},{7,1},{8,14},{9,15},{10,... | collective-permute-start | bytes 368648 | tf_op jit(solution)/shard_map/ppermute | solution.py:575
  49.4 2.5 %collective-permute-done.6.refs_1_ = bf16[120,512]{1,0:T(8,128)(2,1)S(1)} collective-permute-done((bf16[120,512]{1,0:T(8,128)(2,1)S(1)}, bf16[120,512]{1,0:T(8,128)(2,1)S(1)}, u32[]{:S(2)}, u32[]{:S(2)}) %collective-permute-start.6) | collective-permute-done | bytes 122912 | tf_op jit(solution)/shard_map/ppermute | solution.py:575
  51.9 1.9 %collective-permute-done.7.refs_2_ = bf16[120,512]{1,0:T(8,128)(2,1)S(1)} collective-permute-done((bf16[120,512]{1,0:T(8,128)(2,1)S(1)}, bf16[120,512]{1,0:T(8,128)(2,1)S(1)}, u32[]{:S(2)}, u32[]{:S(2)}) %collective-permute-start.7) | collective-permute-done | bytes 122912 | tf_op jit(solution)/shard_map/ppermute | solution.py:575
  53.8 0.6 copy-done.12
  54.5 0.1 collective-permute-start.9
  54.6 0.5 collective-permute-start.10
  55.1 1.8 %collective-permute-start.14 = (bf16[216,512]{1,0:T(8,128)(2,1)S(1)}, bf16[216,512]{1,0:T(8,128)(2,1)S(1)}, u32[]{:S(2)}, u32[]{:S(2)}) collective-permute-start(bf16[216,512]{1,0:T(8,128)(2,1)S(1)} %shard_map.151.refs_8_), channel_id=1, source_target_pairs={{0,2},{1,3},{2,0},{3,1},{4,6},{5,7},{6,4},{7,5},{8,10},{9,11},{10,... | collective-permute-start | bytes 663560 | tf_op jit(solution)/shard_map/ppermute | solution.py:575
  56.9 0.4 collective-permute-start.15
  57.3 1.4 %collective-permute-start.16 = (bf16[216,512]{1,0:T(8,128)(2,1)S(1)}, bf16[216,512]{1,0:T(8,128)(2,1)S(1)}, u32[]{:S(2)}, u32[]{:S(2)}) collective-permute-start(bf16[216,512]{1,0:T(8,128)(2,1)S(1)} %shard_map.151.refs_8_), channel_id=1, source_target_pairs={{0,6},{1,7},{2,4},{3,5},{4,2},{5,3},{6,0},{7,1},{8,14},{9,15},{10,... | collective-permute-start | bytes 663560 | tf_op jit(solution)/shard_map/ppermute | solution.py:575
  58.6 0.5 collective-permute-start.13
  59.1 1.0 %collective-permute-done.11.refs_6_ = bf16[120,512]{1,0:T(8,128)(2,1)S(1)} collective-permute-done((bf16[120,512]{1,0:T(8,128)(2,1)}, bf16[120,512]{1,0:T(8,128)(2,1)S(1)}, u32[]{:S(2)}, u32[]{:S(2)}) %collective-permute-start.11) | collective-permute-done | bytes 122912 | tf_op jit(solution)/shard_map/ppermute | solution.py:644
  60.2 0.1 collective-permute-start.12
  60.3 3.1 %collective-permute-done.14.refs_0_ = bf16[216,512]{1,0:T(8,128)(2,1)S(1)} collective-permute-done((bf16[216,512]{1,0:T(8,128)(2,1)S(1)}, bf16[216,512]{1,0:T(8,128)(2,1)S(1)}, u32[]{:S(2)}, u32[]{:S(2)}) %collective-permute-start.14) | collective-permute-done | bytes 221216 | tf_op jit(solution)/shard_map/ppermute | solution.py:575
  63.4 5.3 %collective-permute-done.15.refs_1_ = bf16[216,512]{1,0:T(8,128)(2,1)S(1)} collective-permute-done((bf16[216,512]{1,0:T(8,128)(2,1)S(1)}, bf16[216,512]{1,0:T(8,128)(2,1)S(1)}, u32[]{:S(2)}, u32[]{:S(2)}) %collective-permute-start.15) | collective-permute-done | bytes 221216 | tf_op jit(solution)/shard_map/ppermute | solution.py:575
  68.8 0.5 collective-permute-start.19
  69.3 1.2 %copy-done.1 = bf16[64,8,4,256]{3,1,2,0:T(8,128)(2,1)S(1)} copy-done((bf16[64,8,4,256]{3,1,2,0:T(8,128)(2,1)S(1)}, bf16[64,8,4,256]{3,1,2,0:T(8,128)(2,1)}, u32[]{:S(2)}) %copy-start.1) | copy-done | bytes 1048600
  70.5 0.8 shard_map.153
  71.3 0.1 broadcast_in_dim.6.lift_ref
  71.4 1.2 %copy-done.2 = bf16[64,8,4,256]{3,1,2,0:T(8,128)(2,1)S(1)} copy-done((bf16[64,8,4,256]{3,1,2,0:T(8,128)(2,1)S(1)}, bf16[64,8,4,256]{3,1,2,0:T(8,128)(2,1)}, u32[]{:S(2)}) %copy-start.2) | copy-done | bytes 1048600
  72.6 6.3 %shard_map.152 = (bf16[4,384,256]{2,1,0:T(8,128)(2,1)S(1)}, f32[384,128]{1,0:T(8,128)S(1)}, f32[4,384,128]{2,1,0:T(8,128)S(1)}) custom-call(f32[384,128]{1,0:T(8,128)S(1)} %concatenate.8.tab_ref, f32[4,128]{1,0:T(4,128)S(1)} %broadcast_in_dim.6.lift_ref, bf16[4,192,512]{2,1,0:T(8,128)(2,1)S(1)} %bitcast.18, bf16[512,1024]{1,0:T(8,128)(2,1)S(1)} %bitcast.13, ...), custom_call_target="tpu_custom_call" | custom-call | flops 1459617792 | bytes 100000 | tf_op jit(solution)/shard_map/pallas_call | solution.py:204
  79.0 5.5 %shard_map.154.heads_ref = bf16[384,512]{1,0:T(8,128)(2,1)S(1)} custom-call(bf16[4,384,256]{2,1,0:T(8,128)(2,1)S(1)} %get-tuple-element.57.query_ref, f32[384,128]{1,0:T(8,128)S(1)} %get-tuple-element.58.stat_ref, f32[4,384,128]{2,1,0:T(8,128)S(1)} %get-tuple-element.59.sum_ref, bf16[4,576,256]{2,1,0:T(8,128)(2,1)S(1)} %get-tuple-element.60.key_ref, ...), custom_call_target="tpu_custom_call" | custom-call | flops 1962934272 | bytes 100000 | tf_op jit(solution)/shard_map/pallas_call | solution.py:204
  84.5 0.1 collective-permute-start.20
  84.5 0.6 shard_map.155.acc_ref
  85.1 0.0 copy-start.5
  85.2 1.1 %collective-permute-done.20.heads_ref = bf16[384,512]{1,0:T(8,128)(2,1)S(1)} collective-permute-done((bf16[384,512]{1,0:T(8,128)(2,1)S(1)}, bf16[384,512]{1,0:T(8,128)(2,1)S(1)}, u32[]{:S(2)}, u32[]{:S(2)}) %collective-permute-start.20) | collective-permute-done | bytes 393248 | tf_op jit(solution)/shard_map/ppermute | solution.py:698
  86.3 1.8 %shard_map.156 = (f32[384,256]{1,0:T(8,128)S(1)}, bf16[384,256]{1,0:T(8,128)(2,1)S(1)}, bf16[384,256]{1,0:T(8,128)(2,1)S(1)}, bf16[384,256]{1,0:T(8,128)(2,1)S(1)}) custom-call(bf16[384,512]{1,0:T(8,128)(2,1)S(1)} %collective-permute-done.20.heads_ref, bf16[4,512,256]{2,1,0:T(8,128)(2,1)} %collective-permute-done.5.w_ref, f32[4,384,256]{2,1,0:T(8,128)S(1)} %shard_map.155.acc_ref), custom_call_target="tpu_custom_call" | custom-call | flops 402653184 | bytes 100000 | tf_op jit(solution)/shard_map/pallas_call | solution.py:204
  88.1 0.4 collective-permute-start.21
  88.5 1.0 %collective-permute-start.22 = (bf16[384,256]{1,0:T(8,128)(2,1)S(1)}, bf16[384,256]{1,0:T(8,128)(2,1)S(1)}, u32[]{:S(2)}, u32[]{:S(2)}) collective-permute-start(bf16[384,256]{1,0:T(8,128)(2,1)S(1)} %get-tuple-element.65), channel_id=1, source_target_pairs={{0,4},{1,5},{2,6},{3,7},{4,0},{5,1},{6,2},{7,3},{8,12},{9,13},{10,... | collective-permute-start | bytes 589832 | tf_op jit(solution)/shard_map/ppermute | solution.py:713
  89.5 2.1 %collective-permute-start.23 = (bf16[384,256]{1,0:T(8,128)(2,1)S(1)}, bf16[384,256]{1,0:T(8,128)(2,1)S(1)}, u32[]{:S(2)}, u32[]{:S(2)}) collective-permute-start(bf16[384,256]{1,0:T(8,128)(2,1)S(1)} %get-tuple-element.66), channel_id=1, source_target_pairs={{0,6},{1,7},{2,4},{3,5},{4,2},{5,3},{6,0},{7,1},{8,14},{9,15},{10,... | collective-permute-start | bytes 589832 | tf_op jit(solution)/shard_map/ppermute | solution.py:713
  91.6 4.3 %collective-permute-done.21.refs_1_ = bf16[384,256]{1,0:T(8,128)(2,1)S(1)} collective-permute-done((bf16[384,256]{1,0:T(8,128)(2,1)S(1)}, bf16[384,256]{1,0:T(8,128)(2,1)S(1)}, u32[]{:S(2)}, u32[]{:S(2)}) %collective-permute-start.21) | collective-permute-done | bytes 196640 | tf_op jit(solution)/shard_map/ppermute | solution.py:713
  95.9 3.5 %collective-permute-done.22.refs_2_ = bf16[384,256]{1,0:T(8,128)(2,1)S(1)} collective-permute-done((bf16[384,256]{1,0:T(8,128)(2,1)S(1)}, bf16[384,256]{1,0:T(8,128)(2,1)S(1)}, u32[]{:S(2)}, u32[]{:S(2)}) %collective-permute-start.22) | collective-permute-done | bytes 196640 | tf_op jit(solution)/shard_map/ppermute | solution.py:713
  99.4 0.8 shard_map.157
  (51 shorter events, 0.2 us)
Async XLA Ops:
  0.0 14.8 %copy-start = (bf16[4,128,2048]{2,1,0:T(8,128)(2,1)S(1)}, bf16[4,128,2048]{2,1,0:T(8,128)(2,1)}, u32[]{:S(2)}) copy-start(bf16[4,128,2048]{2,1,0:T(8,128)(2,1)} %param.29) | copy-start | bytes 6291460
  2.3 8.0 %collective-permute-start = (bf16[512,256]{1,0:T(8,128)(2,1)S(1)}, bf16[512,256]{1,0:T(8,128)(2,1)S(1)}, u32[]{:S(2)}, u32[]{:S(2)}) collective-permute-start(bf16[512,256]{1,0:T(8,128)(2,1)S(1)} %get-tuple-element.36.own_ref), channel_id=1, source_target_pairs={{0,1},{1,0},{2,3},{3,2},{4,5},{5,4},{6,7},{7,6},{8,9},{9,8},{10,11... | collective-permute-start | bytes 786440 | tf_op jit(solution)/shard_map/ppermute | solution.py:590
  3.9 12.2 %collective-permute-start.1 = (bf16[272,512]{1,0:T(8,128)(2,1)S(1)}, bf16[272,512]{1,0:T(8,128)(2,1)S(1)}, u32[]{:S(2)}, u32[]{:S(2)}) collective-permute-start(bf16[272,512]{1,0:T(8,128)(2,1)S(1)} %get-tuple-element.40), channel_id=1, source_target_pairs={{0,1},{1,0},{2,3},{3,2},{4,5},{5,4},{6,7},{7,6},{8,9},{9,8},{10,11... | collective-permute-start | bytes 835592 | tf_op jit(solution)/shard_map/ppermute | solution.py:598
  4.0 12.1 %all-to-all-start = ((f32[8,1,1280]{2,1,0:T(1,128)}), f32[8,1,1280]{2,1,0:T(1,128)S(1)}, u32[]{:S(2)}, u32[]{:S(2)}) async-start(f32[8,1,1280]{2,1,0:T(1,128)} %get-tuple-element.37), calls=%async_computation | async-start | bytes 81920 | tf_op jit(solution)/shard_map/all_to_all | solution.py:592
  11.3 4.8 %collective-permute-start.2 = (f32[8,512]{1,0:T(8,128)S(1)}, f32[8,512]{1,0:T(8,128)S(1)}, u32[]{:S(2)}, u32[]{:S(2)}) collective-permute-start(f32[8,512]{1,0:T(8,128)S(1)} %shard_map.148.sq_ref), channel_id=1, source_target_pairs={{0,2},{1,3},{2,0},{3,1},{4,6},{5,7},{6,4},{7,5},{8,10},{9,11},{10,... | collective-permute-start | bytes 49160 | tf_op jit(solution)/shard_map/ppermute | solution.py:575
  12.8 3.7 %collective-permute-start.3 = (f32[8,512]{1,0:T(8,128)S(1)}, f32[8,512]{1,0:T(8,128)S(1)}, u32[]{:S(2)}, u32[]{:S(2)}) collective-permute-start(f32[8,512]{1,0:T(8,128)S(1)} %shard_map.148.sq_ref), channel_id=1, source_target_pairs={{0,4},{1,5},{2,6},{3,7},{4,0},{5,1},{6,2},{7,3},{8,12},{9,13},{10,... | collective-permute-start | bytes 49160 | tf_op jit(solution)/shard_map/ppermute | solution.py:575
  14.3 4.7 %collective-permute-start.4 = (f32[8,512]{1,0:T(8,128)S(1)}, f32[8,512]{1,0:T(8,128)}, u32[]{:S(2)}, u32[]{:S(2)}) collective-permute-start(f32[8,512]{1,0:T(8,128)S(1)} %shard_map.148.sq_ref), channel_id=1, source_target_pairs={{0,6},{1,7},{2,4},{3,5},{4,2},{5,3},{6,0},{7,1},{8,14},{9,15},{10,... | collective-permute-start | bytes 49160 | tf_op jit(solution)/shard_map/ppermute | solution.py:575
  14.9 1.0 copy-start.8
  16.1 16.9 %collective-permute-start.5 = (bf16[4,512,256]{2,1,0:T(8,128)(2,1)}, bf16[4,512,256]{2,1,0:T(8,128)(2,1)}, u32[]{:S(2)}, u32[]{:S(2)}) collective-permute-start(bf16[4,512,256]{2,1,0:T(8,128)(2,1)} %copy-done.8), channel_id=1, source_target_pairs={{0,1},{1,0},{2,3},{3,2},{4,5},{5,4},{6,7},{7,6},{8,9},{9,8},{10,11... | collective-permute-start | bytes 3145736 | tf_op jit(solution)/shard_map/ppermute | solution.py:602
  20.6 0.9 copy-start.4
  21.5 18.2 %all-to-all-start.1 = ((f32[8,240,128]{2,1,0:T(8,128)}), f32[8,240,128]{2,1,0:T(8,128)S(1)}, u32[]{:S(2)}, u32[]{:S(2)}) async-start(f32[8,240,128]{2,1,0:T(8,128)} %copy-done.4), calls=%async_computation.1 | async-start | bytes 1966080 | tf_op jit(solution)/shard_map/all_to_all | solution.py:618
  26.0 2.5 %copy-start.15 = (f32[384,32]{1,0:T(8,128)S(1)}, f32[384,32]{1,0:T(8,128)}, u32[]{:S(2)}) copy-start(f32[384,32]{1,0:T(8,128)} %copy.18) | copy-start | bytes 147460
  29.1 1.8 %copy-start.14 = (f32[384,32]{1,0:T(8,128)}, f32[384,32]{1,0:T(8,128)S(1)}, u32[]{:S(2)}) copy-start(f32[384,32]{1,0:T(8,128)S(1)} %get-tuple-element.72) | copy-start | bytes 147460
  30.0 9.7 %copy-start.6 = (f32[512]{0:T(512)S(1)}, f32[512]{0:T(512)}, u32[]{:S(2)}) copy-start(f32[512]{0:T(512)} %param.24) | copy-start | bytes 6148
  30.0 9.7 %copy-start.7 = (f32[512]{0:T(512)S(1)}, f32[512]{0:T(512)}, u32[]{:S(2)}) copy-start(f32[512]{0:T(512)} %param.25) | copy-start | bytes 6148
  40.7 30.6 %copy-start.16 = (f32[4]{0:T(128)S(1)}, f32[4]{0:T(128)}, u32[]{:S(2)}) copy-start(f32[4]{0:T(128)} %param.28) | copy-start | bytes 52
  40.7 30.7 %copy-start.9 = (bf16[512,4,192]{0,2,1:T(8,128)(2,1)S(1)}, bf16[512,4,192]{0,2,1:T(8,128)(2,1)}, u32[]{:S(2)}) copy-start(bf16[512,4,192]{0,2,1:T(8,128)(2,1)} %param.26) | copy-start | bytes 2359300
  40.7 13.7 %all-to-all-start.2 = ((bf16[4,72,512]{2,1,0:T(8,128)(2,1)}), bf16[4,72,512]{2,1,0:T(8,128)(2,1)S(1)}, u32[]{:S(2)}, u32[]{:S(2)}) async-start(bf16[4,72,512]{2,1,0:T(8,128)(2,1)} %get-tuple-element.51), calls=%async_computation.2 | async-start | bytes 589824 | tf_op jit(solution)/shard_map/all_to_all | solution.py:641
  45.9 6.0 %collective-permute-start.6 = (bf16[120,512]{1,0:T(8,128)(2,1)S(1)}, bf16[120,512]{1,0:T(8,128)(2,1)S(1)}, u32[]{:S(2)}, u32[]{:S(2)}) collective-permute-start(bf16[120,512]{1,0:T(8,128)(2,1)S(1)} %get-tuple-element.52.refs_0_), channel_id=1, source_target_pairs={{0,2},{1,3},{2,0},{3,1},{4,6},{5,7},{6,4},{7,5},{8,10},{9,11},{10,... | collective-permute-start | bytes 368648 | tf_op jit(solution)/shard_map/ppermute | solution.py:575
  46.4 7.4 %collective-permute-start.7 = (bf16[120,512]{1,0:T(8,128)(2,1)S(1)}, bf16[120,512]{1,0:T(8,128)(2,1)S(1)}, u32[]{:S(2)}, u32[]{:S(2)}) collective-permute-start(bf16[120,512]{1,0:T(8,128)(2,1)S(1)} %get-tuple-element.52.refs_0_), channel_id=1, source_target_pairs={{0,4},{1,5},{2,6},{3,7},{4,0},{5,1},{6,2},{7,3},{8,12},{9,13},{10,... | collective-permute-start | bytes 368648 | tf_op jit(solution)/shard_map/ppermute | solution.py:575
  47.1 7.4 %collective-permute-start.8 = (bf16[120,512]{1,0:T(8,128)(2,1)S(1)}, bf16[120,512]{1,0:T(8,128)(2,1)}, u32[]{:S(2)}, u32[]{:S(2)}) collective-permute-start(bf16[120,512]{1,0:T(8,128)(2,1)S(1)} %get-tuple-element.52.refs_0_), channel_id=1, source_target_pairs={{0,6},{1,7},{2,4},{3,5},{4,2},{5,3},{6,0},{7,1},{8,14},{9,15},{10,... | collective-permute-start | bytes 368648 | tf_op jit(solution)/shard_map/ppermute | solution.py:575
  51.9 1.9 %copy-start.10 = (bf16[120,512]{1,0:T(8,128)(2,1)}, bf16[120,512]{1,0:T(8,128)(2,1)S(1)}, u32[]{:S(2)}) copy-start(bf16[120,512]{1,0:T(8,128)(2,1)S(1)} %collective-permute-done.6.refs_1_) | copy-start | bytes 368644
  53.8 0.7 copy-start.12
  54.5 16.9 %copy-start.11 = (bf16[120,512]{1,0:T(8,128)(2,1)S(1)}, bf16[120,512]{1,0:T(8,128)(2,1)}, u32[]{:S(2)}) copy-start(bf16[120,512]{1,0:T(8,128)(2,1)} %copy-done.10) | copy-start | bytes 368644
  54.5 16.9 %copy-start.13 = (bf16[120,512]{1,0:T(8,128)(2,1)S(1)}, bf16[120,512]{1,0:T(8,128)(2,1)}, u32[]{:S(2)}) copy-start(bf16[120,512]{1,0:T(8,128)(2,1)} %copy-done.12) | copy-start | bytes 368644
  54.5 4.2 %collective-permute-start.9 = (bf16[120,512]{1,0:T(8,128)(2,1)S(1)}, bf16[120,512]{1,0:T(8,128)(2,1)S(1)}, u32[]{:S(2)}, u32[]{:S(2)}) collective-permute-start(bf16[120,512]{1,0:T(8,128)(2,1)S(1)} %get-tuple-element.52.refs_0_), channel_id=1, source_target_pairs={{0,1},{1,0},{2,3},{3,2},{4,5},{5,4},{6,7},{7,6},{8,9},{9,8},{10,11... | collective-permute-start | bytes 368648 | tf_op jit(solution)/shard_map/ppermute | solution.py:644
  54.6 4.1 %collective-permute-start.10 = (bf16[120,512]{1,0:T(8,128)(2,1)}, bf16[120,512]{1,0:T(8,128)(2,1)S(1)}, u32[]{:S(2)}, u32[]{:S(2)}) collective-permute-start(bf16[120,512]{1,0:T(8,128)(2,1)} %copy-done.10), channel_id=1, source_target_pairs={{0,1},{1,0},{2,3},{3,2},{4,5},{5,4},{6,7},{7,6},{8,9},{9,8},{10,11... | collective-permute-start | bytes 368648 | tf_op jit(solution)/shard_map/ppermute | solution.py:644
  55.1 8.4 %collective-permute-start.14 = (bf16[216,512]{1,0:T(8,128)(2,1)S(1)}, bf16[216,512]{1,0:T(8,128)(2,1)S(1)}, u32[]{:S(2)}, u32[]{:S(2)}) collective-permute-start(bf16[216,512]{1,0:T(8,128)(2,1)S(1)} %shard_map.151.refs_8_), channel_id=1, source_target_pairs={{0,2},{1,3},{2,0},{3,1},{4,6},{5,7},{6,4},{7,5},{8,10},{9,11},{10,... | collective-permute-start | bytes 663560 | tf_op jit(solution)/shard_map/ppermute | solution.py:575
  56.9 11.9 %collective-permute-start.15 = (bf16[216,512]{1,0:T(8,128)(2,1)S(1)}, bf16[216,512]{1,0:T(8,128)(2,1)S(1)}, u32[]{:S(2)}, u32[]{:S(2)}) collective-permute-start(bf16[216,512]{1,0:T(8,128)(2,1)S(1)} %shard_map.151.refs_8_), channel_id=1, source_target_pairs={{0,4},{1,5},{2,6},{3,7},{4,0},{5,1},{6,2},{7,3},{8,12},{9,13},{10,... | collective-permute-start | bytes 663560 | tf_op jit(solution)/shard_map/ppermute | solution.py:575
  57.3 11.5 %collective-permute-start.16 = (bf16[216,512]{1,0:T(8,128)(2,1)S(1)}, bf16[216,512]{1,0:T(8,128)(2,1)S(1)}, u32[]{:S(2)}, u32[]{:S(2)}) collective-permute-start(bf16[216,512]{1,0:T(8,128)(2,1)S(1)} %shard_map.151.refs_8_), channel_id=1, source_target_pairs={{0,6},{1,7},{2,4},{3,5},{4,2},{5,3},{6,0},{7,1},{8,14},{9,15},{10,... | collective-permute-start | bytes 663560 | tf_op jit(solution)/shard_map/ppermute | solution.py:575
  58.6 1.5 %collective-permute-start.11 = (bf16[120,512]{1,0:T(8,128)(2,1)}, bf16[120,512]{1,0:T(8,128)(2,1)S(1)}, u32[]{:S(2)}, u32[]{:S(2)}) collective-permute-start(bf16[120,512]{1,0:T(8,128)(2,1)} %copy-done.12), channel_id=1, source_target_pairs={{0,1},{1,0},{2,3},{3,2},{4,5},{5,4},{6,7},{7,6},{8,9},{9,8},{10,11... | collective-permute-start | bytes 368648 | tf_op jit(solution)/shard_map/ppermute | solution.py:644
  58.6 12.7 %collective-permute-start.13 = (bf16[216,512]{1,0:T(8,128)(2,1)S(1)}, bf16[216,512]{1,0:T(8,128)(2,1)S(1)}, u32[]{:S(2)}, u32[]{:S(2)}) collective-permute-start(bf16[216,512]{1,0:T(8,128)(2,1)S(1)} %shard_map.151.refs_8_), channel_id=1, source_target_pairs={{0,1},{1,0},{2,3},{3,2},{4,5},{5,4},{6,7},{7,6},{8,9},{9,8},{10,11... | collective-permute-start | bytes 663560 | tf_op jit(solution)/shard_map/ppermute | solution.py:647
  60.2 11.1 %collective-permute-start.12 = (bf16[120,512]{1,0:T(8,128)(2,1)}, bf16[120,512]{1,0:T(8,128)(2,1)S(1)}, u32[]{:S(2)}, u32[]{:S(2)}) collective-permute-start(bf16[120,512]{1,0:T(8,128)(2,1)} %collective-permute-done.8.refs_3_), channel_id=1, source_target_pairs={{0,1},{1,0},{2,3},{3,2},{4,5},{5,4},{6,7},{7,6},{8,9},{9,8},{10,11... | collective-permute-start | bytes 368648 | tf_op jit(solution)/shard_map/ppermute | solution.py:644
  63.4 15.5 %collective-permute-start.17 = (bf16[216,512]{1,0:T(8,128)(2,1)S(1)}, bf16[216,512]{1,0:T(8,128)(2,1)S(1)}, u32[]{:S(2)}, u32[]{:S(2)}) collective-permute-start(bf16[216,512]{1,0:T(8,128)(2,1)S(1)} %collective-permute-done.14.refs_0_), channel_id=1, source_target_pairs={{0,1},{1,0},{2,3},{3,2},{4,5},{5,4},{6,7},{7,6},{8,9},{9,8},{10,11... | collective-permute-start | bytes 663560 | tf_op jit(solution)/shard_map/ppermute | solution.py:647
  68.7 10.2 %collective-permute-start.18 = (bf16[216,512]{1,0:T(8,128)(2,1)S(1)}, bf16[216,512]{1,0:T(8,128)(2,1)S(1)}, u32[]{:S(2)}, u32[]{:S(2)}) collective-permute-start(bf16[216,512]{1,0:T(8,128)(2,1)S(1)} %collective-permute-done.15.refs_1_), channel_id=1, source_target_pairs={{0,1},{1,0},{2,3},{3,2},{4,5},{5,4},{6,7},{7,6},{8,9},{9,8},{10,11... | collective-permute-start | bytes 663560 | tf_op jit(solution)/shard_map/ppermute | solution.py:647
  68.8 10.2 %collective-permute-start.19 = (bf16[216,512]{1,0:T(8,128)(2,1)S(1)}, bf16[216,512]{1,0:T(8,128)(2,1)S(1)}, u32[]{:S(2)}, u32[]{:S(2)}) collective-permute-start(bf16[216,512]{1,0:T(8,128)(2,1)S(1)} %collective-permute-done.16.refs_2_), channel_id=1, source_target_pairs={{0,1},{1,0},{2,3},{3,2},{4,5},{5,4},{6,7},{7,6},{8,9},{9,8},{10,11... | collective-permute-start | bytes 663560 | tf_op jit(solution)/shard_map/ppermute | solution.py:647
  69.3 1.2 %copy-start.1 = (bf16[64,8,4,256]{3,1,2,0:T(8,128)(2,1)S(1)}, bf16[64,8,4,256]{3,1,2,0:T(8,128)(2,1)}, u32[]{:S(2)}) copy-start(bf16[64,8,4,256]{3,1,2,0:T(8,128)(2,1)} %copy.22) | copy-start | bytes 3145732
  71.4 1.2 %copy-start.2 = (bf16[64,8,4,256]{3,1,2,0:T(8,128)(2,1)S(1)}, bf16[64,8,4,256]{3,1,2,0:T(8,128)(2,1)}, u32[]{:S(2)}) copy-start(bf16[64,8,4,256]{3,1,2,0:T(8,128)(2,1)} %copy.22) | copy-start | bytes 3145732
  72.6 6.3 %copy-start.3 = (bf16[64,8,4,256]{3,1,2,0:T(8,128)(2,1)S(1)}, bf16[64,8,4,256]{3,1,2,0:T(8,128)(2,1)}, u32[]{:S(2)}) copy-start(bf16[64,8,4,256]{3,1,2,0:T(8,128)(2,1)} %copy.22) | copy-start | bytes 3145732
  84.5 1.8 %collective-permute-start.20 = (bf16[384,512]{1,0:T(8,128)(2,1)S(1)}, bf16[384,512]{1,0:T(8,128)(2,1)S(1)}, u32[]{:S(2)}, u32[]{:S(2)}) collective-permute-start(bf16[384,512]{1,0:T(8,128)(2,1)S(1)} %shard_map.154.heads_ref), channel_id=1, source_target_pairs={{0,1},{1,0},{2,3},{3,2},{4,5},{5,4},{6,7},{7,6},{8,9},{9,8},{10,11... | collective-permute-start | bytes 1179656 | tf_op jit(solution)/shard_map/ppermute | solution.py:698
  85.1 14.2 %copy-start.5 = (bf16[384,256]{1,0:T(8,128)(2,1)S(1)}, bf16[384,256]{1,0:T(8,128)(2,1)}, u32[]{:S(2)}) copy-start(bf16[384,256]{1,0:T(8,128)(2,1)} %latent_ref.1) | copy-start | bytes 589828
  88.1 7.8 %collective-permute-start.21 = (bf16[384,256]{1,0:T(8,128)(2,1)S(1)}, bf16[384,256]{1,0:T(8,128)(2,1)S(1)}, u32[]{:S(2)}, u32[]{:S(2)}) collective-permute-start(bf16[384,256]{1,0:T(8,128)(2,1)S(1)} %get-tuple-element.64), channel_id=1, source_target_pairs={{0,2},{1,3},{2,0},{3,1},{4,6},{5,7},{6,4},{7,5},{8,10},{9,11},{10,... | collective-permute-start | bytes 589832 | tf_op jit(solution)/shard_map/ppermute | solution.py:713
  88.5 10.9 %collective-permute-start.22 = (bf16[384,256]{1,0:T(8,128)(2,1)S(1)}, bf16[384,256]{1,0:T(8,128)(2,1)S(1)}, u32[]{:S(2)}, u32[]{:S(2)}) collective-permute-start(bf16[384,256]{1,0:T(8,128)(2,1)S(1)} %get-tuple-element.65), channel_id=1, source_target_pairs={{0,4},{1,5},{2,6},{3,7},{4,0},{5,1},{6,2},{7,3},{8,12},{9,13},{10,... | collective-permute-start | bytes 589832 | tf_op jit(solution)/shard_map/ppermute | solution.py:713
  89.5 9.9 %collective-permute-start.23 = (bf16[384,256]{1,0:T(8,128)(2,1)S(1)}, bf16[384,256]{1,0:T(8,128)(2,1)S(1)}, u32[]{:S(2)}, u32[]{:S(2)}) collective-permute-start(bf16[384,256]{1,0:T(8,128)(2,1)S(1)} %get-tuple-element.66), channel_id=1, source_target_pairs={{0,6},{1,7},{2,4},{3,5},{4,2},{5,3},{6,0},{7,1},{8,14},{9,15},{10,... | collective-permute-start | bytes 589832 | tf_op jit(solution)/shard_map/ppermute | solution.py:713

commit v4 on v3

--- a/solution.py
+++ b/solution.py
@@ -2,6 +2,7 @@
 
 import jax
 import jax.numpy as jnp
+import numpy as np
 from jax import lax
 from jax.experimental import pallas as pl
 from jax.experimental.pallas import tpu as pltpu
@@ -193,7 +194,7 @@
     return (lat_f + modulation[0, 2] * branch).astype(jnp.bfloat16)
 
 
-def call(kernel, outs, *args, flops=1e6, scratch=(), limit=8, held=pltpu.VMEM, kept=True):
+def call(kernel, outs, *args, flops=1e6, scratch=(), limit=8, held=pltpu.VMEM, kept=True, remote=()):
     single = not isinstance(outs, tuple)
     vmem = pl.BlockSpec(memory_space=pltpu.VMEM)
     outs = (outs,) if single else outs
@@ -203,7 +204,7 @@
         args = tuple(pltpu.with_memory_space_constraint(a, held) for a in args)
     result = pl.pallas_call(
         kernel,
-        in_specs=[vmem] * len(args),
+        in_specs=[vmem] * len(args) + [pl.BlockSpec(memory_space=pltpu.HBM)] * len(remote),
         out_specs=(vmem,) * len(outs),
         out_shape=outs,
         scratch_shapes=scratch,
@@ -211,7 +212,7 @@
             flops=int(flops), bytes_accessed=int(1e5), transcendentals=0
         ),
         compiler_params=pltpu.CompilerParams(vmem_limit_bytes=limit << 20),
-    )(*args)
+    )(*args, *remote)
     return result[0] if single else result
 
 
@@ -226,7 +227,25 @@
     )
 
 
-def share_kernel(wq_ref, wkv_ref, wr_ref, own_ref, other_ref):
+def stats_kernel(
+    lat_ref,
+    ctx_ref,
+    cond_ref,
+    cond_ctx_ref,
+    w_ref,
+    g_ref,
+    wq_ref,
+    wkv_ref,
+    wr_ref,
+    out_ref,
+    rows_ref,
+    own_ref,
+    other_ref,
+    *,
+    sp,
+):
+    rows_ref[: lat_ref.shape[0]] = lat_ref[...]
+    rows_ref[lat_ref.shape[0] :] = ctx_ref[...]
     features, rank = wq_ref.shape
     half, width = rank // 2, ROPE // 2
     side = place()[2]
@@ -234,16 +253,10 @@
         start = pl.multiple_of(which * half, half)
         ref[:features, :half] = wq_ref[:, pl.ds(start, half)]
         ref[:features, half:] = wkv_ref[:, pl.ds(start, half)]
-        low = pl.multiple_of(which * width, width)
-        rot = wr_ref[pl.ds(low, width), :]
+        rot = wr_ref[pl.ds(pl.multiple_of(which * width, width), width), :]
         count = width * features // rank
         for i in range(rank // features):
             ref[features:, i * features : (i + 1) * features] = rot[i * count : (i + 1) * count]
-
-
-def stats_kernel(lat_ref, ctx_ref, cond_ref, cond_ctx_ref, w_ref, g_ref, out_ref, rows_ref, *, sp):
-    rows_ref[: lat_ref.shape[0]] = lat_ref[...]
-    rows_ref[lat_ref.shape[0] :] = ctx_ref[...]
     inner = cond_ref.shape[0]
     lat_c = jax.nn.silu(cond_ref[...].astype(jnp.float32).reshape(1, inner))
     ctx_c = jax.nn.silu(cond_ctx_ref[...].astype(jnp.float32).reshape(1, inner))
@@ -270,16 +283,18 @@
 
 
 def project_kernel(
-    own_ref, other_ref, mod_ref, w_own_ref, w_other_ref, sq_ref, *refs, sp, tp, rows
+    own_ref, other_ref, mod_ref, w_own_ref, w_other_ref, *refs, sp, tp, rows
 ):
-    out_ref, gate_ref = refs[-2:]
+    chips = tp // 2
+    squares, out_refs = refs[:chips], refs[chips : 2 * chips]
+    gate_ref, lat_ref, ctx_ref, lat_rot_ref, ctx_rot_ref = refs[2 * chips :]
     count, features = own_ref.shape
     ctx_rows = count - rows
     rank = w_own_ref.shape[1]
     half = rank // 2
-    side = place()[2]
-    total = sq_ref[...]
-    for ref in refs[:-2]:
+    unused, here, side, unused = place()
+    total = squares[0][...]
+    for ref in squares[1:]:
         total = total + ref[...]
     total = jnp.transpose(total)[:, :1]
     mine, partner = mod_ref[side], mod_ref[1 - side]
@@ -314,33 +329,57 @@
         return first, second, rot
 
     lat_q, lat_kv, lat_rot = rows_of(slice(0, rows), 0)
-    _, ctx_kv, ctx_rot = rows_of(slice(rows, count), 1)
+    lat_ref[:, :half], lat_ref[:, half:], lat_rot_ref[...] = lat_q, lat_kv, lat_rot
+    unused, ctx_ref[...], ctx_rot_ref[...] = rows_of(slice(rows, count), 1)
     lat, ctx = rows // tp, ctx_rows // tp
     quarter = (lat + ctx) // 4
-    for d in range(tp):
-        at = 0
-        for source, size in ((lat_q, lat), (lat_kv, lat), (ctx_kv, ctx)):
-            for slab in range(half // 128):
-                out_ref[d, at : at + size, :] = source[
-                    d * size : (d + 1) * size, slab * 128 : (slab + 1) * 128
-                ]
-                at += size
-        rot = jnp.concatenate(
-            [lat_rot[d * lat : (d + 1) * lat], ctx_rot[d * ctx : (d + 1) * ctx]], axis=0
-        )
-        out_ref[d, at : at + quarter, :] = jnp.concatenate(
-            [rot[i * quarter : (i + 1) * quarter] for i in range(4)], axis=1
-        )
-
-
-def norm_kernel(part_ref, gq_ref, gkv_ref, tab_ref, kv_ref, near_ref, *, lat, ctx):
-    chips = part_ref.shape[0] // 2
-    halves = []
-    for core in range(2):
-        acc = part_ref[core]
-        for chip in range(1, chips):
-            acc = acc + part_ref[2 * chip + core]
-        halves.append(acc)
+    for hop in range(chips):
+        for core in range(2):
+            d = 2 * (here ^ hop) + core
+            lats, ctxs = pl.ds(pl.multiple_of(d * lat, 8), lat), pl.ds(pl.multiple_of(d * ctx, 8), ctx)
+            at = 0
+            for source, part, size in ((lat_ref, lats, lat), (ctx_ref, ctxs, ctx)):
+                for slab in range(source.shape[1] // 128):
+                    out_refs[hop][core, at : at + size, :] = source[
+                        part, slab * 128 : (slab + 1) * 128
+                    ]
+                    at += size
+            rot = jnp.concatenate([lat_rot_ref[lats], ctx_rot_ref[ctxs]], axis=0)
+            out_refs[hop][core, at : at + quarter, :] = jnp.concatenate(
+                [rot[i * quarter : (i + 1) * quarter] for i in range(4)], axis=1
+            )
+
+
+def reduce_kernel(*refs):
+    own_ref, other_ref = refs[-2:]
+    side = place()[2]
+    for which, ref in ((side, own_ref), (1 - side, other_ref)):
+        total = refs[0][which]
+        for part in refs[1:-2]:
+            total = total + part[which]
+        ref[...] = total
+
+
+def prepare_kernel(inverse_ref, w_ref, tab_ref, out_ref):
+    rows, lanes = tab_ref.shape
+    position = lax.broadcasted_iota(jnp.int32, (rows, lanes), 0) + lax.axis_index("sp") * rows
+    lane = lax.broadcasted_iota(jnp.int32, (rows, lanes), 1)
+    along = jnp.where(lane % ROPE < ROPE // 2, position // GRID_W, position % GRID_W)
+    angle = along.astype(jnp.float32) * inverse_ref[...]
+    sine = jnp.sin(angle)
+    sine = jnp.where(lane % (ROPE // 2) < ROPE // 4, -sine, sine)
+    tab_ref[...] = jnp.where(lane < ROPE, jnp.cos(angle), sine)
+    width = w_ref.shape[2]
+    for head in range(w_ref.shape[1]):
+        out_ref[:, head * width : (head + 1) * width] = w_ref[:, head, :]
+
+
+def norm_kernel(own_ref, other_ref, gq_ref, gkv_ref, tab_ref, kv_ref, near_ref, *, lat, ctx):
+    unused, unused, side, me = place()
+    first = side == 0
+    own, other = own_ref[...], other_ref[...]
+    tab = tab_ref[pl.ds(pl.multiple_of(me * lat, 8), lat), :]
+    halves = [jnp.where(first, own, other), jnp.where(first, other, own)]
     rank = gq_ref.shape[1]
     slabs = rank // 256
 
@@ -373,7 +412,9 @@
         )
         turned = rot[:lat]
         swapped = jnp.concatenate([turned[:, width // 2 :], turned[:, : width // 2]], axis=1)
-        lat_rot.append(turned * tab_ref[0, core] + swapped * tab_ref[1, core])
+        cosine = tab[:, core * width : (core + 1) * width]
+        sine = tab[:, ROPE + core * width : ROPE + (core + 1) * width]
+        lat_rot.append(turned * cosine + swapped * sine)
         ctx_rot.append(rot[lat:])
     keys = jnp.concatenate(
         [jnp.concatenate(lat_rot, axis=1), jnp.concatenate(ctx_rot, axis=1)], axis=0
@@ -384,17 +425,16 @@
         [keys[i * low : (i + 1) * low] for i in range(pieces)], axis=1
     ).astype(jnp.bfloat16)
     compressed = jnp.concatenate([lat_kv, ctx_kv], axis=0)
-    for ref in [kv_ref.at[copy] for copy in range(kv_ref.shape[0])] + [near_ref]:
+    for ref in (kv_ref, near_ref):
         ref[: lat + ctx] = compressed
         ref[lat + ctx : lat + ctx + low] = keys
     near_ref[lat + ctx + low :] = cq
 
 
-def gather_kernel(kv_ref, out_ref):
-    planes, size = kv_ref.shape[:2]
-    here = lax.axis_index("sp")
-    for i in range(planes - 1):
-        out_ref[i * size : (i + 1) * size] = kv_ref[lax.rem(here + 1 + i, planes)]
+def gather_kernel(*refs):
+    size = refs[0].shape[0]
+    for i, ref in enumerate(refs[:-1]):
+        refs[-1][i * size : (i + 1) * size] = ref[...]
 
 
 def unpack(chunks, kv_ref, key_ref, lat, ctx):
@@ -417,13 +457,20 @@
     return jnp.dot(kv_ref[...], weight, preferred_element_type=jnp.float32).astype(jnp.bfloat16)
 
 
-def weighted(query, keys, values):
-    score = dot_t(query, keys)
+def weighted(score, values):
     peak = jnp.max(score, axis=1, keepdims=True)
     probs = jnp.exp2((score - peak) * ((NOPE + ROPE) ** -0.5 * LOG2E))
     total = jnp.sum(probs, axis=1, keepdims=True)
     summed = jnp.dot(probs.astype(jnp.bfloat16), values, preferred_element_type=jnp.float32)
     return peak, total, summed
+
+
+def staged(steps):
+    score = steps[0][0]()
+    for i, (unused, finish) in enumerate(steps):
+        after = steps[i + 1][0]() if i + 1 < len(steps) else None
+        finish(score)
+        score = after
 
 
 def near_kernel(tab_ref, lift_ref, wq_ref, wkv_ref, *refs, lat, ctx, chips):
@@ -439,12 +486,11 @@
     chunks = [(ref, 0) for ref in own_refs + other_refs]
     chunks += chunks_of(refs[2 * chips : -6], size - lat)
     unpack(chunks, kv_ref, key_ref, lat, ctx)
-    stats = jnp.zeros(stat_ref.shape, jnp.float32)
-    spot = lax.broadcasted_iota(jnp.int32, stat_ref.shape, 1)
     heads = wq_ref.shape[0]
     quarter = ROPE // 4
     lane = lax.broadcasted_iota(jnp.int32, (1, 2 * ROPE), 1)
-    for head in range(wq_ref.shape[0]):
+
+    def prepare(head):
         pieces = [wq_ref[head]]
         for block in (1, 0, 3, 2):
             pieces.append(wq_ref[head, NOPE + block * quarter : NOPE + (block + 1) * quarter])
@@ -460,12 +506,25 @@
         turned = jnp.where(lane < ROPE, turned, lifts)
         query = jnp.concatenate([raw[:, :NOPE], turned], axis=1).astype(jnp.bfloat16)
         query_ref[head] = query
-        pairs = expanded(kv_ref, wkv_ref, head)
-        keys = jnp.concatenate([pairs[:, :NOPE], key_ref[...]], axis=1)
-        peak, total, summed = weighted(query, keys, pairs[:, NOPE:])
-        stats = jnp.where(spot == head, peak, jnp.where(spot == heads + head, total, stats))
-        sum_ref[head] = summed
-    stat_ref[...] = stats
+
+    stats = {}
+
+    def step(head):
+        def score():
+            prepare(head)
+            stats[head] = expanded(kv_ref, wkv_ref, head)
+            keys = jnp.concatenate([stats[head][:, :NOPE], key_ref[...]], axis=1)
+            return dot_t(query_ref[head], keys)
+
+        def finish(values):
+            peak, total, summed = weighted(values, stats[head][:, NOPE:])
+            stat_ref[:, head : head + 1] = peak
+            stat_ref[:, heads + head : heads + head + 1] = total
+            sum_ref[head] = summed
+
+        return score, finish
+
+    staged([step(head) for head in range(heads)])
 
 
 def chunks_of(refs, step):
@@ -484,23 +543,43 @@
 
 
 def far_kernel(query_ref, stat_ref, sum_ref, key_ref, value_ref, w_ref, *refs, lat, ctx):
-    out_ref, kv_ref, rot_ref = refs[-3:]
+    up_ref, out_ref, up_out_ref, kv_ref, rot_ref, done = refs[-6:]
+    copy = pltpu.make_async_copy(up_ref, up_out_ref, done)
+    copy.start()
     step = lat + ctx + (lat + ctx) * ROPE // w_ref.shape[0]
-    unpack(chunks_of(refs[:-3], step), kv_ref, rot_ref, lat, ctx)
+    unpack(chunks_of(refs[:-6], step), kv_ref, rot_ref, lat, ctx)
     heads = query_ref.shape[0]
     factor = (NOPE + ROPE) ** -0.5 * LOG2E
-    for head in range(query_ref.shape[0]):
-        pairs = expanded(kv_ref, w_ref, head)
-        keys = jnp.concatenate([pairs[:, :NOPE], rot_ref[...]], axis=1)
-        keys = jnp.concatenate([key_ref[head], keys], axis=0)
-        values = jnp.concatenate([value_ref[head], pairs[:, NOPE:]], axis=0)
-        peak, total, summed = weighted(query_ref[head], keys, values)
-        near = stat_ref[:, head : head + 1]
-        top = jnp.maximum(peak, near)
-        new, old = jnp.exp2((peak - top) * factor), jnp.exp2((near - top) * factor)
-        total = total * new + stat_ref[:, heads + head : heads + head + 1] * old
-        summed = summed * new + sum_ref[head] * old
-        out_ref[:, head * DV : (head + 1) * DV] = (summed / total).astype(jnp.bfloat16)
+    held = {}
+
+    def step_of(head):
+        def score():
+            pairs = expanded(kv_ref, w_ref, head)
+            keys = jnp.concatenate([pairs[:, :NOPE], rot_ref[...]], axis=1)
+            held[head] = (keys, pairs[:, NOPE:])
+            query = query_ref[head]
+            return dot_t(query, key_ref[head]), dot_t(query, held[head][0])
+
+        def finish(scores):
+            near = stat_ref[:, head : head + 1]
+            top = near
+            for values in scores:
+                top = jnp.maximum(top, jnp.max(values, axis=1, keepdims=True))
+            old = jnp.exp2((near - top) * factor)
+            total = stat_ref[:, heads + head : heads + head + 1] * old
+            summed = sum_ref[head] * old
+            for values, weights in zip(scores, (value_ref[head], held[head][1]), strict=True):
+                probs = jnp.exp2((values - top) * factor)
+                total = total + jnp.sum(probs, axis=1, keepdims=True)
+                summed = summed + jnp.dot(
+                    probs.astype(jnp.bfloat16), weights, preferred_element_type=jnp.float32
+                )
+            out_ref[:, head * DV : (head + 1) * DV] = (summed / total).astype(jnp.bfloat16)
+
+        return score, finish
+
+    staged([step_of(head) for head in range(heads)])
+    copy.wait()
 
 
 def share_out_kernel(w_ref, out_ref):
@@ -565,7 +644,6 @@
     lat, ctx = rows // tp, ctx_rows // tp
     half = rank // 2
     across = [(i, i ^ 1) for i in range(tp)]
-    me = lax.axis_index("tp")
 
     def array(shape, dtype=bf16):
         return jax.ShapeDtypeStruct(shape, dtype)
@@ -576,73 +654,99 @@
             for hop in range(1, chips)
         ]
 
-    modulation, tokens = call(
+    share = array((features + ROPE // 2 * features // rank, rank))
+    modulation, tokens, w_own, w_other = call(
         functools.partial(stats_kernel, sp=sp),
-        (array((2 * sp, 1, 5 * features), f32), array((rows + ctx_rows, features))),
+        (
+            array((2 * sp, 1, 5 * features), f32),
+            array((rows + ctx_rows, features)),
+            share,
+            share,
+        ),
         latent,
         context,
         cond,
         cond_ctx,
         jnp.transpose(w_mod, (1, 0, 2)),
         g_norm,
+        w_dq,
+        w_dkv,
+        w_kr.T,
         held=pltpu.HBM,
     )
+    w_other = lax.ppermute(w_other, "tp", across)
     tokens_other = lax.ppermute(tokens, "tp", across)
     columns = [[s * tp + 2 * c + k for s in range(sp) for k in range(2)] for c in range(chips)]
     modulation = lax.all_to_all(modulation, ("sp", "tp"), 0, 0, axis_index_groups=columns)
     squares = call(square_kernel, array((8, rows + ctx_rows), f32), tokens, tokens_other)
     squares = hopped(squares)
 
-    share = array((features + ROPE // 2 * features // rank, rank))
-    w_own, w_other = call(share_kernel, (share, share), w_dq, w_dkv, w_kr.T, held=pltpu.HBM)
-    w_other = lax.ppermute(w_other, "tp", across)
-    w_up = w_out.reshape(heads * DV, 2 * chips * features)
-    w_up_share = call(share_out_kernel, array((chips, heads * DV, features)), w_up, flops=1e9)
-    modulation, w_up_share = lax.optimization_barrier((modulation, w_up_share))
-    w_up_other = lax.ppermute(w_up_share, "tp", across)
-
     height = half // 128 * (2 * lat + ctx) + (lat + ctx) // 4
-    part, gate = call(
+    share = array((2, height, 128), f32)
+    *parts, gate = call(
         functools.partial(project_kernel, sp=sp, tp=tp, rows=rows),
-        (array((tp, height, 128), f32), array((1, features), f32)),
+        (share,) * chips + (array((1, features), f32),),
         tokens,
         tokens_other,
         modulation,
         w_own,
         w_other,
         *squares,
+        scratch=[
+            pltpu.VMEM((rows, rank), f32),
+            pltpu.VMEM((ctx_rows, half), f32),
+            pltpu.VMEM((rows, ROPE // 2), f32),
+            pltpu.VMEM((ctx_rows, ROPE // 2), f32),
+        ],
         flops=4 * (rows + ctx_rows) * features * (rank + 128),
         limit=16,
     )
-    part, w_kv, zero = lax.optimization_barrier((part, w_ukv, jnp.int32(0)))
-    part = lax.all_to_all(part, "tp", 0, 0)
-
-    positions = zero + lax.axis_index("sp") * rows + jnp.arange(rows, dtype=jnp.int32)
-    cosine, sine = tables(positions)
+    *parts, w_kv, w_up, zero = lax.optimization_barrier((*parts, w_ukv, w_out, jnp.float32(0)))
+    parts = [parts[0]] + [
+        lax.ppermute(part, "tp", [(i, i ^ (2 * hop + 2)) for i in range(tp)])
+        for hop, part in enumerate(parts[1:])
+    ]
+
     quarter = ROPE // 4
-    c0, c1, s0, s1 = cosine[:, :quarter], cosine[:, quarter:], sine[:, :quarter], sine[:, quarter:]
-    q_tab = jnp.concatenate([c0, c0, c1, c1, -s0, s0, -s1, s1], axis=1)
-    k_tab = lax.dynamic_slice_in_dim(q_tab, me * lat, lat, 0)
-    k_tab = k_tab.reshape(lat, 2, 2, ROPE // 2).transpose(1, 2, 0, 3)
-    w_kv = w_kv.reshape(rank, heads * (NOPE + DV))
-    part, q_tab, w_up_other, w_kv = lax.optimization_barrier((part, q_tab, w_up_other, w_kv))
+    inverse = THETA ** (-np.arange(quarter) / quarter)
+    inverse = jnp.asarray(np.tile(inverse, 128 // quarter)[None], f32) + zero
+    q_tab, w_kv = call(
+        prepare_kernel,
+        (array((rows, 128), f32), array((rank, heads * (NOPE + DV)))),
+        inverse,
+        w_kv,
+        flops=1e9,
+    )
+    w_up = w_up.reshape(heads * DV, 2 * chips * features)
+    w_up_other = call(
+        share_out_kernel, array((chips, heads * DV, features)), w_up, flops=1e9, kept=False
+    )
+    w_up_other = lax.ppermute(w_up_other, "tp", across)
+    *parts, q_tab, w_up_other, w_kv = lax.optimization_barrier((*parts, q_tab, w_up_other, w_kv))
+    share = array((height, 128), f32)
+    part, part_other = call(reduce_kernel, (share, share), *parts)
+    part_other = lax.ppermute(part_other, "tp", across)
 
     count = lat + ctx
     step = count + count * ROPE // rank
     kv, near = call(
         functools.partial(norm_kernel, lat=lat, ctx=ctx),
-        (array((sp, step, rank)), array((step + lat, rank))),
+        (array((step, rank)), array((step + lat, rank))),
         part,
+        part_other,
         g_cq[None],
         g_ckv[None],
-        k_tab,
-    )
-
-    kv = lax.all_to_all(kv, "sp", 0, 0)
+        q_tab,
+    )
+
+    planes = [
+        lax.ppermute(kv, "sp", [(i, (i + shift) % sp) for i in range(sp)])
+        for shift in range(1, sp)
+    ]
     near_own = hopped(near)
-    *near_own, kv = lax.optimization_barrier((*near_own, kv))
+    near_own, planes = lax.optimization_barrier((near_own, planes))
     near_other = [lax.ppermute(n, "tp", across) for n in near_own]
-    far = call(gather_kernel, array(((sp - 1) * step, rank)), kv)
+    far = call(gather_kernel, array(((sp - 1) * step, rank)), *planes)
     far_own = hopped(far)
     far_other = [lax.ppermute(f, "tp", across) for f in far_own]
 
@@ -680,9 +784,9 @@
         scratch=scratch,
         flops=2 * keys * rank * 256 * heads,
     )
-    heads_out = call(
+    heads_out, w_up_other = call(
         functools.partial(far_kernel, lat=lat, ctx=ctx),
-        array((rows, heads * DV)),
+        (array((rows, heads * DV)), array(w_up_other.shape)),
         query,
         stats,
         summed,
@@ -690,7 +794,8 @@
         far_values,
         w_kv,
         *far_other[1:],
-        scratch=scratch,
+        remote=(w_up_other,),
+        scratch=scratch + [pltpu.SemaphoreType.DMA],
         flops=2 * heads * keys * (2 * rows * 384 + rank * 256),
         limit=28,
     )

time: 101 us -> 88.3 us (0.87)
  local copies, waits for them, and re-layouts: 11.9 us -> 0.12 us
  waiting for transfers between devices: 32.5 us -> 36.4 us
  Pallas kernels: 22.8 us -> 19.9 us
  other arithmetic: 1.08 us -> 0.01 us
    ppermute x1 -> x8, waiting for transfers between devices: 0.01 us -> 14.8 us  [the longest x3 8.49 us: split_device(): lax.ppermute(part, 'tp', [(i, i ^ 2 * hop + 2) for i in range(tp)])]
    all_to_all x2 -> x0, starting transfers between devices: 8.78 us -> none  [the longest x1 5.22 us: split_device(): kv = lax.all_to_all(kv, 'sp', 0, 0)]
    ppermute x1 -> x8, starting transfers between devices: 0.01 us -> 8.68 us  [the longest x3 4.98 us: split_device(): lax.ppermute(kv, 'sp', [(i, (i + shift) % sp) for i in range(sp)])]
    unnamed x35 -> x16, local copies, waits for them, and re-layouts: 7.52 us -> 0.05 us
    all_to_all x2 -> x0, waiting for transfers between devices: 6.71 us -> none  [the longest x1 6.71 us: split_device(): part = lax.all_to_all(part, 'tp', 0, 0)]
    ppermute x9, waiting for transfers between devices: 15.7 us -> 10 us  [hopped(): lax.ppermute(value, 'tp', [(i, i ^ 2 * hop) for i in range(tp)])]
    pallas_call x13 -> x14, Pallas kernels: 22.8 us -> 19.9 us  [call(): pl.pallas_call(kernel, in_specs=[vmem] * len(args) + [pl.BlockSpec(memory...]
    concatenate x2 -> x0, local copies, waits for them, and re-layouts: 2.59 us -> none  [the longest x1 1.78 us: split_device(): q_tab = jnp.concatenate([c0, c0, c1, c1, -s0, s0, -s1, s1], axis=1)]
  transfers between devices with their start and end apart: 27 -> 32, of which waited for: 12 -> 15; matrix products, arithmetic and copies ran while one was open for 8% -> 0% of each run, Pallas kernels for 11% -> 10%
where the time goes in v4:
time: 88.3 us; the launch traced here: 88.1 us
  waiting for transfers between devices  36.4 us (41%)
  starting transfers between devices  31.5 us (36%)
  Pallas kernels  19.9 us (23%)
    pallas_call x14, Pallas kernels, call(): pl.pallas_call(kernel, in_specs=[vmem] * len(args) + [pl.BlockSpec(memory...  19.9 us
    ppermute x9, starting transfers between devices, hopped(): lax.ppermute(value, 'tp', [(i, i ^ 2 * hop) for i in range(tp)])  10.5 us
    ppermute x9, waiting for transfers between devices, hopped(): lax.ppermute(value, 'tp', [(i, i ^ 2 * hop) for i in range(tp)])  10 us
    ppermute x3, waiting for transfers between devices, split_device(): lax.ppermute(part, 'tp', [(i, i ^ 2 * hop + 2) for i in range(tp)])  8.49 us
    ppermute x3, waiting for transfers between devices, split_device(): lax.ppermute(a, 'tp', [(i, i ^ 2 * hop + 2) for i in range(tp)])  8.19 us
    all_to_all x1, starting transfers between devices, split_device(): lax.all_to_all(modulation, ('sp', 'tp'), 0, 0, axis_index_groups=columns)  6.35 us
    ppermute x3, waiting for transfers between devices, split_device(): lax.ppermute(kv, 'sp', [(i, (i + shift) % sp) for i in range(sp)])  5.03 us
    ppermute x3, starting transfers between devices, split_device(): lax.ppermute(kv, 'sp', [(i, (i + shift) % sp) for i in range(sp)])  4.98 us
  transfers between devices with their start and end apart: 32, of which 15 were waited for; matrix products, arithmetic and copies ran while one was open for 0% of the time, Pallas kernels for 10%

profile of v4, /device:TPU:0, one launch (start us, length us, event | category | flops | bytes accessed | tf_op | source)
XLA Modules:
  0.0 88.1 jit_solution(8953721309520811506)
XLA Ops:
  0.0 2.5 %shard_map.154 = (f32[8,1,1280]{2,1,0:T(1,128)}, bf16[512,256]{1,0:T(8,128)(2,1)S(1)}, bf16[272,512]{1,0:T(8,128)(2,1)S(1)}, bf16[272,512]{1,0:T(8,128)(2,1)S(1)}) custom-call(bf16[384,256]{1,0:T(8,128)(2,1)} %latent_ref.1, bf16[128,256]{1,0:T(8,128)(2,1)} %ctx_ref.1, bf16[512]{0:T(512)(128)(2,1)} %cond_ref.1, bf16[512]{0:T(512)(128)(2,1)} %cond_ctx_ref.1, ...), custom_call_target="tpu_custom_call" | custom-call | flops 1000000 | bytes 100000 | tf_op jit(solution)/shard_map/pallas_call | solution.py:205
  2.5 0.5 collective-permute-start
  3.0 0.0 collective-permute-start.1
  3.0 6.4 %all-to-all-start = ((f32[8,1,1280]{2,1,0:T(1,128)}), f32[8,1,1280]{2,1,0:T(1,128)S(1)}, u32[]{:S(2)}, u32[]{:S(2)}) async-start(f32[8,1,1280]{2,1,0:T(1,128)} %get-tuple-element.53), calls=%async_computation | async-start | bytes 81920 | tf_op jit(solution)/shard_map/all_to_all | solution.py:680
  9.4 0.0 collective-permute-done.other_ref
  9.4 0.9 %shard_map.155.refs_0_ = f32[8,512]{1,0:T(8,128)S(1)} custom-call(bf16[512,256]{1,0:T(8,128)(2,1)S(1)} %get-tuple-element.52.own_ref, bf16[512,256]{1,0:T(8,128)(2,1)S(1)} %collective-permute-done.other_ref), custom_call_target="tpu_custom_call" | custom-call | flops 1000000 | bytes 100000 | tf_op jit(solution)/shard_map/pallas_call | solution.py:205
  10.3 2.5 %collective-permute-start.4 = (f32[8,512]{1,0:T(8,128)S(1)}, f32[8,512]{1,0:T(8,128)S(1)}, u32[]{:S(2)}, u32[]{:S(2)}) collective-permute-start(f32[8,512]{1,0:T(8,128)S(1)} %shard_map.155.refs_0_), channel_id=1, source_target_pairs={{0,6},{1,7},{2,4},{3,5},{4,2},{5,3},{6,0},{7,1},{8,14},{9,15},{10,... | collective-permute-start | bytes 49160 | tf_op jit(solution)/shard_map/ppermute | solution.py:653
  12.8 0.5 collective-permute-start.3
  13.3 0.5 collective-permute-start.2
  13.8 1.3 %all-to-all-done.mod_ref = f32[8,1,1280]{2,1,0:T(1,128)S(1)} async-done(((f32[8,1,1280]{2,1,0:T(1,128)}), f32[8,1,1280]{2,1,0:T(1,128)S(1)}, u32[]{:S(2)}, u32[]{:S(2)}) %all-to-all-start) | async-done | bytes 40992 | tf_op jit(solution)/shard_map/all_to_all | solution.py:680
  15.1 1.3 %collective-permute-done.3.refs_2_ = f32[8,512]{1,0:T(8,128)S(1)} collective-permute-done((f32[8,512]{1,0:T(8,128)S(1)}, f32[8,512]{1,0:T(8,128)S(1)}, u32[]{:S(2)}, u32[]{:S(2)}) %collective-permute-start.3) | collective-permute-done | bytes 16416 | tf_op jit(solution)/shard_map/ppermute | solution.py:653
  16.5 0.6 collective-permute-done.2.refs_1_
  17.1 1.6 %shard_map.156 = (f32[2,240,128]{2,1,0:T(8,128)S(1)}, f32[2,240,128]{2,1,0:T(8,128)S(1)}, f32[2,240,128]{2,1,0:T(8,128)S(1)}, f32[2,240,128]{2,1,0:T(8,128)S(1)}, f32[1,256]{1,0:T(1,128)S(1)}) custom-call(bf16[512,256]{1,0:T(8,128)(2,1)S(1)} %get-tuple-element.52.own_ref, bf16[512,256]{1,0:T(8,128)(2,1)S(1)} %collective-permute-done.other_ref, ...), custom_call_target="tpu_custom_call" | custom-call | flops 335544320 | bytes 100000 | tf_op jit(solution)/shard_map/pallas_call | solution.py:205
  18.7 0.0 copy-start.7
  18.7 0.0 copy-start.4
  18.7 0.2 shard_map.158
  18.9 0.1 collective-permute-start.8
  19.0 0.6 collective-permute-start.5
  19.6 1.5 %collective-permute-start.6 = (f32[2,240,128]{2,1,0:T(8,128)S(1)}, f32[2,240,128]{2,1,0:T(8,128)S(1)}, u32[]{:S(2)}, u32[]{:S(2)}) collective-permute-start(f32[2,240,128]{2,1,0:T(8,128)S(1)} %get-tuple-element.63), channel_id=1, source_target_pairs={{0,4},{1,5},{2,6},{3,7},{4,0},{5,1},{6,2},{7,3},{8,12},{9,13},{10,... | collective-permute-start | bytes 737288 | tf_op jit(solution)/shard_map/ppermute | solution.py:706
  21.1 1.4 %collective-permute-start.7 = (f32[2,240,128]{2,1,0:T(8,128)S(1)}, f32[2,240,128]{2,1,0:T(8,128)S(1)}, u32[]{:S(2)}, u32[]{:S(2)}) collective-permute-start(f32[2,240,128]{2,1,0:T(8,128)S(1)} %get-tuple-element.64), channel_id=1, source_target_pairs={{0,6},{1,7},{2,4},{3,5},{4,2},{5,3},{6,0},{7,1},{8,14},{9,15},{10,... | collective-permute-start | bytes 737288 | tf_op jit(solution)/shard_map/ppermute | solution.py:706
  22.5 0.0 copy-start.3
  22.6 2.5 %shard_map.157 = (f32[384,128]{1,0:T(8,128)S(1)}, bf16[512,1024]{1,0:T(8,128)(2,1)S(1)}) custom-call(f32[1,128]{1,0:T(1,128)S(1)} %broadcast_add_fusion.inverse_ref, bf16[512,4,256]{2,1,0:T(4,128)(2,1)S(1)} %copy-done.4), custom_call_target="tpu_custom_call" | custom-call | flops 1000000000 | bytes 100000 | tf_op jit(solution)/shard_map/pallas_call | solution.py:205
  25.1 2.8 %collective-permute-done.5.refs_1_ = f32[2,240,128]{2,1,0:T(8,128)S(1)} collective-permute-done((f32[2,240,128]{2,1,0:T(8,128)S(1)}, f32[2,240,128]{2,1,0:T(8,128)S(1)}, u32[]{:S(2)}, u32[]{:S(2)}) %collective-permute-start.5) | collective-permute-done | bytes 245792 | tf_op jit(solution)/shard_map/ppermute | solution.py:706
  27.9 4.1 %collective-permute-done.6.refs_2_ = f32[2,240,128]{2,1,0:T(8,128)S(1)} collective-permute-done((f32[2,240,128]{2,1,0:T(8,128)S(1)}, f32[2,240,128]{2,1,0:T(8,128)S(1)}, u32[]{:S(2)}, u32[]{:S(2)}) %collective-permute-start.6) | collective-permute-done | bytes 245792 | tf_op jit(solution)/shard_map/ppermute | solution.py:706
  31.9 1.6 %collective-permute-done.7.refs_3_ = f32[2,240,128]{2,1,0:T(8,128)S(1)} collective-permute-done((f32[2,240,128]{2,1,0:T(8,128)S(1)}, f32[2,240,128]{2,1,0:T(8,128)S(1)}, u32[]{:S(2)}, u32[]{:S(2)}) %collective-permute-start.7) | collective-permute-done | bytes 245792 | tf_op jit(solution)/shard_map/ppermute | solution.py:706
  33.6 0.0 copy-start.6
  33.6 0.0 copy-start.5
  33.6 0.1 collective-permute-start.9
  33.7 1.3 %collective-permute-done.9.other_ref = f32[240,128]{1,0:T(8,128)S(1)} collective-permute-done((f32[240,128]{1,0:T(8,128)S(1)}, f32[240,128]{1,0:T(8,128)S(1)}, u32[]{:S(2)}, u32[]{:S(2)}) %collective-permute-start.9) | collective-permute-done | bytes 122912 | tf_op jit(solution)/shard_map/ppermute | solution.py:728
  35.0 0.3 shard_map.160
  35.3 3.9 %collective-permute-start.15 = (bf16[72,512]{1,0:T(8,128)(2,1)S(1)}, bf16[72,512]{1,0:T(8,128)(2,1)S(1)}, u32[]{:S(2)}, u32[]{:S(2)}) collective-permute-start(bf16[72,512]{1,0:T(8,128)(2,1)S(1)} %get-tuple-element.79), channel_id=1, source_target_pairs={{0,24},{8,0},{16,8},{24,16},{1,25},{9,1},{17,9},{25,17},{2,26},{10... | collective-permute-start | bytes 221192 | tf_op jit(solution)/shard_map/ppermute | solution.py:743
  39.2 1.8 %collective-permute-start.12 = (bf16[120,512]{1,0:T(8,128)(2,1)S(1)}, bf16[120,512]{1,0:T(8,128)(2,1)S(1)}, u32[]{:S(2)}, u32[]{:S(2)}) collective-permute-start(bf16[120,512]{1,0:T(8,128)(2,1)S(1)} %get-tuple-element.80.refs_0_), channel_id=1, source_target_pairs={{0,6},{1,7},{2,4},{3,5},{4,2},{5,3},{6,0},{7,1},{8,14},{9,15},{10,... | collective-permute-start | bytes 368648 | tf_op jit(solution)/shard_map/ppermute | solution.py:653
  41.0 0.5 collective-permute-start.11
  41.5 1.2 %collective-permute-start.10 = (bf16[120,512]{1,0:T(8,128)(2,1)S(1)}, bf16[120,512]{1,0:T(8,128)(2,1)S(1)}, u32[]{:S(2)}, u32[]{:S(2)}) collective-permute-start(bf16[120,512]{1,0:T(8,128)(2,1)S(1)} %get-tuple-element.80.refs_0_), channel_id=1, source_target_pairs={{0,2},{1,3},{2,0},{3,1},{4,6},{5,7},{6,4},{7,5},{8,10},{9,11},{10,... | collective-permute-start | bytes 368648 | tf_op jit(solution)/shard_map/ppermute | solution.py:653
  42.7 1.1 %collective-permute-start.13 = (bf16[72,512]{1,0:T(8,128)(2,1)S(1)}, bf16[72,512]{1,0:T(8,128)(2,1)S(1)}, u32[]{:S(2)}, u32[]{:S(2)}) collective-permute-start(bf16[72,512]{1,0:T(8,128)(2,1)S(1)} %get-tuple-element.79), channel_id=1, source_target_pairs={{0,8},{8,16},{16,24},{24,0},{1,9},{9,17},{17,25},{25,1},{2,10},{10... | collective-permute-start | bytes 221192 | tf_op jit(solution)/shard_map/ppermute | solution.py:743
  43.8 4.2 %collective-permute-done.14.refs_1_ = bf16[72,512]{1,0:T(8,128)(2,1)S(1)} collective-permute-done((bf16[72,512]{1,0:T(8,128)(2,1)S(1)}, bf16[72,512]{1,0:T(8,128)(2,1)S(1)}, u32[]{:S(2)}, u32[]{:S(2)}) %collective-permute-start.14) | collective-permute-done | bytes 73760 | tf_op jit(solution)/shard_map/ppermute | solution.py:743
  48.0 0.8 collective-permute-done.13.refs_0_
  48.9 0.1 collective-permute-start.16
  48.9 0.5 collective-permute-start.17
  49.5 1.8 %collective-permute-start.23 = (bf16[216,512]{1,0:T(8,128)(2,1)S(1)}, bf16[216,512]{1,0:T(8,128)(2,1)S(1)}, u32[]{:S(2)}, u32[]{:S(2)}) collective-permute-start(bf16[216,512]{1,0:T(8,128)(2,1)S(1)} %shard_map.161.refs_8_), channel_id=1, source_target_pairs={{0,6},{1,7},{2,4},{3,5},{4,2},{5,3},{6,0},{7,1},{8,14},{9,15},{10,... | collective-permute-start | bytes 663560 | tf_op jit(solution)/shard_map/ppermute | solution.py:653
  51.3 0.5 collective-permute-start.22
  51.8 1.2 %collective-permute-start.21 = (bf16[216,512]{1,0:T(8,128)(2,1)S(1)}, bf16[216,512]{1,0:T(8,128)(2,1)S(1)}, u32[]{:S(2)}, u32[]{:S(2)}) collective-permute-start(bf16[216,512]{1,0:T(8,128)(2,1)S(1)} %shard_map.161.refs_8_), channel_id=1, source_target_pairs={{0,2},{1,3},{2,0},{3,1},{4,6},{5,7},{6,4},{7,5},{8,10},{9,11},{10,... | collective-permute-start | bytes 663560 | tf_op jit(solution)/shard_map/ppermute | solution.py:653
  53.0 0.5 collective-permute-start.20
  53.5 0.8 collective-permute-done.18.refs_6_
  54.4 0.1 collective-permute-start.19
  54.5 4.3 %collective-permute-done.23.refs_2_ = bf16[216,512]{1,0:T(8,128)(2,1)S(1)} collective-permute-done((bf16[216,512]{1,0:T(8,128)(2,1)S(1)}, bf16[216,512]{1,0:T(8,128)(2,1)S(1)}, u32[]{:S(2)}, u32[]{:S(2)}) %collective-permute-start.23) | collective-permute-done | bytes 221216 | tf_op jit(solution)/shard_map/ppermute | solution.py:653
  58.8 3.8 %collective-permute-done.22.refs_1_ = bf16[216,512]{1,0:T(8,128)(2,1)S(1)} collective-permute-done((bf16[216,512]{1,0:T(8,128)(2,1)S(1)}, bf16[216,512]{1,0:T(8,128)(2,1)S(1)}, u32[]{:S(2)}, u32[]{:S(2)}) %collective-permute-start.22) | collective-permute-done | bytes 221216 | tf_op jit(solution)/shard_map/ppermute | solution.py:653
  62.6 0.0 collective-permute-start.25
  62.6 0.5 collective-permute-start.24
  63.1 0.8 shard_map.163
  63.9 0.1 broadcast_in_dim.12.lift_ref
  64.0 3.9 %shard_map.162 = (bf16[4,384,256]{2,1,0:T(8,128)(2,1)S(1)}, f32[384,128]{1,0:T(8,128)S(1)}, f32[4,384,128]{2,1,0:T(8,128)S(1)}) custom-call(f32[384,128]{1,0:T(8,128)S(1)} %get-tuple-element.70.tab_ref, f32[4,128]{1,0:T(4,128)S(1)} %broadcast_in_dim.12.lift_ref, bf16[4,192,512]{2,1,0:T(8,128)(2,1)S(1)} %bitcast.10, ...), custom_call_target="tpu_custom_call" | custom-call | flops 1459617792 | bytes 100000 | tf_op jit(solution)/shard_map/pallas_call | solution.py:205
  68.0 5.2 %shard_map.164 = (bf16[384,512]{1,0:T(8,128)(2,1)S(1)}, bf16[4,512,256]{2,1,0:T(8,128)(2,1)S(1)}) custom-call(bf16[4,384,256]{2,1,0:T(8,128)(2,1)S(1)} %get-tuple-element.87.query_ref, f32[384,128]{1,0:T(8,128)S(1)} %get-tuple-element.88.stat_ref, f32[4,384,128]{2,1,0:T(8,128)S(1)} %get-tuple-element.89.sum_ref, ...), custom_call_target="tpu_custom_call" | custom-call | flops 1962934272 | bytes 100000 | tf_op jit(solution)/shard_map/pallas_call | solution.py:205
  73.1 0.1 collective-permute-start.27
  73.2 0.6 shard_map.165.acc_ref
  73.8 0.0 copy-start.1
  73.8 1.1 %collective-permute-done.27.heads_ref = bf16[384,512]{1,0:T(8,128)(2,1)S(1)} collective-permute-done((bf16[384,512]{1,0:T(8,128)(2,1)S(1)}, bf16[384,512]{1,0:T(8,128)(2,1)S(1)}, u32[]{:S(2)}, u32[]{:S(2)}) %collective-permute-start.27) | collective-permute-done | bytes 393248 | tf_op jit(solution)/shard_map/ppermute | solution.py:803
  74.9 0.6 shard_map.166
  75.5 0.9 collective-permute-start.28
  76.4 1.5 %collective-permute-start.29 = (bf16[384,256]{1,0:T(8,128)(2,1)S(1)}, bf16[384,256]{1,0:T(8,128)(2,1)S(1)}, u32[]{:S(2)}, u32[]{:S(2)}) collective-permute-start(bf16[384,256]{1,0:T(8,128)(2,1)S(1)} %get-tuple-element.97), channel_id=1, source_target_pairs={{0,4},{1,5},{2,6},{3,7},{4,0},{5,1},{6,2},{7,3},{8,12},{9,13},{10,... | collective-permute-start | bytes 589832 | tf_op jit(solution)/shard_map/ppermute | solution.py:818
  77.9 1.2 %collective-permute-start.30 = (bf16[384,256]{1,0:T(8,128)(2,1)S(1)}, bf16[384,256]{1,0:T(8,128)(2,1)S(1)}, u32[]{:S(2)}, u32[]{:S(2)}) collective-permute-start(bf16[384,256]{1,0:T(8,128)(2,1)S(1)} %get-tuple-element.98), channel_id=1, source_target_pairs={{0,6},{1,7},{2,4},{3,5},{4,2},{5,3},{6,0},{7,1},{8,14},{9,15},{10,... | collective-permute-start | bytes 589832 | tf_op jit(solution)/shard_map/ppermute | solution.py:818
  79.1 4.3 %collective-permute-done.28.refs_1_ = bf16[384,256]{1,0:T(8,128)(2,1)S(1)} collective-permute-done((bf16[384,256]{1,0:T(8,128)(2,1)S(1)}, bf16[384,256]{1,0:T(8,128)(2,1)S(1)}, u32[]{:S(2)}, u32[]{:S(2)}) %collective-permute-start.28) | collective-permute-done | bytes 196640 | tf_op jit(solution)/shard_map/ppermute | solution.py:818
  83.3 3.9 %collective-permute-done.29.refs_2_ = bf16[384,256]{1,0:T(8,128)(2,1)S(1)} collective-permute-done((bf16[384,256]{1,0:T(8,128)(2,1)S(1)}, bf16[384,256]{1,0:T(8,128)(2,1)S(1)}, u32[]{:S(2)}, u32[]{:S(2)}) %collective-permute-start.29) | collective-permute-done | bytes 196640 | tf_op jit(solution)/shard_map/ppermute | solution.py:818
  87.2 0.8 shard_map.167
  (32 shorter events, 0.1 us)
Async XLA Ops:
  0.0 18.7 %copy-start = (bf16[4,128,2048]{2,1,0:T(8,128)(2,1)S(1)}, bf16[4,128,2048]{2,1,0:T(8,128)(2,1)}, u32[]{:S(2)}) copy-start(bf16[4,128,2048]{2,1,0:T(8,128)(2,1)} %param.30) | copy-start | bytes 6291460
  2.5 6.9 %collective-permute-start = (bf16[512,256]{1,0:T(8,128)(2,1)S(1)}, bf16[512,256]{1,0:T(8,128)(2,1)S(1)}, u32[]{:S(2)}, u32[]{:S(2)}) collective-permute-start(bf16[512,256]{1,0:T(8,128)(2,1)S(1)} %get-tuple-element.52.own_ref), channel_id=1, source_target_pairs={{0,1},{1,0},{2,3},{3,2},{4,5},{5,4},{6,7},{7,6},{8,9},{9,8},{10,11... | collective-permute-start | bytes 786440 | tf_op jit(solution)/shard_map/ppermute | solution.py:678
  3.0 14.1 %collective-permute-start.1 = (bf16[272,512]{1,0:T(8,128)(2,1)S(1)}, bf16[272,512]{1,0:T(8,128)(2,1)S(1)}, u32[]{:S(2)}, u32[]{:S(2)}) collective-permute-start(bf16[272,512]{1,0:T(8,128)(2,1)S(1)} %get-tuple-element.55), channel_id=1, source_target_pairs={{0,1},{1,0},{2,3},{3,2},{4,5},{5,4},{6,7},{7,6},{8,9},{9,8},{10,11... | collective-permute-start | bytes 835592 | tf_op jit(solution)/shard_map/ppermute | solution.py:677
  3.0 12.1 %all-to-all-start = ((f32[8,1,1280]{2,1,0:T(1,128)}), f32[8,1,1280]{2,1,0:T(1,128)S(1)}, u32[]{:S(2)}, u32[]{:S(2)}) async-start(f32[8,1,1280]{2,1,0:T(1,128)} %get-tuple-element.53), calls=%async_computation | async-start | bytes 81920 | tf_op jit(solution)/shard_map/all_to_all | solution.py:680
  10.3 4.9 %collective-permute-start.4 = (f32[8,512]{1,0:T(8,128)S(1)}, f32[8,512]{1,0:T(8,128)S(1)}, u32[]{:S(2)}, u32[]{:S(2)}) collective-permute-start(f32[8,512]{1,0:T(8,128)S(1)} %shard_map.155.refs_0_), channel_id=1, source_target_pairs={{0,6},{1,7},{2,4},{3,5},{4,2},{5,3},{6,0},{7,1},{8,14},{9,15},{10,... | collective-permute-start | bytes 49160 | tf_op jit(solution)/shard_map/ppermute | solution.py:653
  12.8 3.7 %collective-permute-start.3 = (f32[8,512]{1,0:T(8,128)S(1)}, f32[8,512]{1,0:T(8,128)S(1)}, u32[]{:S(2)}, u32[]{:S(2)}) collective-permute-start(f32[8,512]{1,0:T(8,128)S(1)} %shard_map.155.refs_0_), channel_id=1, source_target_pairs={{0,4},{1,5},{2,6},{3,7},{4,0},{5,1},{6,2},{7,3},{8,12},{9,13},{10,... | collective-permute-start | bytes 49160 | tf_op jit(solution)/shard_map/ppermute | solution.py:653
  13.3 3.8 %collective-permute-start.2 = (f32[8,512]{1,0:T(8,128)S(1)}, f32[8,512]{1,0:T(8,128)}, u32[]{:S(2)}, u32[]{:S(2)}) collective-permute-start(f32[8,512]{1,0:T(8,128)S(1)} %shard_map.155.refs_0_), channel_id=1, source_target_pairs={{0,2},{1,3},{2,0},{3,1},{4,6},{5,7},{6,4},{7,5},{8,10},{9,11},{10,... | collective-permute-start | bytes 49160 | tf_op jit(solution)/shard_map/ppermute | solution.py:653
  18.7 3.8 %copy-start.7 = (f32[1,128]{1,0:T(1,128)S(1)}, f32[1,128]{1,0:T(1,128)}, u32[]{:S(2)}) copy-start(f32[1,128]{1,0:T(1,128)} %constant.4.clone) | copy-start | bytes 1540
  18.7 3.8 %copy-start.4 = (bf16[512,4,256]{2,1,0:T(4,128)(2,1)S(1)}, bf16[512,4,256]{2,1,0:T(4,128)(2,1)}, u32[]{:S(2)}) copy-start(bf16[512,4,256]{2,1,0:T(4,128)(2,1)} %w_ref) | copy-start | bytes 3145732
  18.9 14.7 %collective-permute-start.8 = (bf16[4,512,256]{2,1,0:T(8,128)(2,1)S(1)}, bf16[4,512,256]{2,1,0:T(8,128)(2,1)S(1)}, u32[]{:S(2)}, u32[]{:S(2)}) collective-permute-start(bf16[4,512,256]{2,1,0:T(8,128)(2,1)S(1)} %shard_map.158), channel_id=1, source_target_pairs={{0,1},{1,0},{2,3},{3,2},{4,5},{5,4},{6,7},{7,6},{8,9},{9,8},{10,11... | collective-permute-start | bytes 3145736 | tf_op jit(solution)/shard_map/ppermute | solution.py:724
  19.0 8.9 %collective-permute-start.5 = (f32[2,240,128]{2,1,0:T(8,128)S(1)}, f32[2,240,128]{2,1,0:T(8,128)S(1)}, u32[]{:S(2)}, u32[]{:S(2)}) collective-permute-start(f32[2,240,128]{2,1,0:T(8,128)S(1)} %get-tuple-element.62), channel_id=1, source_target_pairs={{0,2},{1,3},{2,0},{3,1},{4,6},{5,7},{6,4},{7,5},{8,10},{9,11},{10,... | collective-permute-start | bytes 737288 | tf_op jit(solution)/shard_map/ppermute | solution.py:706
  19.6 12.3 %collective-permute-start.6 = (f32[2,240,128]{2,1,0:T(8,128)S(1)}, f32[2,240,128]{2,1,0:T(8,128)S(1)}, u32[]{:S(2)}, u32[]{:S(2)}) collective-permute-start(f32[2,240,128]{2,1,0:T(8,128)S(1)} %get-tuple-element.63), channel_id=1, source_target_pairs={{0,4},{1,5},{2,6},{3,7},{4,0},{5,1},{6,2},{7,3},{8,12},{9,13},{10,... | collective-permute-start | bytes 737288 | tf_op jit(solution)/shard_map/ppermute | solution.py:706
  21.1 12.5 %collective-permute-start.7 = (f32[2,240,128]{2,1,0:T(8,128)S(1)}, f32[2,240,128]{2,1,0:T(8,128)S(1)}, u32[]{:S(2)}, u32[]{:S(2)}) collective-permute-start(f32[2,240,128]{2,1,0:T(8,128)S(1)} %get-tuple-element.64), channel_id=1, source_target_pairs={{0,6},{1,7},{2,4},{3,5},{4,2},{5,3},{6,0},{7,1},{8,14},{9,15},{10,... | collective-permute-start | bytes 737288 | tf_op jit(solution)/shard_map/ppermute | solution.py:706
  22.5 12.5 %copy-start.2 = (f32[512]{0:T(512)S(1)}, f32[512]{0:T(512)}, u32[]{:S(2)}) copy-start(f32[512]{0:T(512)} %param.25) | copy-start | bytes 6148
  22.5 12.5 %copy-start.3 = (f32[512]{0:T(512)S(1)}, f32[512]{0:T(512)}, u32[]{:S(2)}) copy-start(f32[512]{0:T(512)} %param.26) | copy-start | bytes 6148
  33.6 30.3 %copy-start.6 = (f32[4]{0:T(128)S(1)}, f32[4]{0:T(128)}, u32[]{:S(2)}) copy-start(f32[4]{0:T(128)} %param.29) | copy-start | bytes 52
  33.6 30.4 %copy-start.5 = (bf16[512,4,192]{0,2,1:T(8,128)(2,1)S(1)}, bf16[512,4,192]{0,2,1:T(8,128)(2,1)}, u32[]{:S(2)}) copy-start(bf16[512,4,192]{0,2,1:T(8,128)(2,1)} %param.27) | copy-start | bytes 2359300
  33.6 1.4 %collective-permute-start.9 = (f32[240,128]{1,0:T(8,128)S(1)}, f32[240,128]{1,0:T(8,128)S(1)}, u32[]{:S(2)}, u32[]{:S(2)}) collective-permute-start(f32[240,128]{1,0:T(8,128)S(1)} %get-tuple-element.77), channel_id=1, source_target_pairs={{0,1},{1,0},{2,3},{3,2},{4,5},{5,4},{6,7},{7,6},{8,9},{9,8},{10,11... | collective-permute-start | bytes 368648 | tf_op jit(solution)/shard_map/ppermute | solution.py:728
  35.3 7.4 %collective-permute-start.15 = (bf16[72,512]{1,0:T(8,128)(2,1)S(1)}, bf16[72,512]{1,0:T(8,128)(2,1)S(1)}, u32[]{:S(2)}, u32[]{:S(2)}) collective-permute-start(bf16[72,512]{1,0:T(8,128)(2,1)S(1)} %get-tuple-element.79), channel_id=1, source_target_pairs={{0,24},{8,0},{16,8},{24,16},{1,25},{9,1},{17,9},{25,17},{2,26},{10... | collective-permute-start | bytes 221192 | tf_op jit(solution)/shard_map/ppermute | solution.py:743
  39.2 9.7 %collective-permute-start.12 = (bf16[120,512]{1,0:T(8,128)(2,1)S(1)}, bf16[120,512]{1,0:T(8,128)(2,1)S(1)}, u32[]{:S(2)}, u32[]{:S(2)}) collective-permute-start(bf16[120,512]{1,0:T(8,128)(2,1)S(1)} %get-tuple-element.80.refs_0_), channel_id=1, source_target_pairs={{0,6},{1,7},{2,4},{3,5},{4,2},{5,3},{6,0},{7,1},{8,14},{9,15},{10,... | collective-permute-start | bytes 368648 | tf_op jit(solution)/shard_map/ppermute | solution.py:653
  41.0 7.9 %collective-permute-start.11 = (bf16[120,512]{1,0:T(8,128)(2,1)S(1)}, bf16[120,512]{1,0:T(8,128)(2,1)S(1)}, u32[]{:S(2)}, u32[]{:S(2)}) collective-permute-start(bf16[120,512]{1,0:T(8,128)(2,1)S(1)} %get-tuple-element.80.refs_0_), channel_id=1, source_target_pairs={{0,4},{1,5},{2,6},{3,7},{4,0},{5,1},{6,2},{7,3},{8,12},{9,13},{10,... | collective-permute-start | bytes 368648 | tf_op jit(solution)/shard_map/ppermute | solution.py:653
  41.5 7.4 %collective-permute-start.10 = (bf16[120,512]{1,0:T(8,128)(2,1)S(1)}, bf16[120,512]{1,0:T(8,128)(2,1)S(1)}, u32[]{:S(2)}, u32[]{:S(2)}) collective-permute-start(bf16[120,512]{1,0:T(8,128)(2,1)S(1)} %get-tuple-element.80.refs_0_), channel_id=1, source_target_pairs={{0,2},{1,3},{2,0},{3,1},{4,6},{5,7},{6,4},{7,5},{8,10},{9,11},{10,... | collective-permute-start | bytes 368648 | tf_op jit(solution)/shard_map/ppermute | solution.py:653
  42.7 5.3 %collective-permute-start.14 = (bf16[72,512]{1,0:T(8,128)(2,1)S(1)}, bf16[72,512]{1,0:T(8,128)(2,1)S(1)}, u32[]{:S(2)}, u32[]{:S(2)}) collective-permute-start(bf16[72,512]{1,0:T(8,128)(2,1)S(1)} %get-tuple-element.79), channel_id=1, source_target_pairs={{0,16},{8,24},{16,0},{24,8},{1,17},{9,25},{17,1},{25,9},{2,18},{10... | collective-permute-start | bytes 221192 | tf_op jit(solution)/shard_map/ppermute | solution.py:743
  42.7 6.2 %collective-permute-start.13 = (bf16[72,512]{1,0:T(8,128)(2,1)S(1)}, bf16[72,512]{1,0:T(8,128)(2,1)S(1)}, u32[]{:S(2)}, u32[]{:S(2)}) collective-permute-start(bf16[72,512]{1,0:T(8,128)(2,1)S(1)} %get-tuple-element.79), channel_id=1, source_target_pairs={{0,8},{8,16},{16,24},{24,0},{1,9},{9,17},{17,25},{25,1},{2,10},{10... | collective-permute-start | bytes 221192 | tf_op jit(solution)/shard_map/ppermute | solution.py:743
  48.9 4.2 %collective-permute-start.16 = (bf16[120,512]{1,0:T(8,128)(2,1)S(1)}, bf16[120,512]{1,0:T(8,128)(2,1)S(1)}, u32[]{:S(2)}, u32[]{:S(2)}) collective-permute-start(bf16[120,512]{1,0:T(8,128)(2,1)S(1)} %get-tuple-element.80.refs_0_), channel_id=1, source_target_pairs={{0,1},{1,0},{2,3},{3,2},{4,5},{5,4},{6,7},{7,6},{8,9},{9,8},{10,11... | collective-permute-start | bytes 368648 | tf_op jit(solution)/shard_map/ppermute | solution.py:748
  48.9 4.1 %collective-permute-start.17 = (bf16[120,512]{1,0:T(8,128)(2,1)S(1)}, bf16[120,512]{1,0:T(8,128)(2,1)S(1)}, u32[]{:S(2)}, u32[]{:S(2)}) collective-permute-start(bf16[120,512]{1,0:T(8,128)(2,1)S(1)} %collective-permute-done.10.refs_1_), channel_id=1, source_target_pairs={{0,1},{1,0},{2,3},{3,2},{4,5},{5,4},{6,7},{7,6},{8,9},{9,8},{10,11... | collective-permute-start | bytes 368648 | tf_op jit(solution)/shard_map/ppermute | solution.py:748
  49.5 9.3 %collective-permute-start.23 = (bf16[216,512]{1,0:T(8,128)(2,1)S(1)}, bf16[216,512]{1,0:T(8,128)(2,1)S(1)}, u32[]{:S(2)}, u32[]{:S(2)}) collective-permute-start(bf16[216,512]{1,0:T(8,128)(2,1)S(1)} %shard_map.161.refs_8_), channel_id=1, source_target_pairs={{0,6},{1,7},{2,4},{3,5},{4,2},{5,3},{6,0},{7,1},{8,14},{9,15},{10,... | collective-permute-start | bytes 663560 | tf_op jit(solution)/shard_map/ppermute | solution.py:653
  51.3 11.3 %collective-permute-start.22 = (bf16[216,512]{1,0:T(8,128)(2,1)S(1)}, bf16[216,512]{1,0:T(8,128)(2,1)S(1)}, u32[]{:S(2)}, u32[]{:S(2)}) collective-permute-start(bf16[216,512]{1,0:T(8,128)(2,1)S(1)} %shard_map.161.refs_8_), channel_id=1, source_target_pairs={{0,4},{1,5},{2,6},{3,7},{4,0},{5,1},{6,2},{7,3},{8,12},{9,13},{10,... | collective-permute-start | bytes 663560 | tf_op jit(solution)/shard_map/ppermute | solution.py:653
  51.8 10.8 %collective-permute-start.21 = (bf16[216,512]{1,0:T(8,128)(2,1)S(1)}, bf16[216,512]{1,0:T(8,128)(2,1)S(1)}, u32[]{:S(2)}, u32[]{:S(2)}) collective-permute-start(bf16[216,512]{1,0:T(8,128)(2,1)S(1)} %shard_map.161.refs_8_), channel_id=1, source_target_pairs={{0,2},{1,3},{2,0},{3,1},{4,6},{5,7},{6,4},{7,5},{8,10},{9,11},{10,... | collective-permute-start | bytes 663560 | tf_op jit(solution)/shard_map/ppermute | solution.py:653
  53.0 1.3 %collective-permute-start.18 = (bf16[120,512]{1,0:T(8,128)(2,1)S(1)}, bf16[120,512]{1,0:T(8,128)(2,1)S(1)}, u32[]{:S(2)}, u32[]{:S(2)}) collective-permute-start(bf16[120,512]{1,0:T(8,128)(2,1)S(1)} %collective-permute-done.11.refs_2_), channel_id=1, source_target_pairs={{0,1},{1,0},{2,3},{3,2},{4,5},{5,4},{6,7},{7,6},{8,9},{9,8},{10,11... | collective-permute-start | bytes 368648 | tf_op jit(solution)/shard_map/ppermute | solution.py:748
  53.0 10.9 %collective-permute-start.20 = (bf16[216,512]{1,0:T(8,128)(2,1)S(1)}, bf16[216,512]{1,0:T(8,128)(2,1)S(1)}, u32[]{:S(2)}, u32[]{:S(2)}) collective-permute-start(bf16[216,512]{1,0:T(8,128)(2,1)S(1)} %shard_map.161.refs_8_), channel_id=1, source_target_pairs={{0,1},{1,0},{2,3},{3,2},{4,5},{5,4},{6,7},{7,6},{8,9},{9,8},{10,11... | collective-permute-start | bytes 663560 | tf_op jit(solution)/shard_map/ppermute | solution.py:751
  54.4 9.6 %collective-permute-start.19 = (bf16[120,512]{1,0:T(8,128)(2,1)S(1)}, bf16[120,512]{1,0:T(8,128)(2,1)S(1)}, u32[]{:S(2)}, u32[]{:S(2)}) collective-permute-start(bf16[120,512]{1,0:T(8,128)(2,1)S(1)} %collective-permute-done.12.refs_3_), channel_id=1, source_target_pairs={{0,1},{1,0},{2,3},{3,2},{4,5},{5,4},{6,7},{7,6},{8,9},{9,8},{10,11... | collective-permute-start | bytes 368648 | tf_op jit(solution)/shard_map/ppermute | solution.py:748
  58.8 9.2 %collective-permute-start.26 = (bf16[216,512]{1,0:T(8,128)(2,1)S(1)}, bf16[216,512]{1,0:T(8,128)(2,1)S(1)}, u32[]{:S(2)}, u32[]{:S(2)}) collective-permute-start(bf16[216,512]{1,0:T(8,128)(2,1)S(1)} %collective-permute-done.23.refs_2_), channel_id=1, source_target_pairs={{0,1},{1,0},{2,3},{3,2},{4,5},{5,4},{6,7},{7,6},{8,9},{9,8},{10,11... | collective-permute-start | bytes 663560 | tf_op jit(solution)/shard_map/ppermute | solution.py:751
  62.6 5.4 %collective-permute-start.25 = (bf16[216,512]{1,0:T(8,128)(2,1)S(1)}, bf16[216,512]{1,0:T(8,128)(2,1)S(1)}, u32[]{:S(2)}, u32[]{:S(2)}) collective-permute-start(bf16[216,512]{1,0:T(8,128)(2,1)S(1)} %collective-permute-done.22.refs_1_), channel_id=1, source_target_pairs={{0,1},{1,0},{2,3},{3,2},{4,5},{5,4},{6,7},{7,6},{8,9},{9,8},{10,11... | collective-permute-start | bytes 663560 | tf_op jit(solution)/shard_map/ppermute | solution.py:751
  62.6 5.4 %collective-permute-start.24 = (bf16[216,512]{1,0:T(8,128)(2,1)S(1)}, bf16[216,512]{1,0:T(8,128)(2,1)S(1)}, u32[]{:S(2)}, u32[]{:S(2)}) collective-permute-start(bf16[216,512]{1,0:T(8,128)(2,1)S(1)} %collective-permute-done.21.refs_0_), channel_id=1, source_target_pairs={{0,1},{1,0},{2,3},{3,2},{4,5},{5,4},{6,7},{7,6},{8,9},{9,8},{10,11... | collective-permute-start | bytes 663560 | tf_op jit(solution)/shard_map/ppermute | solution.py:751
  73.1 1.8 %collective-permute-start.27 = (bf16[384,512]{1,0:T(8,128)(2,1)S(1)}, bf16[384,512]{1,0:T(8,128)(2,1)S(1)}, u32[]{:S(2)}, u32[]{:S(2)}) collective-permute-start(bf16[384,512]{1,0:T(8,128)(2,1)S(1)} %get-tuple-element.93.heads_ref), channel_id=1, source_target_pairs={{0,1},{1,0},{2,3},{3,2},{4,5},{5,4},{6,7},{7,6},{8,9},{9,8},{10,11... | collective-permute-start | bytes 1179656 | tf_op jit(solution)/shard_map/ppermute | solution.py:803
  73.8 13.4 %copy-start.1 = (bf16[384,256]{1,0:T(8,128)(2,1)S(1)}, bf16[384,256]{1,0:T(8,128)(2,1)}, u32[]{:S(2)}) copy-start(bf16[384,256]{1,0:T(8,128)(2,1)} %latent_ref.1) | copy-start | bytes 589828
  75.5 7.8 %collective-permute-start.28 = (bf16[384,256]{1,0:T(8,128)(2,1)S(1)}, bf16[384,256]{1,0:T(8,128)(2,1)S(1)}, u32[]{:S(2)}, u32[]{:S(2)}) collective-permute-start(bf16[384,256]{1,0:T(8,128)(2,1)S(1)} %get-tuple-element.96), channel_id=1, source_target_pairs={{0,2},{1,3},{2,0},{3,1},{4,6},{5,7},{6,4},{7,5},{8,10},{9,11},{10,... | collective-permute-start | bytes 589832 | tf_op jit(solution)/shard_map/ppermute | solution.py:818
  76.4 10.9 %collective-permute-start.29 = (bf16[384,256]{1,0:T(8,128)(2,1)S(1)}, bf16[384,256]{1,0:T(8,128)(2,1)S(1)}, u32[]{:S(2)}, u32[]{:S(2)}) collective-permute-start(bf16[384,256]{1,0:T(8,128)(2,1)S(1)} %get-tuple-element.97), channel_id=1, source_target_pairs={{0,4},{1,5},{2,6},{3,7},{4,0},{5,1},{6,2},{7,3},{8,12},{9,13},{10,... | collective-permute-start | bytes 589832 | tf_op jit(solution)/shard_map/ppermute | solution.py:818
  77.9 9.4 %collective-permute-start.30 = (bf16[384,256]{1,0:T(8,128)(2,1)S(1)}, bf16[384,256]{1,0:T(8,128)(2,1)S(1)}, u32[]{:S(2)}, u32[]{:S(2)}) collective-permute-start(bf16[384,256]{1,0:T(8,128)(2,1)S(1)} %get-tuple-element.98), channel_id=1, source_target_pairs={{0,6},{1,7},{2,4},{3,5},{4,2},{5,3},{6,0},{7,1},{8,14},{9,15},{10,... | collective-permute-start | bytes 589832 | tf_op jit(solution)/shard_map/ppermute | solution.py:818

commit v5 on v4

--- a/solution.py
+++ b/solution.py
@@ -286,8 +286,8 @@
     own_ref, other_ref, mod_ref, w_own_ref, w_other_ref, *refs, sp, tp, rows
 ):
     chips = tp // 2
-    squares, out_refs = refs[:chips], refs[chips : 2 * chips]
-    gate_ref, lat_ref, ctx_ref, lat_rot_ref, ctx_rot_ref = refs[2 * chips :]
+    squares, kv_refs, q_refs = refs[:chips], refs[chips : 2 * chips], refs[2 * chips : 3 * chips]
+    gate_ref, lat_ref, ctx_ref, lat_rot_ref, ctx_rot_ref = refs[3 * chips :]
     count, features = own_ref.shape
     ctx_rows = count - rows
     rank = w_own_ref.shape[1]
@@ -337,15 +337,20 @@
         for core in range(2):
             d = 2 * (here ^ hop) + core
             lats, ctxs = pl.ds(pl.multiple_of(d * lat, 8), lat), pl.ds(pl.multiple_of(d * ctx, 8), ctx)
+            for slab in range(half // 128):
+                q_refs[hop][core, slab * lat : (slab + 1) * lat, :] = lat_ref[
+                    lats, slab * 128 : (slab + 1) * 128
+                ]
             at = 0
-            for source, part, size in ((lat_ref, lats, lat), (ctx_ref, ctxs, ctx)):
-                for slab in range(source.shape[1] // 128):
-                    out_refs[hop][core, at : at + size, :] = source[
-                        part, slab * 128 : (slab + 1) * 128
-                    ]
+            for source, part, first, size in (
+                (lat_ref, lats, half, lat),
+                (ctx_ref, ctxs, 0, ctx),
+            ):
+                for column in range(first, source.shape[1], 128):
+                    kv_refs[hop][core, at : at + size, :] = source[part, column : column + 128]
                     at += size
             rot = jnp.concatenate([lat_rot_ref[lats], ctx_rot_ref[ctxs]], axis=0)
-            out_refs[hop][core, at : at + quarter, :] = jnp.concatenate(
+            kv_refs[hop][core, at : at + quarter, :] = jnp.concatenate(
                 [rot[i * quarter : (i + 1) * quarter] for i in range(4)], axis=1
             )
 
@@ -360,7 +365,7 @@
         ref[...] = total
 
 
-def prepare_kernel(inverse_ref, w_ref, tab_ref, out_ref):
+def tables_kernel(inverse_ref, tab_ref):
     rows, lanes = tab_ref.shape
     position = lax.broadcasted_iota(jnp.int32, (rows, lanes), 0) + lax.axis_index("sp") * rows
     lane = lax.broadcasted_iota(jnp.int32, (rows, lanes), 1)
@@ -369,38 +374,43 @@
     sine = jnp.sin(angle)
     sine = jnp.where(lane % (ROPE // 2) < ROPE // 4, -sine, sine)
     tab_ref[...] = jnp.where(lane < ROPE, jnp.cos(angle), sine)
+
+
+def relay_kernel(w_ref, out_ref):
     width = w_ref.shape[2]
     for head in range(w_ref.shape[1]):
         out_ref[:, head * width : (head + 1) * width] = w_ref[:, head, :]
 
 
-def norm_kernel(own_ref, other_ref, gq_ref, gkv_ref, tab_ref, kv_ref, near_ref, *, lat, ctx):
-    unused, unused, side, me = place()
-    first = side == 0
+def halves_of(own_ref, other_ref):
+    first = place()[2] == 0
     own, other = own_ref[...], other_ref[...]
+    return [jnp.where(first, own, other), jnp.where(first, other, own)]
+
+
+def normed(halves, start, count, gain_ref):
+    slabs = gain_ref.shape[1] // 256
+    values = jnp.concatenate(
+        [
+            half[start + i * count : start + (i + 1) * count]
+            for half in halves
+            for i in range(slabs)
+        ],
+        axis=1,
+    )
+    factor = lax.rsqrt(jnp.mean(values * values, axis=1, keepdims=True) + EPS)
+    return (values * factor * gain_ref[...]).astype(jnp.bfloat16)
+
+
+def norm_kernel(own_ref, other_ref, gain_ref, tab_ref, kv_ref, *, lat, ctx):
+    me = place()[3]
     tab = tab_ref[pl.ds(pl.multiple_of(me * lat, 8), lat), :]
-    halves = [jnp.where(first, own, other), jnp.where(first, other, own)]
-    rank = gq_ref.shape[1]
+    halves = halves_of(own_ref, other_ref)
+    rank = gain_ref.shape[1]
     slabs = rank // 256
-
-    def columns(start, count):
-        return jnp.concatenate(
-            [
-                half[start + i * count : start + (i + 1) * count]
-                for half in halves
-                for i in range(slabs)
-            ],
-            axis=1,
-        )
-
-    def normed(values, gain):
-        factor = lax.rsqrt(jnp.mean(values * values, axis=1, keepdims=True) + EPS)
-        return (values * factor * gain).astype(jnp.bfloat16)
-
-    cq = normed(columns(0, lat), gq_ref[...])
-    lat_kv = normed(columns(slabs * lat, lat), gkv_ref[...])
-    at = 2 * slabs * lat
-    ctx_kv = normed(columns(at, ctx), gkv_ref[...])
+    lat_kv = normed(halves, 0, lat, gain_ref)
+    at = slabs * lat
+    ctx_kv = normed(halves, at, ctx, gain_ref)
     at += slabs * ctx
     quarter = (lat + ctx) // 4
     width = ROPE // 2
@@ -424,11 +434,14 @@
     keys = jnp.concatenate(
         [keys[i * low : (i + 1) * low] for i in range(pieces)], axis=1
     ).astype(jnp.bfloat16)
-    compressed = jnp.concatenate([lat_kv, ctx_kv], axis=0)
-    for ref in (kv_ref, near_ref):
-        ref[: lat + ctx] = compressed
-        ref[lat + ctx : lat + ctx + low] = keys
-    near_ref[lat + ctx + low :] = cq
+    kv_ref[: lat + ctx] = jnp.concatenate([lat_kv, ctx_kv], axis=0)
+    kv_ref[lat + ctx :] = keys
+
+
+def norm_query_kernel(own_ref, other_ref, gain_ref, kv_ref, near_ref):
+    size, lat = kv_ref.shape[0], near_ref.shape[0] - kv_ref.shape[0]
+    near_ref[:size] = kv_ref[...]
+    near_ref[size:] = normed(halves_of(own_ref, other_ref), 0, lat, gain_ref)
 
 
 def gather_kernel(*refs):
@@ -681,11 +694,11 @@
     squares = call(square_kernel, array((8, rows + ctx_rows), f32), tokens, tokens_other)
     squares = hopped(squares)
 
-    height = half // 128 * (2 * lat + ctx) + (lat + ctx) // 4
-    share = array((2, height, 128), f32)
+    q_part = array((2, half // 128 * lat, 128), f32)
+    kv_part = array((2, half // 128 * (lat + ctx) + (lat + ctx) // 4, 128), f32)
     *parts, gate = call(
         functools.partial(project_kernel, sp=sp, tp=tp, rows=rows),
-        (share,) * chips + (array((1, features), f32),),
+        (kv_part,) * chips + (q_part,) * chips + (array((1, features), f32),),
         tokens,
         tokens_other,
         modulation,
@@ -702,49 +715,49 @@
         limit=16,
     )
     *parts, w_kv, w_up, zero = lax.optimization_barrier((*parts, w_ukv, w_out, jnp.float32(0)))
-    parts = [parts[0]] + [
-        lax.ppermute(part, "tp", [(i, i ^ (2 * hop + 2)) for i in range(tp)])
-        for hop, part in enumerate(parts[1:])
-    ]
+
+    def collected(parts):
+        return [parts[0]] + [
+            lax.ppermute(part, "tp", [(i, i ^ (2 * hop + 2)) for i in range(tp)])
+            for hop, part in enumerate(parts[1:])
+        ]
+
+    def reduced(parts):
+        shape = array(parts[0].shape[1:], f32)
+        own, other = call(reduce_kernel, (shape, shape), *parts)
+        return own, lax.ppermute(other, "tp", across)
+
+    kv_parts = collected(parts[:chips])
+    q_parts = collected(parts[chips:])
 
     quarter = ROPE // 4
     inverse = THETA ** (-np.arange(quarter) / quarter)
     inverse = jnp.asarray(np.tile(inverse, 128 // quarter)[None], f32) + zero
-    q_tab, w_kv = call(
-        prepare_kernel,
-        (array((rows, 128), f32), array((rank, heads * (NOPE + DV)))),
-        inverse,
-        w_kv,
-        flops=1e9,
-    )
+    q_tab = call(tables_kernel, array((rows, 128), f32), inverse, flops=1e9)
+    w_kv = call(relay_kernel, array((rank, heads * (NOPE + DV))), w_kv, flops=1e9)
     w_up = w_up.reshape(heads * DV, 2 * chips * features)
     w_up_other = call(
         share_out_kernel, array((chips, heads * DV, features)), w_up, flops=1e9, kept=False
     )
     w_up_other = lax.ppermute(w_up_other, "tp", across)
-    *parts, q_tab, w_up_other, w_kv = lax.optimization_barrier((*parts, q_tab, w_up_other, w_kv))
-    share = array((height, 128), f32)
-    part, part_other = call(reduce_kernel, (share, share), *parts)
-    part_other = lax.ppermute(part_other, "tp", across)
-
     count = lat + ctx
     step = count + count * ROPE // rank
-    kv, near = call(
+    kv = call(
         functools.partial(norm_kernel, lat=lat, ctx=ctx),
-        (array((step, rank)), array((step + lat, rank))),
-        part,
-        part_other,
-        g_cq[None],
+        array((step, rank)),
+        *reduced(kv_parts),
         g_ckv[None],
         q_tab,
     )
-
+    *q_parts, w_up_other = lax.optimization_barrier((*q_parts, w_up_other))
+
+    even = sp & (sp - 1) == 0
     planes = [
-        lax.ppermute(kv, "sp", [(i, (i + shift) % sp) for i in range(sp)])
-        for shift in range(1, sp)
+        lax.ppermute(kv, "sp", [(i, i ^ hop if even else (i + hop) % sp) for i in range(sp)])
+        for hop in range(1, sp)
     ]
+    near = call(norm_query_kernel, array((step + lat, rank)), *reduced(q_parts), g_cq[None], kv)
     near_own = hopped(near)
-    near_own, planes = lax.optimization_barrier((near_own, planes))
     near_other = [lax.ppermute(n, "tp", across) for n in near_own]
     far = call(gather_kernel, array(((sp - 1) * step, rank)), *planes)
     far_own = hopped(far)

time: 88.3 us -> 91.9 us (1.041)
  starting transfers between devices: 31.5 us -> 38 us
  waiting for transfers between devices: 36.4 us -> 32.8 us
    ppermute x7 -> x11, starting transfers between devices: 8.61 us -> 15.2 us  [the longest x6 7.62 us: collected(): lax.ppermute(part, 'tp', [(i, i ^ 2 * hop + 2) for i in range(tp)])]
    ppermute x7 -> x11, waiting for transfers between devices: 14.8 us -> 10.6 us  [the longest x6 7.94 us: collected(): lax.ppermute(part, 'tp', [(i, i ^ 2 * hop + 2) for i in range(tp)])]
    pallas_call x14 -> x17, Pallas kernels: 19.9 us -> 20.2 us  [call(): pl.pallas_call(kernel, in_specs=[vmem] * len(args) + [pl.BlockSpec(memory...]
  transfers between devices with their start and end apart: 32 -> 36, of which waited for: 15 -> 19; matrix products, arithmetic and copies ran while one was open for 0% -> 0% of each run, Pallas kernels for 10% -> 10%
where the time goes in v5:
time: 91.9 us; the launch traced here: 91.6 us
  starting transfers between devices  38 us (41%)
  waiting for transfers between devices  32.8 us (36%)
  Pallas kernels  20.2 us (22%)
    pallas_call x17, Pallas kernels, call(): pl.pallas_call(kernel, in_specs=[vmem] * len(args) + [pl.BlockSpec(memory...  20.2 us
    ppermute x9, starting transfers between devices, hopped(): lax.ppermute(value, 'tp', [(i, i ^ 2 * hop) for i in range(tp)])  11.1 us
    ppermute x9, waiting for transfers between devices, hopped(): lax.ppermute(value, 'tp', [(i, i ^ 2 * hop) for i in range(tp)])  10.9 us
    ppermute x3, waiting for transfers between devices, split_device(): lax.ppermute(a, 'tp', [(i, i ^ 2 * hop + 2) for i in range(tp)])  8.88 us
    ppermute x6, waiting for transfers between devices, collected(): lax.ppermute(part, 'tp', [(i, i ^ 2 * hop + 2) for i in range(tp)])  7.94 us
    ppermute x6, starting transfers between devices, collected(): lax.ppermute(part, 'tp', [(i, i ^ 2 * hop + 2) for i in range(tp)])  7.62 us
    ppermute x3, starting transfers between devices, split_device(): lax.ppermute(kv, 'sp', [(i, i ^ hop if even else (i + hop) % sp) for i in...  7.43 us
    all_to_all x1, starting transfers between devices, split_device(): lax.all_to_all(modulation, ('sp', 'tp'), 0, 0, axis_index_groups=columns)  6.35 us
  transfers between devices with their start and end apart: 36, of which 19 were waited for; matrix products, arithmetic and copies ran while one was open for 0% of the time, Pallas kernels for 10%

profile of v5, /device:TPU:0, one launch (start us, length us, event | category | flops | bytes accessed | tf_op | source)
XLA Modules:
  0.0 91.6 jit_solution(16741438945554999879)
XLA Ops:
  0.0 2.5 %shard_map.154 = (f32[8,1,1280]{2,1,0:T(1,128)}, bf16[512,256]{1,0:T(8,128)(2,1)S(1)}, bf16[272,512]{1,0:T(8,128)(2,1)S(1)}, bf16[272,512]{1,0:T(8,128)(2,1)S(1)}) custom-call(bf16[384,256]{1,0:T(8,128)(2,1)} %latent_ref.1, bf16[128,256]{1,0:T(8,128)(2,1)} %ctx_ref.1, bf16[512]{0:T(512)(128)(2,1)} %cond_ref.1, bf16[512]{0:T(512)(128)(2,1)} %cond_ctx_ref.1, ...), custom_call_target="tpu_custom_call" | custom-call | flops 1000000 | bytes 100000 | tf_op jit(solution)/shard_map/pallas_call | solution.py:205
  2.5 0.5 collective-permute-start
  3.0 6.4 %all-to-all-start = ((f32[8,1,1280]{2,1,0:T(1,128)}), f32[8,1,1280]{2,1,0:T(1,128)S(1)}, u32[]{:S(2)}, u32[]{:S(2)}) async-start(f32[8,1,1280]{2,1,0:T(1,128)} %get-tuple-element.50), calls=%async_computation | async-start | bytes 81920 | tf_op jit(solution)/shard_map/all_to_all | solution.py:693
  9.4 0.9 %shard_map.155.refs_0_ = f32[8,512]{1,0:T(8,128)S(1)} custom-call(bf16[512,256]{1,0:T(8,128)(2,1)S(1)} %get-tuple-element.49.own_ref, bf16[512,256]{1,0:T(8,128)(2,1)S(1)} %collective-permute-done.other_ref), custom_call_target="tpu_custom_call" | custom-call | flops 1000000 | bytes 100000 | tf_op jit(solution)/shard_map/pallas_call | solution.py:205
  10.3 2.5 %collective-permute-start.4 = (f32[8,512]{1,0:T(8,128)S(1)}, f32[8,512]{1,0:T(8,128)S(1)}, u32[]{:S(2)}, u32[]{:S(2)}) collective-permute-start(f32[8,512]{1,0:T(8,128)S(1)} %shard_map.155.refs_0_), channel_id=1, source_target_pairs={{0,6},{1,7},{2,4},{3,5},{4,2},{5,3},{6,0},{7,1},{8,14},{9,15},{10,... | collective-permute-start | bytes 49160 | tf_op jit(solution)/shard_map/ppermute | solution.py:666
  12.8 0.5 collective-permute-start.3
  13.3 0.5 collective-permute-start.2
  13.8 1.3 %all-to-all-done.mod_ref = f32[8,1,1280]{2,1,0:T(1,128)S(1)} async-done(((f32[8,1,1280]{2,1,0:T(1,128)}), f32[8,1,1280]{2,1,0:T(1,128)S(1)}, u32[]{:S(2)}, u32[]{:S(2)}) %all-to-all-start) | async-done | bytes 40992 | tf_op jit(solution)/shard_map/all_to_all | solution.py:693
  15.1 1.3 %collective-permute-done.3.refs_2_ = f32[8,512]{1,0:T(8,128)S(1)} collective-permute-done((f32[8,512]{1,0:T(8,128)S(1)}, f32[8,512]{1,0:T(8,128)S(1)}, u32[]{:S(2)}, u32[]{:S(2)}) %collective-permute-start.3) | collective-permute-done | bytes 16416 | tf_op jit(solution)/shard_map/ppermute | solution.py:666
  16.5 0.6 collective-permute-done.2.refs_1_
  17.1 1.6 %shard_map.156 = (f32[2,144,128]{2,1,0:T(8,128)S(1)}, f32[2,144,128]{2,1,0:T(8,128)S(1)}, f32[2,144,128]{2,1,0:T(8,128)S(1)}, f32[2,144,128]{2,1,0:T(8,128)S(1)}...) custom-call(bf16[512,256]{1,0:T(8,128)(2,1)S(1)} %get-tuple-element., ...), custom_call_target="tpu_custom_call" | custom-call | flops 335544320 | bytes 100000 | tf_op jit(solution)/shard_map/pallas_call | solution.py:205
  18.7 0.2 shard_map.159
  18.9 0.1 collective-permute-start.8
  19.0 0.6 collective-permute-start.10
  19.6 1.5 %collective-permute-start.11 = (f32[2,144,128]{2,1,0:T(8,128)S(1)}, f32[2,144,128]{2,1,0:T(8,128)S(1)}, u32[]{:S(2)}, u32[]{:S(2)}) collective-permute-start(f32[2,144,128]{2,1,0:T(8,128)S(1)} %get-tuple-element.77), channel_id=1, source_target_pairs={{0,4},{1,5},{2,6},{3,7},{4,0},{5,1},{6,2},{7,3},{8,12},{9,13},{10,... | collective-permute-start | bytes 442376 | tf_op jit(solution)/shard_map/ppermute | solution.py:721
  21.1 1.4 %collective-permute-start.12 = (f32[2,144,128]{2,1,0:T(8,128)S(1)}, f32[2,144,128]{2,1,0:T(8,128)S(1)}, u32[]{:S(2)}, u32[]{:S(2)}) collective-permute-start(f32[2,144,128]{2,1,0:T(8,128)S(1)} %get-tuple-element.78), channel_id=1, source_target_pairs={{0,6},{1,7},{2,4},{3,5},{4,2},{5,3},{6,0},{7,1},{8,14},{9,15},{10,... | collective-permute-start | bytes 442376 | tf_op jit(solution)/shard_map/ppermute | solution.py:721
  22.5 3.2 %collective-permute-done.10.refs_1_ = f32[2,144,128]{2,1,0:T(8,128)S(1)} collective-permute-done((f32[2,144,128]{2,1,0:T(8,128)S(1)}, f32[2,144,128]{2,1,0:T(8,128)S(1)}, u32[]{:S(2)}, u32[]{:S(2)}) %collective-permute-start.10) | collective-permute-done | bytes 147488 | tf_op jit(solution)/shard_map/ppermute | solution.py:721
  25.8 2.0 %collective-permute-done.11.refs_2_ = f32[2,144,128]{2,1,0:T(8,128)S(1)} collective-permute-done((f32[2,144,128]{2,1,0:T(8,128)S(1)}, f32[2,144,128]{2,1,0:T(8,128)S(1)}, u32[]{:S(2)}, u32[]{:S(2)}) %collective-permute-start.11) | collective-permute-done | bytes 147488 | tf_op jit(solution)/shard_map/ppermute | solution.py:721
  27.7 1.6 %collective-permute-done.12.refs_3_ = f32[2,144,128]{2,1,0:T(8,128)S(1)} collective-permute-done((f32[2,144,128]{2,1,0:T(8,128)S(1)}, f32[2,144,128]{2,1,0:T(8,128)S(1)}, u32[]{:S(2)}, u32[]{:S(2)}) %collective-permute-start.12) | collective-permute-done | bytes 147488 | tf_op jit(solution)/shard_map/ppermute | solution.py:721
  29.4 0.1 collective-permute-start.13
  29.5 0.9 shard_map.157.tab_ref
  30.4 0.4 collective-permute-done.13.other_ref
  30.7 0.3 shard_map.162.kv_ref
  31.0 3.9 %collective-permute-start.23 = (bf16[72,512]{1,0:T(8,128)(2,1)S(1)}, bf16[72,512]{1,0:T(8,128)(2,1)S(1)}, u32[]{:S(2)}, u32[]{:S(2)}) collective-permute-start(bf16[72,512]{1,0:T(8,128)(2,1)S(1)} %shard_map.162.kv_ref), channel_id=1, source_target_pairs={{0,24},{8,16},{16,8},{24,0},{1,25},{9,17},{17,9},{25,1},{2,26},{10... | collective-permute-start | bytes 221192 | tf_op jit(solution)/shard_map/ppermute | solution.py:756
  34.9 0.8 collective-permute-start.5
  35.7 1.5 %collective-permute-start.6 = (f32[2,96,128]{2,1,0:T(8,128)S(1)}, f32[2,96,128]{2,1,0:T(8,128)S(1)}, u32[]{:S(2)}, u32[]{:S(2)}) collective-permute-start(f32[2,96,128]{2,1,0:T(8,128)S(1)} %get-tuple-element.66), channel_id=1, source_target_pairs={{0,4},{1,5},{2,6},{3,7},{4,0},{5,1},{6,2},{7,3},{8,12},{9,13},{10,... | collective-permute-start | bytes 294920 | tf_op jit(solution)/shard_map/ppermute | solution.py:721
  37.2 0.5 collective-permute-done.23.refs_2_
  37.8 3.6 %collective-permute-start.21 = (bf16[72,512]{1,0:T(8,128)(2,1)S(1)}, bf16[72,512]{1,0:T(8,128)(2,1)S(1)}, u32[]{:S(2)}, u32[]{:S(2)}) collective-permute-start(bf16[72,512]{1,0:T(8,128)(2,1)S(1)} %shard_map.162.kv_ref), channel_id=1, source_target_pairs={{0,8},{8,0},{16,24},{24,16},{1,9},{9,1},{17,25},{25,17},{2,10},{10... | collective-permute-start | bytes 221192 | tf_op jit(solution)/shard_map/ppermute | solution.py:756
  41.3 0.4 collective-permute-done.22.refs_1_
  41.7 1.8 %collective-permute-start.7 = (f32[2,96,128]{2,1,0:T(8,128)S(1)}, f32[2,96,128]{2,1,0:T(8,128)S(1)}, u32[]{:S(2)}, u32[]{:S(2)}) collective-permute-start(f32[2,96,128]{2,1,0:T(8,128)S(1)} %get-tuple-element.67), channel_id=1, source_target_pairs={{0,6},{1,7},{2,4},{3,5},{4,2},{5,3},{6,0},{7,1},{8,14},{9,15},{10,... | collective-permute-start | bytes 294920 | tf_op jit(solution)/shard_map/ppermute | solution.py:721
  43.4 0.2 collective-permute-done.21.refs_0_
  43.7 1.8 %collective-permute-start.27 = (bf16[216,512]{1,0:T(8,128)(2,1)S(1)}, bf16[216,512]{1,0:T(8,128)(2,1)S(1)}, u32[]{:S(2)}, u32[]{:S(2)}) collective-permute-start(bf16[216,512]{1,0:T(8,128)(2,1)S(1)} %shard_map.164.refs_8_), channel_id=1, source_target_pairs={{0,6},{1,7},{2,4},{3,5},{4,2},{5,3},{6,0},{7,1},{8,14},{9,15},{10,... | collective-permute-start | bytes 663560 | tf_op jit(solution)/shard_map/ppermute | solution.py:666
  45.5 0.5 collective-permute-start.26
  46.0 1.2 %collective-permute-start.25 = (bf16[216,512]{1,0:T(8,128)(2,1)S(1)}, bf16[216,512]{1,0:T(8,128)(2,1)S(1)}, u32[]{:S(2)}, u32[]{:S(2)}) collective-permute-start(bf16[216,512]{1,0:T(8,128)(2,1)S(1)} %shard_map.164.refs_8_), channel_id=1, source_target_pairs={{0,2},{1,3},{2,0},{3,1},{4,6},{5,7},{6,4},{7,5},{8,10},{9,11},{10,... | collective-permute-start | bytes 663560 | tf_op jit(solution)/shard_map/ppermute | solution.py:666
  47.2 1.1 %collective-permute-done.7.refs_3_ = f32[2,96,128]{2,1,0:T(8,128)S(1)} collective-permute-done((f32[2,96,128]{2,1,0:T(8,128)S(1)}, f32[2,96,128]{2,1,0:T(8,128)S(1)}, u32[]{:S(2)}, u32[]{:S(2)}) %collective-permute-start.7) | collective-permute-done | bytes 98336 | tf_op jit(solution)/shard_map/ppermute | solution.py:721
  48.4 0.1 collective-permute-start.9
  48.5 1.2 %collective-permute-done.9.other_ref = f32[96,128]{1,0:T(8,128)S(1)} collective-permute-done((f32[96,128]{1,0:T(8,128)S(1)}, f32[96,128]{1,0:T(8,128)S(1)}, u32[]{:S(2)}, u32[]{:S(2)}) %collective-permute-start.9) | collective-permute-done | bytes 49184 | tf_op jit(solution)/shard_map/ppermute | solution.py:728
  49.7 0.1 shard_map.163.refs_0_
  49.8 1.8 %collective-permute-start.16 = (bf16[120,512]{1,0:T(8,128)(2,1)S(1)}, bf16[120,512]{1,0:T(8,128)(2,1)S(1)}, u32[]{:S(2)}, u32[]{:S(2)}) collective-permute-start(bf16[120,512]{1,0:T(8,128)(2,1)S(1)} %shard_map.163.refs_0_), channel_id=1, source_target_pairs={{0,6},{1,7},{2,4},{3,5},{4,2},{5,3},{6,0},{7,1},{8,14},{9,15},{10,... | collective-permute-start | bytes 368648 | tf_op jit(solution)/shard_map/ppermute | solution.py:666
  51.6 1.4 %collective-permute-done.27.refs_2_ = bf16[216,512]{1,0:T(8,128)(2,1)S(1)} collective-permute-done((bf16[216,512]{1,0:T(8,128)(2,1)S(1)}, bf16[216,512]{1,0:T(8,128)(2,1)S(1)}, u32[]{:S(2)}, u32[]{:S(2)}) %collective-permute-start.27) | collective-permute-done | bytes 221216 | tf_op jit(solution)/shard_map/ppermute | solution.py:666
  53.0 4.6 %collective-permute-done.26.refs_1_ = bf16[216,512]{1,0:T(8,128)(2,1)S(1)} collective-permute-done((bf16[216,512]{1,0:T(8,128)(2,1)S(1)}, bf16[216,512]{1,0:T(8,128)(2,1)S(1)}, u32[]{:S(2)}, u32[]{:S(2)}) %collective-permute-start.26) | collective-permute-done | bytes 221216 | tf_op jit(solution)/shard_map/ppermute | solution.py:666
  57.7 0.8 collective-permute-start.15
  58.5 1.5 %collective-permute-start.14 = (bf16[120,512]{1,0:T(8,128)(2,1)S(1)}, bf16[120,512]{1,0:T(8,128)(2,1)S(1)}, u32[]{:S(2)}, u32[]{:S(2)}) collective-permute-start(bf16[120,512]{1,0:T(8,128)(2,1)S(1)} %shard_map.163.refs_0_), channel_id=1, source_target_pairs={{0,2},{1,3},{2,0},{3,1},{4,6},{5,7},{6,4},{7,5},{8,10},{9,11},{10,... | collective-permute-start | bytes 368648 | tf_op jit(solution)/shard_map/ppermute | solution.py:666
  60.0 0.5 collective-permute-start.30
  60.5 0.1 collective-permute-start.29
  60.6 2.3 %collective-permute-done.15.refs_2_ = bf16[120,512]{1,0:T(8,128)(2,1)S(1)} collective-permute-done((bf16[120,512]{1,0:T(8,128)(2,1)S(1)}, bf16[120,512]{1,0:T(8,128)(2,1)S(1)}, u32[]{:S(2)}, u32[]{:S(2)}) %collective-permute-start.15) | collective-permute-done | bytes 122912 | tf_op jit(solution)/shard_map/ppermute | solution.py:666
  62.8 0.5 collective-permute-done.14.refs_1_
  63.4 0.5 collective-permute-start.18
  63.9 1.6 %shard_map.158.wkv_ref.w_ref = bf16[512,1024]{1,0:T(8,128)(2,1)S(1)} custom-call(bf16[512,4,256]{2,1,0:T(4,128)(2,1)S(1)} %copy-done.4), custom_call_target="tpu_custom_call" | custom-call | flops 1000000000 | bytes 100000 | tf_op jit(solution)/shard_map/pallas_call | solution.py:205
  65.6 0.8 shard_map.166
  66.4 0.1 broadcast_in_dim.12.lift_ref
  66.5 0.2 copy-done.5
  66.7 4.0 %shard_map.165 = (bf16[4,384,256]{2,1,0:T(8,128)(2,1)S(1)}, f32[384,128]{1,0:T(8,128)S(1)}, f32[4,384,128]{2,1,0:T(8,128)S(1)}) custom-call(f32[384,128]{1,0:T(8,128)S(1)} %shard_map.157.tab_ref, f32[4,128]{1,0:T(4,128)S(1)} %broadcast_in_dim.12.lift_ref, bf16[4,192,512]{2,1,0:T(8,128)(2,1)S(1)} %bitcast.10, bf16[512,1024]{1,0:T(8,128)(2,1)S(1)} %shard_map.158.wkv_ref.w_ref, ...), custom_call_target="tpu_custom_call" | custom-call | flops 1459617792 | bytes 100000 | tf_op jit(solution)/shard_map/pallas_call | solution.py:205
  70.7 5.3 %shard_map.167 = (bf16[384,512]{1,0:T(8,128)(2,1)S(1)}, bf16[4,512,256]{2,1,0:T(8,128)(2,1)S(1)}) custom-call(bf16[4,384,256]{2,1,0:T(8,128)(2,1)S(1)} %get-tuple-element.81.query_ref, f32[384,128]{1,0:T(8,128)S(1)} %get-tuple-element.82.stat_ref, f32[4,384,128]{2,1,0:T(8,128)S(1)} %get-tuple-element.83.sum_ref, ...), custom_call_target="tpu_custom_call" | custom-call | flops 1962934272 | bytes 100000 | tf_op jit(solution)/shard_map/pallas_call | solution.py:205
  76.0 0.1 collective-permute-start.31
  76.1 0.6 shard_map.168.acc_ref
  76.7 1.1 %collective-permute-done.31.heads_ref = bf16[384,512]{1,0:T(8,128)(2,1)S(1)} collective-permute-done((bf16[384,512]{1,0:T(8,128)(2,1)S(1)}, bf16[384,512]{1,0:T(8,128)(2,1)S(1)}, u32[]{:S(2)}, u32[]{:S(2)}) %collective-permute-start.31) | collective-permute-done | bytes 393248 | tf_op jit(solution)/shard_map/ppermute | solution.py:816
  77.8 0.6 shard_map.169
  78.4 1.6 %collective-permute-start.32 = (bf16[384,256]{1,0:T(8,128)(2,1)S(1)}, bf16[384,256]{1,0:T(8,128)(2,1)S(1)}, u32[]{:S(2)}, u32[]{:S(2)}) collective-permute-start(bf16[384,256]{1,0:T(8,128)(2,1)S(1)} %get-tuple-element.90), channel_id=1, source_target_pairs={{0,2},{1,3},{2,0},{3,1},{4,6},{5,7},{6,4},{7,5},{8,10},{9,11},{10,... | collective-permute-start | bytes 589832 | tf_op jit(solution)/shard_map/ppermute | solution.py:831
  79.9 0.5 collective-permute-start.33
  80.4 1.5 %collective-permute-start.34 = (bf16[384,256]{1,0:T(8,128)(2,1)S(1)}, bf16[384,256]{1,0:T(8,128)(2,1)S(1)}, u32[]{:S(2)}, u32[]{:S(2)}) collective-permute-start(bf16[384,256]{1,0:T(8,128)(2,1)S(1)} %get-tuple-element.92), channel_id=1, source_target_pairs={{0,6},{1,7},{2,4},{3,5},{4,2},{5,3},{6,0},{7,1},{8,14},{9,15},{10,... | collective-permute-start | bytes 589832 | tf_op jit(solution)/shard_map/ppermute | solution.py:831
  81.9 4.3 %collective-permute-done.32.refs_1_ = bf16[384,256]{1,0:T(8,128)(2,1)S(1)} collective-permute-done((bf16[384,256]{1,0:T(8,128)(2,1)S(1)}, bf16[384,256]{1,0:T(8,128)(2,1)S(1)}, u32[]{:S(2)}, u32[]{:S(2)}) %collective-permute-start.32) | collective-permute-done | bytes 196640 | tf_op jit(solution)/shard_map/ppermute | solution.py:831
  86.2 4.6 %collective-permute-done.33.refs_2_ = bf16[384,256]{1,0:T(8,128)(2,1)S(1)} collective-permute-done((bf16[384,256]{1,0:T(8,128)(2,1)S(1)}, bf16[384,256]{1,0:T(8,128)(2,1)S(1)}, u32[]{:S(2)}, u32[]{:S(2)}) %collective-permute-start.33) | collective-permute-done | bytes 196640 | tf_op jit(solution)/shard_map/ppermute | solution.py:831
  90.8 0.8 shard_map.170
  (43 shorter events, 0.2 us)
Async XLA Ops:
  0.0 18.7 %copy-start = (bf16[4,128,2048]{2,1,0:T(8,128)(2,1)S(1)}, bf16[4,128,2048]{2,1,0:T(8,128)(2,1)}, u32[]{:S(2)}) copy-start(bf16[4,128,2048]{2,1,0:T(8,128)(2,1)} %param.30) | copy-start | bytes 6291460
  2.5 6.9 %collective-permute-start = (bf16[512,256]{1,0:T(8,128)(2,1)S(1)}, bf16[512,256]{1,0:T(8,128)(2,1)S(1)}, u32[]{:S(2)}, u32[]{:S(2)}) collective-permute-start(bf16[512,256]{1,0:T(8,128)(2,1)S(1)} %get-tuple-element.49.own_ref), channel_id=1, source_target_pairs={{0,1},{1,0},{2,3},{3,2},{4,5},{5,4},{6,7},{7,6},{8,9},{9,8},{10,11... | collective-permute-start | bytes 786440 | tf_op jit(solution)/shard_map/ppermute | solution.py:691
  3.0 14.1 %collective-permute-start.1 = (bf16[272,512]{1,0:T(8,128)(2,1)S(1)}, bf16[272,512]{1,0:T(8,128)(2,1)S(1)}, u32[]{:S(2)}, u32[]{:S(2)}) collective-permute-start(bf16[272,512]{1,0:T(8,128)(2,1)S(1)} %get-tuple-element.52), channel_id=1, source_target_pairs={{0,1},{1,0},{2,3},{3,2},{4,5},{5,4},{6,7},{7,6},{8,9},{9,8},{10,11... | collective-permute-start | bytes 835592 | tf_op jit(solution)/shard_map/ppermute | solution.py:690
  3.0 12.1 %all-to-all-start = ((f32[8,1,1280]{2,1,0:T(1,128)}), f32[8,1,1280]{2,1,0:T(1,128)S(1)}, u32[]{:S(2)}, u32[]{:S(2)}) async-start(f32[8,1,1280]{2,1,0:T(1,128)} %get-tuple-element.50), calls=%async_computation | async-start | bytes 81920 | tf_op jit(solution)/shard_map/all_to_all | solution.py:693
  10.3 4.9 %collective-permute-start.4 = (f32[8,512]{1,0:T(8,128)S(1)}, f32[8,512]{1,0:T(8,128)S(1)}, u32[]{:S(2)}, u32[]{:S(2)}) collective-permute-start(f32[8,512]{1,0:T(8,128)S(1)} %shard_map.155.refs_0_), channel_id=1, source_target_pairs={{0,6},{1,7},{2,4},{3,5},{4,2},{5,3},{6,0},{7,1},{8,14},{9,15},{10,... | collective-permute-start | bytes 49160 | tf_op jit(solution)/shard_map/ppermute | solution.py:666
  12.8 3.7 %collective-permute-start.3 = (f32[8,512]{1,0:T(8,128)S(1)}, f32[8,512]{1,0:T(8,128)S(1)}, u32[]{:S(2)}, u32[]{:S(2)}) collective-permute-start(f32[8,512]{1,0:T(8,128)S(1)} %shard_map.155.refs_0_), channel_id=1, source_target_pairs={{0,4},{1,5},{2,6},{3,7},{4,0},{5,1},{6,2},{7,3},{8,12},{9,13},{10,... | collective-permute-start | bytes 49160 | tf_op jit(solution)/shard_map/ppermute | solution.py:666
  13.3 3.8 %collective-permute-start.2 = (f32[8,512]{1,0:T(8,128)S(1)}, f32[8,512]{1,0:T(8,128)}, u32[]{:S(2)}, u32[]{:S(2)}) collective-permute-start(f32[8,512]{1,0:T(8,128)S(1)} %shard_map.155.refs_0_), channel_id=1, source_target_pairs={{0,2},{1,3},{2,0},{3,1},{4,6},{5,7},{6,4},{7,5},{8,10},{9,11},{10,... | collective-permute-start | bytes 49160 | tf_op jit(solution)/shard_map/ppermute | solution.py:666
  18.7 3.8 %copy-start.7 = (f32[1,128]{1,0:T(1,128)S(1)}, f32[1,128]{1,0:T(1,128)}, u32[]{:S(2)}) copy-start(f32[1,128]{1,0:T(1,128)} %constant.4.clone) | copy-start | bytes 1540
  18.9 29.5 %collective-permute-start.8 = (bf16[4,512,256]{2,1,0:T(8,128)(2,1)S(1)}, bf16[4,512,256]{2,1,0:T(8,128)(2,1)S(1)}, u32[]{:S(2)}, u32[]{:S(2)}) collective-permute-start(bf16[4,512,256]{2,1,0:T(8,128)(2,1)S(1)} %shard_map.159), channel_id=1, source_target_pairs={{0,1},{1,0},{2,3},{3,2},{4,5},{5,4},{6,7},{7,6},{8,9},{9,8},{10,11... | collective-permute-start | bytes 3145736 | tf_op jit(solution)/shard_map/ppermute | solution.py:742
  19.0 6.8 %collective-permute-start.10 = (f32[2,144,128]{2,1,0:T(8,128)S(1)}, f32[2,144,128]{2,1,0:T(8,128)S(1)}, u32[]{:S(2)}, u32[]{:S(2)}) collective-permute-start(f32[2,144,128]{2,1,0:T(8,128)S(1)} %get-tuple-element.76), channel_id=1, source_target_pairs={{0,2},{1,3},{2,0},{3,1},{4,6},{5,7},{6,4},{7,5},{8,10},{9,11},{10,... | collective-permute-start | bytes 442376 | tf_op jit(solution)/shard_map/ppermute | solution.py:721
  19.6 8.1 %collective-permute-start.11 = (f32[2,144,128]{2,1,0:T(8,128)S(1)}, f32[2,144,128]{2,1,0:T(8,128)S(1)}, u32[]{:S(2)}, u32[]{:S(2)}) collective-permute-start(f32[2,144,128]{2,1,0:T(8,128)S(1)} %get-tuple-element.77), channel_id=1, source_target_pairs={{0,4},{1,5},{2,6},{3,7},{4,0},{5,1},{6,2},{7,3},{8,12},{9,13},{10,... | collective-permute-start | bytes 442376 | tf_op jit(solution)/shard_map/ppermute | solution.py:721
  21.1 8.2 %collective-permute-start.12 = (f32[2,144,128]{2,1,0:T(8,128)S(1)}, f32[2,144,128]{2,1,0:T(8,128)S(1)}, u32[]{:S(2)}, u32[]{:S(2)}) collective-permute-start(f32[2,144,128]{2,1,0:T(8,128)S(1)} %get-tuple-element.78), channel_id=1, source_target_pairs={{0,6},{1,7},{2,4},{3,5},{4,2},{5,3},{6,0},{7,1},{8,14},{9,15},{10,... | collective-permute-start | bytes 442376 | tf_op jit(solution)/shard_map/ppermute | solution.py:721
  29.4 1.4 %copy-start.2 = (f32[512]{0:T(512)S(1)}, f32[512]{0:T(512)}, u32[]{:S(2)}) copy-start(f32[512]{0:T(512)} %param.26) | copy-start | bytes 6148
  29.4 20.3 %copy-start.3 = (f32[512]{0:T(512)S(1)}, f32[512]{0:T(512)}, u32[]{:S(2)}) copy-start(f32[512]{0:T(512)} %param.25) | copy-start | bytes 6148
  29.4 34.5 %copy-start.4 = (bf16[512,4,256]{2,1,0:T(4,128)(2,1)S(1)}, bf16[512,4,256]{2,1,0:T(4,128)(2,1)}, u32[]{:S(2)}) copy-start(bf16[512,4,256]{2,1,0:T(4,128)(2,1)} %w_ref) | copy-start | bytes 3145732
  29.4 1.3 %collective-permute-start.13 = (f32[144,128]{1,0:T(8,128)S(1)}, f32[144,128]{1,0:T(8,128)S(1)}, u32[]{:S(2)}, u32[]{:S(2)}) collective-permute-start(f32[144,128]{1,0:T(8,128)S(1)} %get-tuple-element.80), channel_id=1, source_target_pairs={{0,1},{1,0},{2,3},{3,2},{4,5},{5,4},{6,7},{7,6},{8,9},{9,8},{10,11... | collective-permute-start | bytes 221192 | tf_op jit(solution)/shard_map/ppermute | solution.py:728
  31.0 6.7 %collective-permute-start.23 = (bf16[72,512]{1,0:T(8,128)(2,1)S(1)}, bf16[72,512]{1,0:T(8,128)(2,1)S(1)}, u32[]{:S(2)}, u32[]{:S(2)}) collective-permute-start(bf16[72,512]{1,0:T(8,128)(2,1)S(1)} %shard_map.162.kv_ref), channel_id=1, source_target_pairs={{0,24},{8,16},{16,8},{24,0},{1,25},{9,17},{17,9},{25,1},{2,26},{10... | collective-permute-start | bytes 221192 | tf_op jit(solution)/shard_map/ppermute | solution.py:756
  34.9 6.8 %collective-permute-start.22 = (bf16[72,512]{1,0:T(8,128)(2,1)S(1)}, bf16[72,512]{1,0:T(8,128)(2,1)S(1)}, u32[]{:S(2)}, u32[]{:S(2)}) collective-permute-start(bf16[72,512]{1,0:T(8,128)(2,1)S(1)} %shard_map.162.kv_ref), channel_id=1, source_target_pairs={{0,16},{8,24},{16,0},{24,8},{1,17},{9,25},{17,1},{25,9},{2,18},{10... | collective-permute-start | bytes 221192 | tf_op jit(solution)/shard_map/ppermute | solution.py:756
  34.9 10.6 %collective-permute-start.5 = (f32[2,96,128]{2,1,0:T(8,128)S(1)}, f32[2,96,128]{2,1,0:T(8,128)S(1)}, u32[]{:S(2)}, u32[]{:S(2)}) collective-permute-start(f32[2,96,128]{2,1,0:T(8,128)S(1)} %get-tuple-element.65), channel_id=1, source_target_pairs={{0,2},{1,3},{2,0},{3,1},{4,6},{5,7},{6,4},{7,5},{8,10},{9,11},{10,... | collective-permute-start | bytes 294920 | tf_op jit(solution)/shard_map/ppermute | solution.py:721
  35.7 10.3 %collective-permute-start.6 = (f32[2,96,128]{2,1,0:T(8,128)S(1)}, f32[2,96,128]{2,1,0:T(8,128)S(1)}, u32[]{:S(2)}, u32[]{:S(2)}) collective-permute-start(f32[2,96,128]{2,1,0:T(8,128)S(1)} %get-tuple-element.66), channel_id=1, source_target_pairs={{0,4},{1,5},{2,6},{3,7},{4,0},{5,1},{6,2},{7,3},{8,12},{9,13},{10,... | collective-permute-start | bytes 294920 | tf_op jit(solution)/shard_map/ppermute | solution.py:721
  37.8 5.9 %collective-permute-start.21 = (bf16[72,512]{1,0:T(8,128)(2,1)S(1)}, bf16[72,512]{1,0:T(8,128)(2,1)S(1)}, u32[]{:S(2)}, u32[]{:S(2)}) collective-permute-start(bf16[72,512]{1,0:T(8,128)(2,1)S(1)} %shard_map.162.kv_ref), channel_id=1, source_target_pairs={{0,8},{8,0},{16,24},{24,16},{1,9},{9,1},{17,25},{25,17},{2,10},{10... | collective-permute-start | bytes 221192 | tf_op jit(solution)/shard_map/ppermute | solution.py:756
  41.7 6.7 %collective-permute-start.7 = (f32[2,96,128]{2,1,0:T(8,128)S(1)}, f32[2,96,128]{2,1,0:T(8,128)S(1)}, u32[]{:S(2)}, u32[]{:S(2)}) collective-permute-start(f32[2,96,128]{2,1,0:T(8,128)S(1)} %get-tuple-element.67), channel_id=1, source_target_pairs={{0,6},{1,7},{2,4},{3,5},{4,2},{5,3},{6,0},{7,1},{8,14},{9,15},{10,... | collective-permute-start | bytes 294920 | tf_op jit(solution)/shard_map/ppermute | solution.py:721
  43.7 9.4 %collective-permute-start.27 = (bf16[216,512]{1,0:T(8,128)(2,1)S(1)}, bf16[216,512]{1,0:T(8,128)(2,1)S(1)}, u32[]{:S(2)}, u32[]{:S(2)}) collective-permute-start(bf16[216,512]{1,0:T(8,128)(2,1)S(1)} %shard_map.164.refs_8_), channel_id=1, source_target_pairs={{0,6},{1,7},{2,4},{3,5},{4,2},{5,3},{6,0},{7,1},{8,14},{9,15},{10,... | collective-permute-start | bytes 663560 | tf_op jit(solution)/shard_map/ppermute | solution.py:666
  45.5 12.2 %collective-permute-start.26 = (bf16[216,512]{1,0:T(8,128)(2,1)S(1)}, bf16[216,512]{1,0:T(8,128)(2,1)S(1)}, u32[]{:S(2)}, u32[]{:S(2)}) collective-permute-start(bf16[216,512]{1,0:T(8,128)(2,1)S(1)} %shard_map.164.refs_8_), channel_id=1, source_target_pairs={{0,4},{1,5},{2,6},{3,7},{4,0},{5,1},{6,2},{7,3},{8,12},{9,13},{10,... | collective-permute-start | bytes 663560 | tf_op jit(solution)/shard_map/ppermute | solution.py:666
  46.0 12.5 %collective-permute-start.25 = (bf16[216,512]{1,0:T(8,128)(2,1)S(1)}, bf16[216,512]{1,0:T(8,128)(2,1)S(1)}, u32[]{:S(2)}, u32[]{:S(2)}) collective-permute-start(bf16[216,512]{1,0:T(8,128)(2,1)S(1)} %shard_map.164.refs_8_), channel_id=1, source_target_pairs={{0,2},{1,3},{2,0},{3,1},{4,6},{5,7},{6,4},{7,5},{8,10},{9,11},{10,... | collective-permute-start | bytes 663560 | tf_op jit(solution)/shard_map/ppermute | solution.py:666
  48.4 1.3 %collective-permute-start.9 = (f32[96,128]{1,0:T(8,128)S(1)}, f32[96,128]{1,0:T(8,128)S(1)}, u32[]{:S(2)}, u32[]{:S(2)}) collective-permute-start(f32[96,128]{1,0:T(8,128)S(1)} %get-tuple-element.74), channel_id=1, source_target_pairs={{0,1},{1,0},{2,3},{3,2},{4,5},{5,4},{6,7},{7,6},{8,9},{9,8},{10,11... | collective-permute-start | bytes 147464 | tf_op jit(solution)/shard_map/ppermute | solution.py:728
  49.8 10.2 %collective-permute-start.16 = (bf16[120,512]{1,0:T(8,128)(2,1)S(1)}, bf16[120,512]{1,0:T(8,128)(2,1)S(1)}, u32[]{:S(2)}, u32[]{:S(2)}) collective-permute-start(bf16[120,512]{1,0:T(8,128)(2,1)S(1)} %shard_map.163.refs_0_), channel_id=1, source_target_pairs={{0,6},{1,7},{2,4},{3,5},{4,2},{5,3},{6,0},{7,1},{8,14},{9,15},{10,... | collective-permute-start | bytes 368648 | tf_op jit(solution)/shard_map/ppermute | solution.py:666
  51.6 8.4 %collective-permute-start.24 = (bf16[216,512]{1,0:T(8,128)(2,1)S(1)}, bf16[216,512]{1,0:T(8,128)(2,1)S(1)}, u32[]{:S(2)}, u32[]{:S(2)}) collective-permute-start(bf16[216,512]{1,0:T(8,128)(2,1)S(1)} %shard_map.164.refs_8_), channel_id=1, source_target_pairs={{0,1},{1,0},{2,3},{3,2},{4,5},{5,4},{6,7},{7,6},{8,9},{9,8},{10,11... | collective-permute-start | bytes 663560 | tf_op jit(solution)/shard_map/ppermute | solution.py:764
  53.0 7.4 %collective-permute-start.17 = (bf16[120,512]{1,0:T(8,128)(2,1)S(1)}, bf16[120,512]{1,0:T(8,128)(2,1)S(1)}, u32[]{:S(2)}, u32[]{:S(2)}) collective-permute-start(bf16[120,512]{1,0:T(8,128)(2,1)S(1)} %shard_map.163.refs_0_), channel_id=1, source_target_pairs={{0,1},{1,0},{2,3},{3,2},{4,5},{5,4},{6,7},{7,6},{8,9},{9,8},{10,11... | collective-permute-start | bytes 368648 | tf_op jit(solution)/shard_map/ppermute | solution.py:761
  57.7 5.1 %collective-permute-start.15 = (bf16[120,512]{1,0:T(8,128)(2,1)S(1)}, bf16[120,512]{1,0:T(8,128)(2,1)S(1)}, u32[]{:S(2)}, u32[]{:S(2)}) collective-permute-start(bf16[120,512]{1,0:T(8,128)(2,1)S(1)} %shard_map.163.refs_0_), channel_id=1, source_target_pairs={{0,4},{1,5},{2,6},{3,7},{4,0},{5,1},{6,2},{7,3},{8,12},{9,13},{10,... | collective-permute-start | bytes 368648 | tf_op jit(solution)/shard_map/ppermute | solution.py:666
  58.5 4.9 %collective-permute-start.14 = (bf16[120,512]{1,0:T(8,128)(2,1)S(1)}, bf16[120,512]{1,0:T(8,128)(2,1)S(1)}, u32[]{:S(2)}, u32[]{:S(2)}) collective-permute-start(bf16[120,512]{1,0:T(8,128)(2,1)S(1)} %shard_map.163.refs_0_), channel_id=1, source_target_pairs={{0,2},{1,3},{2,0},{3,1},{4,6},{5,7},{6,4},{7,5},{8,10},{9,11},{10,... | collective-permute-start | bytes 368648 | tf_op jit(solution)/shard_map/ppermute | solution.py:666
  60.0 3.4 %collective-permute-start.20 = (bf16[120,512]{1,0:T(8,128)(2,1)S(1)}, bf16[120,512]{1,0:T(8,128)(2,1)S(1)}, u32[]{:S(2)}, u32[]{:S(2)}) collective-permute-start(bf16[120,512]{1,0:T(8,128)(2,1)S(1)} %collective-permute-done.16.refs_3_), channel_id=1, source_target_pairs={{0,1},{1,0},{2,3},{3,2},{4,5},{5,4},{6,7},{7,6},{8,9},{9,8},{10,11... | collective-permute-start | bytes 368648 | tf_op jit(solution)/shard_map/ppermute | solution.py:761
  60.0 10.7 %collective-permute-start.30 = (bf16[216,512]{1,0:T(8,128)(2,1)S(1)}, bf16[216,512]{1,0:T(8,128)(2,1)S(1)}, u32[]{:S(2)}, u32[]{:S(2)}) collective-permute-start(bf16[216,512]{1,0:T(8,128)(2,1)S(1)} %collective-permute-done.27.refs_2_), channel_id=1, source_target_pairs={{0,1},{1,0},{2,3},{3,2},{4,5},{5,4},{6,7},{7,6},{8,9},{9,8},{10,11... | collective-permute-start | bytes 663560 | tf_op jit(solution)/shard_map/ppermute | solution.py:764
  60.5 10.2 %collective-permute-start.29 = (bf16[216,512]{1,0:T(8,128)(2,1)S(1)}, bf16[216,512]{1,0:T(8,128)(2,1)S(1)}, u32[]{:S(2)}, u32[]{:S(2)}) collective-permute-start(bf16[216,512]{1,0:T(8,128)(2,1)S(1)} %collective-permute-done.26.refs_1_), channel_id=1, source_target_pairs={{0,1},{1,0},{2,3},{3,2},{4,5},{5,4},{6,7},{7,6},{8,9},{9,8},{10,11... | collective-permute-start | bytes 663560 | tf_op jit(solution)/shard_map/ppermute | solution.py:764
  62.8 7.8 %collective-permute-start.28 = (bf16[216,512]{1,0:T(8,128)(2,1)S(1)}, bf16[216,512]{1,0:T(8,128)(2,1)S(1)}, u32[]{:S(2)}, u32[]{:S(2)}) collective-permute-start(bf16[216,512]{1,0:T(8,128)(2,1)S(1)} %collective-permute-done.25.refs_0_), channel_id=1, source_target_pairs={{0,1},{1,0},{2,3},{3,2},{4,5},{5,4},{6,7},{7,6},{8,9},{9,8},{10,11... | collective-permute-start | bytes 663560 | tf_op jit(solution)/shard_map/ppermute | solution.py:764
  63.4 3.0 %collective-permute-start.19 = (bf16[120,512]{1,0:T(8,128)(2,1)S(1)}, bf16[120,512]{1,0:T(8,128)(2,1)S(1)}, u32[]{:S(2)}, u32[]{:S(2)}) collective-permute-start(bf16[120,512]{1,0:T(8,128)(2,1)S(1)} %collective-permute-done.15.refs_2_), channel_id=1, source_target_pairs={{0,1},{1,0},{2,3},{3,2},{4,5},{5,4},{6,7},{7,6},{8,9},{9,8},{10,11... | collective-permute-start | bytes 368648 | tf_op jit(solution)/shard_map/ppermute | solution.py:761
  63.4 3.0 %collective-permute-start.18 = (bf16[120,512]{1,0:T(8,128)(2,1)S(1)}, bf16[120,512]{1,0:T(8,128)(2,1)S(1)}, u32[]{:S(2)}, u32[]{:S(2)}) collective-permute-start(bf16[120,512]{1,0:T(8,128)(2,1)S(1)} %collective-permute-done.14.refs_1_), channel_id=1, source_target_pairs={{0,1},{1,0},{2,3},{3,2},{4,5},{5,4},{6,7},{7,6},{8,9},{9,8},{10,11... | collective-permute-start | bytes 368648 | tf_op jit(solution)/shard_map/ppermute | solution.py:761
  65.5 0.9 copy-start.6
  65.5 1.1 %copy-start.5 = (bf16[512,4,192]{0,2,1:T(8,128)(2,1)S(1)}, bf16[512,4,192]{0,2,1:T(8,128)(2,1)}, u32[]{:S(2)}) copy-start(bf16[512,4,192]{0,2,1:T(8,128)(2,1)} %param.27) | copy-start | bytes 2359300
  76.0 1.8 %collective-permute-start.31 = (bf16[384,512]{1,0:T(8,128)(2,1)S(1)}, bf16[384,512]{1,0:T(8,128)(2,1)S(1)}, u32[]{:S(2)}, u32[]{:S(2)}) collective-permute-start(bf16[384,512]{1,0:T(8,128)(2,1)S(1)} %get-tuple-element.87.heads_ref), channel_id=1, source_target_pairs={{0,1},{1,0},{2,3},{3,2},{4,5},{5,4},{6,7},{7,6},{8,9},{9,8},{10,11... | collective-permute-start | bytes 1179656 | tf_op jit(solution)/shard_map/ppermute | solution.py:816
  76.7 14.1 %copy-start.1 = (bf16[384,256]{1,0:T(8,128)(2,1)S(1)}, bf16[384,256]{1,0:T(8,128)(2,1)}, u32[]{:S(2)}) copy-start(bf16[384,256]{1,0:T(8,128)(2,1)} %latent_ref.1) | copy-start | bytes 589828
  78.4 7.8 %collective-permute-start.32 = (bf16[384,256]{1,0:T(8,128)(2,1)S(1)}, bf16[384,256]{1,0:T(8,128)(2,1)S(1)}, u32[]{:S(2)}, u32[]{:S(2)}) collective-permute-start(bf16[384,256]{1,0:T(8,128)(2,1)S(1)} %get-tuple-element.90), channel_id=1, source_target_pairs={{0,2},{1,3},{2,0},{3,1},{4,6},{5,7},{6,4},{7,5},{8,10},{9,11},{10,... | collective-permute-start | bytes 589832 | tf_op jit(solution)/shard_map/ppermute | solution.py:831
  79.9 10.9 %collective-permute-start.33 = (bf16[384,256]{1,0:T(8,128)(2,1)S(1)}, bf16[384,256]{1,0:T(8,128)(2,1)S(1)}, u32[]{:S(2)}, u32[]{:S(2)}) collective-permute-start(bf16[384,256]{1,0:T(8,128)(2,1)S(1)} %get-tuple-element.91), channel_id=1, source_target_pairs={{0,4},{1,5},{2,6},{3,7},{4,0},{5,1},{6,2},{7,3},{8,12},{9,13},{10,... | collective-permute-start | bytes 589832 | tf_op jit(solution)/shard_map/ppermute | solution.py:831
  80.4 10.4 %collective-permute-start.34 = (bf16[384,256]{1,0:T(8,128)(2,1)S(1)}, bf16[384,256]{1,0:T(8,128)(2,1)S(1)}, u32[]{:S(2)}, u32[]{:S(2)}) collective-permute-start(bf16[384,256]{1,0:T(8,128)(2,1)S(1)} %get-tuple-element.92), channel_id=1, source_target_pairs={{0,6},{1,7},{2,4},{3,5},{4,2},{5,3},{6,0},{7,1},{8,14},{9,15},{10,... | collective-permute-start | bytes 589832 | tf_op jit(solution)/shard_map/ppermute | solution.py:831

commit v6 on v5

--- a/solution.py
+++ b/solution.py
@@ -569,24 +569,20 @@
         def score():
             pairs = expanded(kv_ref, w_ref, head)
             keys = jnp.concatenate([pairs[:, :NOPE], rot_ref[...]], axis=1)
-            held[head] = (keys, pairs[:, NOPE:])
-            query = query_ref[head]
-            return dot_t(query, key_ref[head]), dot_t(query, held[head][0])
-
-        def finish(scores):
+            keys = jnp.concatenate([key_ref[head], keys], axis=0)
+            held[head] = jnp.concatenate([value_ref[head], pairs[:, NOPE:]], axis=0)
+            return dot_t(query_ref[head], keys)
+
+        def finish(values):
             near = stat_ref[:, head : head + 1]
-            top = near
-            for values in scores:
-                top = jnp.maximum(top, jnp.max(values, axis=1, keepdims=True))
+            top = jnp.maximum(near, jnp.max(values, axis=1, keepdims=True))
             old = jnp.exp2((near - top) * factor)
+            probs = jnp.exp2((values - top) * factor)
             total = stat_ref[:, heads + head : heads + head + 1] * old
-            summed = sum_ref[head] * old
-            for values, weights in zip(scores, (value_ref[head], held[head][1]), strict=True):
-                probs = jnp.exp2((values - top) * factor)
-                total = total + jnp.sum(probs, axis=1, keepdims=True)
-                summed = summed + jnp.dot(
-                    probs.astype(jnp.bfloat16), weights, preferred_element_type=jnp.float32
-                )
+            total = total + jnp.sum(probs, axis=1, keepdims=True)
+            summed = sum_ref[head] * old + jnp.dot(
+                probs.astype(jnp.bfloat16), held[head], preferred_element_type=jnp.float32
+            )
             out_ref[:, head * DV : (head + 1) * DV] = (summed / total).astype(jnp.bfloat16)
 
         return score, finish
@@ -749,7 +745,6 @@
         g_ckv[None],
         q_tab,
     )
-    *q_parts, w_up_other = lax.optimization_barrier((*q_parts, w_up_other))
 
     even = sp & (sp - 1) == 0
     planes = [

time: 91.9 us -> 88.5 us (0.963)
  starting transfers between devices: 38 us -> 33.9 us
  waiting for transfers between devices: 32.8 us -> 34.5 us
    ppermute x3, waiting for transfers between devices: 1.11 us -> 4.48 us  [split_device(): lax.ppermute(kv, 'sp', [(i, i ^ hop if even else (i + hop) % sp) for i in...]
    ppermute x3, starting transfers between devices: 7.43 us -> 4.38 us  [split_device(): lax.ppermute(kv, 'sp', [(i, i ^ hop if even else (i + hop) % sp) for i in...]
    ppermute x6, waiting for transfers between devices: 7.94 us -> 6.13 us  [collected(): lax.ppermute(part, 'tp', [(i, i ^ 2 * hop + 2) for i in range(tp)])]
    ppermute x4, waiting for transfers between devices: 0.01 us -> 1.34 us  [split_device(): near_other = [lax.ppermute(n, 'tp', across) for n in near_own]]
    ppermute x2, waiting for transfers between devices: 1.57 us -> 0.36 us  [reduced(): return (own, lax.ppermute(other, 'tp', across))]
    pallas_call x17, Pallas kernels: 20.2 us -> 19.3 us  [call(): pl.pallas_call(kernel, in_specs=[vmem] * len(args) + [pl.BlockSpec(memory...]
  transfers between devices with their start and end apart: 36 -> 36, of which waited for: 19 -> 18; matrix products, arithmetic and copies ran while one was open for 0% -> 0% of each run, Pallas kernels for 10% -> 11%
where the time goes in v6:
time: 88.5 us; the launch traced here: 88.2 us
  waiting for transfers between devices  34.5 us (39%)
  starting transfers between devices  33.9 us (38%)
  Pallas kernels  19.3 us (22%)
    pallas_call x17, Pallas kernels, call(): pl.pallas_call(kernel, in_specs=[vmem] * len(args) + [pl.BlockSpec(memory...  19.3 us
    ppermute x9, waiting for transfers between devices, hopped(): lax.ppermute(value, 'tp', [(i, i ^ 2 * hop) for i in range(tp)])  11.6 us
    ppermute x9, starting transfers between devices, hopped(): lax.ppermute(value, 'tp', [(i, i ^ 2 * hop) for i in range(tp)])  10.6 us
    ppermute x3, waiting for transfers between devices, split_device(): lax.ppermute(a, 'tp', [(i, i ^ 2 * hop + 2) for i in range(tp)])  8.16 us
    ppermute x6, starting transfers between devices, collected(): lax.ppermute(part, 'tp', [(i, i ^ 2 * hop + 2) for i in range(tp)])  7.11 us
    all_to_all x1, starting transfers between devices, split_device(): lax.all_to_all(modulation, ('sp', 'tp'), 0, 0, axis_index_groups=columns)  6.35 us
    ppermute x6, waiting for transfers between devices, collected(): lax.ppermute(part, 'tp', [(i, i ^ 2 * hop + 2) for i in range(tp)])  6.13 us
    ppermute x3, waiting for transfers between devices, split_device(): lax.ppermute(kv, 'sp', [(i, i ^ hop if even else (i + hop) % sp) for i in...  4.48 us
  transfers between devices with their start and end apart: 36, of which 18 were waited for; matrix products, arithmetic and copies ran while one was open for 0% of the time, Pallas kernels for 11%

profile of v6, /device:TPU:0, one launch (start us, length us, event | category | flops | bytes accessed | tf_op | source)
XLA Modules:
  0.0 88.2 jit_solution(13973043868338170387)
XLA Ops:
  0.0 2.5 %shard_map.154 = (f32[8,1,1280]{2,1,0:T(1,128)}, bf16[512,256]{1,0:T(8,128)(2,1)S(1)}, bf16[272,512]{1,0:T(8,128)(2,1)S(1)}, bf16[272,512]{1,0:T(8,128)(2,1)S(1)}) custom-call(bf16[384,256]{1,0:T(8,128)(2,1)} %latent_ref.1, bf16[128,256]{1,0:T(8,128)(2,1)} %ctx_ref.1, bf16[512]{0:T(512)(128)(2,1)} %cond_ref.1, bf16[512]{0:T(512)(128)(2,1)} %cond_ctx_ref.1, ...), custom_call_target="tpu_custom_call" | custom-call | flops 1000000 | bytes 100000 | tf_op jit(solution)/shard_map/pallas_call | solution.py:205
  2.5 0.5 collective-permute-start
  3.0 0.0 collective-permute-start.1
  3.0 6.4 %all-to-all-start = ((f32[8,1,1280]{2,1,0:T(1,128)}), f32[8,1,1280]{2,1,0:T(1,128)S(1)}, u32[]{:S(2)}, u32[]{:S(2)}) async-start(f32[8,1,1280]{2,1,0:T(1,128)} %get-tuple-element.45), calls=%async_computation | async-start | bytes 81920 | tf_op jit(solution)/shard_map/all_to_all | solution.py:689
  9.4 0.9 %shard_map.155.refs_0_ = f32[8,512]{1,0:T(8,128)S(1)} custom-call(bf16[512,256]{1,0:T(8,128)(2,1)S(1)} %get-tuple-element.44.own_ref, bf16[512,256]{1,0:T(8,128)(2,1)S(1)} %collective-permute-done.other_ref), custom_call_target="tpu_custom_call" | custom-call | flops 1000000 | bytes 100000 | tf_op jit(solution)/shard_map/pallas_call | solution.py:205
  10.3 2.5 %collective-permute-start.4 = (f32[8,512]{1,0:T(8,128)S(1)}, f32[8,512]{1,0:T(8,128)S(1)}, u32[]{:S(2)}, u32[]{:S(2)}) collective-permute-start(f32[8,512]{1,0:T(8,128)S(1)} %shard_map.155.refs_0_), channel_id=1, source_target_pairs={{0,6},{1,7},{2,4},{3,5},{4,2},{5,3},{6,0},{7,1},{8,14},{9,15},{10,... | collective-permute-start | bytes 49160 | tf_op jit(solution)/shard_map/ppermute | solution.py:662
  12.8 0.5 collective-permute-start.3
  13.3 0.5 collective-permute-start.2
  13.8 1.3 %all-to-all-done.mod_ref = f32[8,1,1280]{2,1,0:T(1,128)S(1)} async-done(((f32[8,1,1280]{2,1,0:T(1,128)}), f32[8,1,1280]{2,1,0:T(1,128)S(1)}, u32[]{:S(2)}, u32[]{:S(2)}) %all-to-all-start) | async-done | bytes 40992 | tf_op jit(solution)/shard_map/all_to_all | solution.py:689
  15.1 1.3 %collective-permute-done.3.refs_2_ = f32[8,512]{1,0:T(8,128)S(1)} collective-permute-done((f32[8,512]{1,0:T(8,128)S(1)}, f32[8,512]{1,0:T(8,128)S(1)}, u32[]{:S(2)}, u32[]{:S(2)}) %collective-permute-start.3) | collective-permute-done | bytes 16416 | tf_op jit(solution)/shard_map/ppermute | solution.py:662
  16.5 0.6 collective-permute-done.2.refs_1_
  17.1 1.6 %shard_map.156 = (f32[2,144,128]{2,1,0:T(8,128)S(1)}, f32[2,144,128]{2,1,0:T(8,128)S(1)}, f32[2,144,128]{2,1,0:T(8,128)S(1)}, f32[2,144,128]{2,1,0:T(8,128)S(1)}...) custom-call(bf16[512,256]{1,0:T(8,128)(2,1)S(1)} %get-tuple-element., ...), custom_call_target="tpu_custom_call" | custom-call | flops 335544320 | bytes 100000 | tf_op jit(solution)/shard_map/pallas_call | solution.py:205
  18.7 0.6 collective-permute-start.5
  19.3 1.5 %collective-permute-start.6 = (f32[2,96,128]{2,1,0:T(8,128)S(1)}, f32[2,96,128]{2,1,0:T(8,128)S(1)}, u32[]{:S(2)}, u32[]{:S(2)}) collective-permute-start(f32[2,96,128]{2,1,0:T(8,128)S(1)} %get-tuple-element.61), channel_id=1, source_target_pairs={{0,4},{1,5},{2,6},{3,7},{4,0},{5,1},{6,2},{7,3},{8,12},{9,13},{10,... | collective-permute-start | bytes 294920 | tf_op jit(solution)/shard_map/ppermute | solution.py:717
  20.8 1.4 %collective-permute-start.7 = (f32[2,96,128]{2,1,0:T(8,128)S(1)}, f32[2,96,128]{2,1,0:T(8,128)S(1)}, u32[]{:S(2)}, u32[]{:S(2)}) collective-permute-start(f32[2,96,128]{2,1,0:T(8,128)S(1)} %get-tuple-element.62), channel_id=1, source_target_pairs={{0,6},{1,7},{2,4},{3,5},{4,2},{5,3},{6,0},{7,1},{8,14},{9,15},{10,... | collective-permute-start | bytes 294920 | tf_op jit(solution)/shard_map/ppermute | solution.py:717
  22.3 0.5 collective-permute-start.9
  22.8 1.5 %collective-permute-start.10 = (f32[2,144,128]{2,1,0:T(8,128)S(1)}, f32[2,144,128]{2,1,0:T(8,128)S(1)}, u32[]{:S(2)}, u32[]{:S(2)}) collective-permute-start(f32[2,144,128]{2,1,0:T(8,128)S(1)} %get-tuple-element.67), channel_id=1, source_target_pairs={{0,4},{1,5},{2,6},{3,7},{4,0},{5,1},{6,2},{7,3},{8,12},{9,13},{10,... | collective-permute-start | bytes 442376 | tf_op jit(solution)/shard_map/ppermute | solution.py:717
  24.3 0.1 shard_map.166
  24.5 1.5 %collective-permute-start.11 = (f32[2,144,128]{2,1,0:T(8,128)S(1)}, f32[2,144,128]{2,1,0:T(8,128)S(1)}, u32[]{:S(2)}, u32[]{:S(2)}) collective-permute-start(f32[2,144,128]{2,1,0:T(8,128)S(1)} %get-tuple-element.68), channel_id=1, source_target_pairs={{0,6},{1,7},{2,4},{3,5},{4,2},{5,3},{6,0},{7,1},{8,14},{9,15},{10,... | collective-permute-start | bytes 442376 | tf_op jit(solution)/shard_map/ppermute | solution.py:717
  26.0 0.3 collective-permute-done.6.refs_2_
  26.3 1.3 %collective-permute-done.7.refs_3_ = f32[2,96,128]{2,1,0:T(8,128)S(1)} collective-permute-done((f32[2,96,128]{2,1,0:T(8,128)S(1)}, f32[2,96,128]{2,1,0:T(8,128)S(1)}, u32[]{:S(2)}, u32[]{:S(2)}) %collective-permute-start.7) | collective-permute-done | bytes 98336 | tf_op jit(solution)/shard_map/ppermute | solution.py:717
  27.6 0.1 collective-permute-start.8
  27.7 2.0 %collective-permute-done.9.refs_1_ = f32[2,144,128]{2,1,0:T(8,128)S(1)} collective-permute-done((f32[2,144,128]{2,1,0:T(8,128)S(1)}, f32[2,144,128]{2,1,0:T(8,128)S(1)}, u32[]{:S(2)}, u32[]{:S(2)}) %collective-permute-start.9) | collective-permute-done | bytes 147488 | tf_op jit(solution)/shard_map/ppermute | solution.py:717
  29.7 1.0 %collective-permute-done.10.refs_2_ = f32[2,144,128]{2,1,0:T(8,128)S(1)} collective-permute-done((f32[2,144,128]{2,1,0:T(8,128)S(1)}, f32[2,144,128]{2,1,0:T(8,128)S(1)}, u32[]{:S(2)}, u32[]{:S(2)}) %collective-permute-start.10) | collective-permute-done | bytes 147488 | tf_op jit(solution)/shard_map/ppermute | solution.py:717
  30.7 1.5 %collective-permute-done.11.refs_3_ = f32[2,144,128]{2,1,0:T(8,128)S(1)} collective-permute-done((f32[2,144,128]{2,1,0:T(8,128)S(1)}, f32[2,144,128]{2,1,0:T(8,128)S(1)}, u32[]{:S(2)}, u32[]{:S(2)}) %collective-permute-start.11) | collective-permute-done | bytes 147488 | tf_op jit(solution)/shard_map/ppermute | solution.py:717
  32.2 0.1 shard_map.160
  32.3 0.1 collective-permute-start.12
  32.4 0.9 %shard_map.157.tab_ref = f32[384,128]{1,0:T(8,128)S(1)} custom-call(f32[1,128]{1,0:T(1,128)S(1)} %broadcast_add_fusion.inverse_ref), custom_call_target="tpu_custom_call" | custom-call | flops 1000000000 | bytes 100000 | tf_op jit(solution)/shard_map/pallas_call | solution.py:205
  33.3 0.4 collective-permute-done.12.other_ref
  33.6 0.3 shard_map.161.kv_ref
  33.9 3.5 %collective-permute-start.22 = (bf16[72,512]{1,0:T(8,128)(2,1)S(1)}, bf16[72,512]{1,0:T(8,128)(2,1)S(1)}, u32[]{:S(2)}, u32[]{:S(2)}) collective-permute-start(bf16[72,512]{1,0:T(8,128)(2,1)S(1)} %shard_map.161.kv_ref), channel_id=1, source_target_pairs={{0,24},{8,16},{16,8},{24,0},{1,25},{9,17},{17,9},{25,1},{2,26},{10... | collective-permute-start | bytes 221192 | tf_op jit(solution)/shard_map/ppermute | solution.py:751
  37.4 0.1 shard_map.162.refs_0_
  37.5 2.0 %collective-permute-start.15 = (bf16[120,512]{1,0:T(8,128)(2,1)S(1)}, bf16[120,512]{1,0:T(8,128)(2,1)S(1)}, u32[]{:S(2)}, u32[]{:S(2)}) collective-permute-start(bf16[120,512]{1,0:T(8,128)(2,1)S(1)} %shard_map.162.refs_0_), channel_id=1, source_target_pairs={{0,6},{1,7},{2,4},{3,5},{4,2},{5,3},{6,0},{7,1},{8,14},{9,15},{10,... | collective-permute-start | bytes 368648 | tf_op jit(solution)/shard_map/ppermute | solution.py:662
  39.6 1.1 %collective-permute-start.14 = (bf16[120,512]{1,0:T(8,128)(2,1)S(1)}, bf16[120,512]{1,0:T(8,128)(2,1)S(1)}, u32[]{:S(2)}, u32[]{:S(2)}) collective-permute-start(bf16[120,512]{1,0:T(8,128)(2,1)S(1)} %shard_map.162.refs_0_), channel_id=1, source_target_pairs={{0,4},{1,5},{2,6},{3,7},{4,0},{5,1},{6,2},{7,3},{8,12},{9,13},{10,... | collective-permute-start | bytes 368648 | tf_op jit(solution)/shard_map/ppermute | solution.py:662
  40.6 0.9 %collective-permute-start.20 = (bf16[72,512]{1,0:T(8,128)(2,1)S(1)}, bf16[72,512]{1,0:T(8,128)(2,1)S(1)}, u32[]{:S(2)}, u32[]{:S(2)}) collective-permute-start(bf16[72,512]{1,0:T(8,128)(2,1)S(1)} %shard_map.161.kv_ref), channel_id=1, source_target_pairs={{0,8},{8,0},{16,24},{24,16},{1,9},{9,1},{17,25},{25,17},{2,10},{10... | collective-permute-start | bytes 221192 | tf_op jit(solution)/shard_map/ppermute | solution.py:751
  41.5 4.5 %collective-permute-done.21.refs_1_ = bf16[72,512]{1,0:T(8,128)(2,1)S(1)} collective-permute-done((bf16[72,512]{1,0:T(8,128)(2,1)S(1)}, bf16[72,512]{1,0:T(8,128)(2,1)S(1)}, u32[]{:S(2)}, u32[]{:S(2)}) %collective-permute-start.21) | collective-permute-done | bytes 73760 | tf_op jit(solution)/shard_map/ppermute | solution.py:751
  46.0 0.8 collective-permute-start.13
  46.8 0.5 collective-permute-start.18
  47.4 1.7 %collective-permute-start.26 = (bf16[216,512]{1,0:T(8,128)(2,1)S(1)}, bf16[216,512]{1,0:T(8,128)(2,1)S(1)}, u32[]{:S(2)}, u32[]{:S(2)}) collective-permute-start(bf16[216,512]{1,0:T(8,128)(2,1)S(1)} %shard_map.163.refs_8_), channel_id=1, source_target_pairs={{0,6},{1,7},{2,4},{3,5},{4,2},{5,3},{6,0},{7,1},{8,14},{9,15},{10,... | collective-permute-start | bytes 663560 | tf_op jit(solution)/shard_map/ppermute | solution.py:662
  49.0 3.1 %collective-permute-done.13.refs_1_ = bf16[120,512]{1,0:T(8,128)(2,1)S(1)} collective-permute-done((bf16[120,512]{1,0:T(8,128)(2,1)S(1)}, bf16[120,512]{1,0:T(8,128)(2,1)S(1)}, u32[]{:S(2)}, u32[]{:S(2)}) %collective-permute-start.13) | collective-permute-done | bytes 122912 | tf_op jit(solution)/shard_map/ppermute | solution.py:662
  52.2 1.0 %collective-permute-start.25 = (bf16[216,512]{1,0:T(8,128)(2,1)S(1)}, bf16[216,512]{1,0:T(8,128)(2,1)S(1)}, u32[]{:S(2)}, u32[]{:S(2)}) collective-permute-start(bf16[216,512]{1,0:T(8,128)(2,1)S(1)} %shard_map.163.refs_8_), channel_id=1, source_target_pairs={{0,4},{1,5},{2,6},{3,7},{4,0},{5,1},{6,2},{7,3},{8,12},{9,13},{10,... | collective-permute-start | bytes 663560 | tf_op jit(solution)/shard_map/ppermute | solution.py:662
  53.2 0.5 collective-permute-start.24
  53.7 1.3 %collective-permute-done.17.refs_5_ = bf16[120,512]{1,0:T(8,128)(2,1)S(1)} collective-permute-done((bf16[120,512]{1,0:T(8,128)(2,1)S(1)}, bf16[120,512]{1,0:T(8,128)(2,1)S(1)}, u32[]{:S(2)}, u32[]{:S(2)}) %collective-permute-start.17) | collective-permute-done | bytes 122912 | tf_op jit(solution)/shard_map/ppermute | solution.py:756
  55.0 0.1 collective-permute-start.23
  55.2 2.2 %collective-permute-done.26.refs_2_ = bf16[216,512]{1,0:T(8,128)(2,1)S(1)} collective-permute-done((bf16[216,512]{1,0:T(8,128)(2,1)S(1)}, bf16[216,512]{1,0:T(8,128)(2,1)S(1)}, u32[]{:S(2)}, u32[]{:S(2)}) %collective-permute-start.26) | collective-permute-done | bytes 221216 | tf_op jit(solution)/shard_map/ppermute | solution.py:662
  57.4 4.2 %collective-permute-done.25.refs_1_ = bf16[216,512]{1,0:T(8,128)(2,1)S(1)} collective-permute-done((bf16[216,512]{1,0:T(8,128)(2,1)S(1)}, bf16[216,512]{1,0:T(8,128)(2,1)S(1)}, u32[]{:S(2)}, u32[]{:S(2)}) %collective-permute-start.25) | collective-permute-done | bytes 221216 | tf_op jit(solution)/shard_map/ppermute | solution.py:662
  61.6 0.5 collective-permute-start.27
  62.1 1.6 %shard_map.158.wkv_ref.w_ref = bf16[512,1024]{1,0:T(8,128)(2,1)S(1)} custom-call(bf16[512,4,256]{2,1,0:T(4,128)(2,1)S(1)} %copy-done.4), custom_call_target="tpu_custom_call" | custom-call | flops 1000000000 | bytes 100000 | tf_op jit(solution)/shard_map/pallas_call | solution.py:205
  63.8 0.8 shard_map.165
  64.6 0.1 broadcast_in_dim.12.lift_ref
  64.7 0.2 copy-done.5
  64.9 3.9 %shard_map.164 = (bf16[4,384,256]{2,1,0:T(8,128)(2,1)S(1)}, f32[384,128]{1,0:T(8,128)S(1)}, f32[4,384,128]{2,1,0:T(8,128)S(1)}) custom-call(f32[384,128]{1,0:T(8,128)S(1)} %shard_map.157.tab_ref, f32[4,128]{1,0:T(4,128)S(1)} %broadcast_in_dim.12.lift_ref, bf16[4,192,512]{2,1,0:T(8,128)(2,1)S(1)} %bitcast.10, bf16[512,1024]{1,0:T(8,128)(2,1)S(1)} %shard_map.158.wkv_ref.w_ref, ...), custom_call_target="tpu_custom_call" | custom-call | flops 1459617792 | bytes 100000 | tf_op jit(solution)/shard_map/pallas_call | solution.py:205
  68.9 4.4 %shard_map.167 = (bf16[384,512]{1,0:T(8,128)(2,1)S(1)}, bf16[4,512,256]{2,1,0:T(8,128)(2,1)S(1)}) custom-call(bf16[4,384,256]{2,1,0:T(8,128)(2,1)S(1)} %get-tuple-element.71.query_ref, f32[384,128]{1,0:T(8,128)S(1)} %get-tuple-element.72.stat_ref, f32[4,384,128]{2,1,0:T(8,128)S(1)} %get-tuple-element.73.sum_ref, ...), custom_call_target="tpu_custom_call" | custom-call | flops 1962934272 | bytes 100000 | tf_op jit(solution)/shard_map/pallas_call | solution.py:205
  73.3 0.1 collective-permute-start.31
  73.4 0.6 shard_map.168.acc_ref
  74.0 1.1 %collective-permute-done.31.heads_ref = bf16[384,512]{1,0:T(8,128)(2,1)S(1)} collective-permute-done((bf16[384,512]{1,0:T(8,128)(2,1)S(1)}, bf16[384,512]{1,0:T(8,128)(2,1)S(1)}, u32[]{:S(2)}, u32[]{:S(2)}) %collective-permute-start.31) | collective-permute-done | bytes 393248 | tf_op jit(solution)/shard_map/ppermute | solution.py:811
  75.1 0.6 shard_map.169
  75.7 0.7 collective-permute-start.32
  76.4 1.0 %collective-permute-start.33 = (bf16[384,256]{1,0:T(8,128)(2,1)S(1)}, bf16[384,256]{1,0:T(8,128)(2,1)S(1)}, u32[]{:S(2)}, u32[]{:S(2)}) collective-permute-start(bf16[384,256]{1,0:T(8,128)(2,1)S(1)} %get-tuple-element.81), channel_id=1, source_target_pairs={{0,4},{1,5},{2,6},{3,7},{4,0},{5,1},{6,2},{7,3},{8,12},{9,13},{10,... | collective-permute-start | bytes 589832 | tf_op jit(solution)/shard_map/ppermute | solution.py:826
  77.4 1.9 %collective-permute-start.34 = (bf16[384,256]{1,0:T(8,128)(2,1)S(1)}, bf16[384,256]{1,0:T(8,128)(2,1)S(1)}, u32[]{:S(2)}, u32[]{:S(2)}) collective-permute-start(bf16[384,256]{1,0:T(8,128)(2,1)S(1)} %get-tuple-element.82), channel_id=1, source_target_pairs={{0,6},{1,7},{2,4},{3,5},{4,2},{5,3},{6,0},{7,1},{8,14},{9,15},{10,... | collective-permute-start | bytes 589832 | tf_op jit(solution)/shard_map/ppermute | solution.py:826
  79.3 4.3 %collective-permute-done.32.refs_1_ = bf16[384,256]{1,0:T(8,128)(2,1)S(1)} collective-permute-done((bf16[384,256]{1,0:T(8,128)(2,1)S(1)}, bf16[384,256]{1,0:T(8,128)(2,1)S(1)}, u32[]{:S(2)}, u32[]{:S(2)}) %collective-permute-start.32) | collective-permute-done | bytes 196640 | tf_op jit(solution)/shard_map/ppermute | solution.py:826
  83.5 0.1 collective-permute-done.33.refs_2_
  83.7 3.8 %collective-permute-done.34.refs_3_ = bf16[384,256]{1,0:T(8,128)(2,1)S(1)} collective-permute-done((bf16[384,256]{1,0:T(8,128)(2,1)S(1)}, bf16[384,256]{1,0:T(8,128)(2,1)S(1)}, u32[]{:S(2)}, u32[]{:S(2)}) %collective-permute-start.34) | collective-permute-done | bytes 196640 | tf_op jit(solution)/shard_map/ppermute | solution.py:826
  87.4 0.8 shard_map.170
  (43 shorter events, 0.2 us)
Async XLA Ops:
  0.0 24.3 %copy-start = (bf16[4,128,2048]{2,1,0:T(8,128)(2,1)S(1)}, bf16[4,128,2048]{2,1,0:T(8,128)(2,1)}, u32[]{:S(2)}) copy-start(bf16[4,128,2048]{2,1,0:T(8,128)(2,1)} %param.30) | copy-start | bytes 6291460
  2.5 6.9 %collective-permute-start = (bf16[512,256]{1,0:T(8,128)(2,1)S(1)}, bf16[512,256]{1,0:T(8,128)(2,1)S(1)}, u32[]{:S(2)}, u32[]{:S(2)}) collective-permute-start(bf16[512,256]{1,0:T(8,128)(2,1)S(1)} %get-tuple-element.44.own_ref), channel_id=1, source_target_pairs={{0,1},{1,0},{2,3},{3,2},{4,5},{5,4},{6,7},{7,6},{8,9},{9,8},{10,11... | collective-permute-start | bytes 786440 | tf_op jit(solution)/shard_map/ppermute | solution.py:687
  3.0 14.1 %collective-permute-start.1 = (bf16[272,512]{1,0:T(8,128)(2,1)S(1)}, bf16[272,512]{1,0:T(8,128)(2,1)S(1)}, u32[]{:S(2)}, u32[]{:S(2)}) collective-permute-start(bf16[272,512]{1,0:T(8,128)(2,1)S(1)} %get-tuple-element.47), channel_id=1, source_target_pairs={{0,1},{1,0},{2,3},{3,2},{4,5},{5,4},{6,7},{7,6},{8,9},{9,8},{10,11... | collective-permute-start | bytes 835592 | tf_op jit(solution)/shard_map/ppermute | solution.py:686
  3.0 12.1 %all-to-all-start = ((f32[8,1,1280]{2,1,0:T(1,128)}), f32[8,1,1280]{2,1,0:T(1,128)S(1)}, u32[]{:S(2)}, u32[]{:S(2)}) async-start(f32[8,1,1280]{2,1,0:T(1,128)} %get-tuple-element.45), calls=%async_computation | async-start | bytes 81920 | tf_op jit(solution)/shard_map/all_to_all | solution.py:689
  10.3 4.9 %collective-permute-start.4 = (f32[8,512]{1,0:T(8,128)S(1)}, f32[8,512]{1,0:T(8,128)S(1)}, u32[]{:S(2)}, u32[]{:S(2)}) collective-permute-start(f32[8,512]{1,0:T(8,128)S(1)} %shard_map.155.refs_0_), channel_id=1, source_target_pairs={{0,6},{1,7},{2,4},{3,5},{4,2},{5,3},{6,0},{7,1},{8,14},{9,15},{10,... | collective-permute-start | bytes 49160 | tf_op jit(solution)/shard_map/ppermute | solution.py:662
  12.8 3.7 %collective-permute-start.3 = (f32[8,512]{1,0:T(8,128)S(1)}, f32[8,512]{1,0:T(8,128)S(1)}, u32[]{:S(2)}, u32[]{:S(2)}) collective-permute-start(f32[8,512]{1,0:T(8,128)S(1)} %shard_map.155.refs_0_), channel_id=1, source_target_pairs={{0,4},{1,5},{2,6},{3,7},{4,0},{5,1},{6,2},{7,3},{8,12},{9,13},{10,... | collective-permute-start | bytes 49160 | tf_op jit(solution)/shard_map/ppermute | solution.py:662
  13.3 3.8 %collective-permute-start.2 = (f32[8,512]{1,0:T(8,128)S(1)}, f32[8,512]{1,0:T(8,128)}, u32[]{:S(2)}, u32[]{:S(2)}) collective-permute-start(f32[8,512]{1,0:T(8,128)S(1)} %shard_map.155.refs_0_), channel_id=1, source_target_pairs={{0,2},{1,3},{2,0},{3,1},{4,6},{5,7},{6,4},{7,5},{8,10},{9,11},{10,... | collective-permute-start | bytes 49160 | tf_op jit(solution)/shard_map/ppermute | solution.py:662
  18.7 5.8 %collective-permute-start.5 = (f32[2,96,128]{2,1,0:T(8,128)S(1)}, f32[2,96,128]{2,1,0:T(8,128)S(1)}, u32[]{:S(2)}, u32[]{:S(2)}) collective-permute-start(f32[2,96,128]{2,1,0:T(8,128)S(1)} %get-tuple-element.60), channel_id=1, source_target_pairs={{0,2},{1,3},{2,0},{3,1},{4,6},{5,7},{6,4},{7,5},{8,10},{9,11},{10,... | collective-permute-start | bytes 294920 | tf_op jit(solution)/shard_map/ppermute | solution.py:717
  19.3 7.0 %collective-permute-start.6 = (f32[2,96,128]{2,1,0:T(8,128)S(1)}, f32[2,96,128]{2,1,0:T(8,128)S(1)}, u32[]{:S(2)}, u32[]{:S(2)}) collective-permute-start(f32[2,96,128]{2,1,0:T(8,128)S(1)} %get-tuple-element.61), channel_id=1, source_target_pairs={{0,4},{1,5},{2,6},{3,7},{4,0},{5,1},{6,2},{7,3},{8,12},{9,13},{10,... | collective-permute-start | bytes 294920 | tf_op jit(solution)/shard_map/ppermute | solution.py:717
  20.8 6.8 %collective-permute-start.7 = (f32[2,96,128]{2,1,0:T(8,128)S(1)}, f32[2,96,128]{2,1,0:T(8,128)S(1)}, u32[]{:S(2)}, u32[]{:S(2)}) collective-permute-start(f32[2,96,128]{2,1,0:T(8,128)S(1)} %get-tuple-element.62), channel_id=1, source_target_pairs={{0,6},{1,7},{2,4},{3,5},{4,2},{5,3},{6,0},{7,1},{8,14},{9,15},{10,... | collective-permute-start | bytes 294920 | tf_op jit(solution)/shard_map/ppermute | solution.py:717
  22.3 7.4 %collective-permute-start.9 = (f32[2,144,128]{2,1,0:T(8,128)S(1)}, f32[2,144,128]{2,1,0:T(8,128)S(1)}, u32[]{:S(2)}, u32[]{:S(2)}) collective-permute-start(f32[2,144,128]{2,1,0:T(8,128)S(1)} %get-tuple-element.66), channel_id=1, source_target_pairs={{0,2},{1,3},{2,0},{3,1},{4,6},{5,7},{6,4},{7,5},{8,10},{9,11},{10,... | collective-permute-start | bytes 442376 | tf_op jit(solution)/shard_map/ppermute | solution.py:717
  22.8 7.9 %collective-permute-start.10 = (f32[2,144,128]{2,1,0:T(8,128)S(1)}, f32[2,144,128]{2,1,0:T(8,128)S(1)}, u32[]{:S(2)}, u32[]{:S(2)}) collective-permute-start(f32[2,144,128]{2,1,0:T(8,128)S(1)} %get-tuple-element.67), channel_id=1, source_target_pairs={{0,4},{1,5},{2,6},{3,7},{4,0},{5,1},{6,2},{7,3},{8,12},{9,13},{10,... | collective-permute-start | bytes 442376 | tf_op jit(solution)/shard_map/ppermute | solution.py:717
  24.3 2.0 %copy-start.7 = (f32[1,128]{1,0:T(1,128)S(1)}, f32[1,128]{1,0:T(1,128)}, u32[]{:S(2)}) copy-start(f32[1,128]{1,0:T(1,128)} %constant.4.clone) | copy-start | bytes 1540
  24.5 7.7 %collective-permute-start.11 = (f32[2,144,128]{2,1,0:T(8,128)S(1)}, f32[2,144,128]{2,1,0:T(8,128)S(1)}, u32[]{:S(2)}, u32[]{:S(2)}) collective-permute-start(f32[2,144,128]{2,1,0:T(8,128)S(1)} %get-tuple-element.68), channel_id=1, source_target_pairs={{0,6},{1,7},{2,4},{3,5},{4,2},{5,3},{6,0},{7,1},{8,14},{9,15},{10,... | collective-permute-start | bytes 442376 | tf_op jit(solution)/shard_map/ppermute | solution.py:717
  26.3 42.6 %collective-permute-start.30 = (bf16[4,512,256]{2,1,0:T(8,128)(2,1)S(1)}, bf16[4,512,256]{2,1,0:T(8,128)(2,1)S(1)}, u32[]{:S(2)}, u32[]{:S(2)}) collective-permute-start(bf16[4,512,256]{2,1,0:T(8,128)(2,1)S(1)} %shard_map.166), channel_id=1, source_target_pairs={{0,1},{1,0},{2,3},{3,2},{4,5},{5,4},{6,7},{7,6},{8,9},{9,8},{10,11... | collective-permute-start | bytes 3145736 | tf_op jit(solution)/shard_map/ppermute | solution.py:738
  27.6 9.8 %collective-permute-start.8 = (f32[96,128]{1,0:T(8,128)S(1)}, f32[96,128]{1,0:T(8,128)S(1)}, u32[]{:S(2)}, u32[]{:S(2)}) collective-permute-start(f32[96,128]{1,0:T(8,128)S(1)} %get-tuple-element.64), channel_id=1, source_target_pairs={{0,1},{1,0},{2,3},{3,2},{4,5},{5,4},{6,7},{7,6},{8,9},{9,8},{10,11... | collective-permute-start | bytes 147464 | tf_op jit(solution)/shard_map/ppermute | solution.py:724
  32.3 1.4 %copy-start.2 = (f32[512]{0:T(512)S(1)}, f32[512]{0:T(512)}, u32[]{:S(2)}) copy-start(f32[512]{0:T(512)} %param.26) | copy-start | bytes 6148
  32.3 5.1 %copy-start.3 = (f32[512]{0:T(512)S(1)}, f32[512]{0:T(512)}, u32[]{:S(2)}) copy-start(f32[512]{0:T(512)} %param.25) | copy-start | bytes 6148
  32.3 29.8 %copy-start.4 = (bf16[512,4,256]{2,1,0:T(4,128)(2,1)S(1)}, bf16[512,4,256]{2,1,0:T(4,128)(2,1)}, u32[]{:S(2)}) copy-start(bf16[512,4,256]{2,1,0:T(4,128)(2,1)} %w_ref) | copy-start | bytes 3145732
  32.3 1.3 %collective-permute-start.12 = (f32[144,128]{1,0:T(8,128)S(1)}, f32[144,128]{1,0:T(8,128)S(1)}, u32[]{:S(2)}, u32[]{:S(2)}) collective-permute-start(f32[144,128]{1,0:T(8,128)S(1)} %get-tuple-element.70), channel_id=1, source_target_pairs={{0,1},{1,0},{2,3},{3,2},{4,5},{5,4},{6,7},{7,6},{8,9},{9,8},{10,11... | collective-permute-start | bytes 221192 | tf_op jit(solution)/shard_map/ppermute | solution.py:724
  33.9 6.7 %collective-permute-start.22 = (bf16[72,512]{1,0:T(8,128)(2,1)S(1)}, bf16[72,512]{1,0:T(8,128)(2,1)S(1)}, u32[]{:S(2)}, u32[]{:S(2)}) collective-permute-start(bf16[72,512]{1,0:T(8,128)(2,1)S(1)} %shard_map.161.kv_ref), channel_id=1, source_target_pairs={{0,24},{8,16},{16,8},{24,0},{1,25},{9,17},{17,9},{25,1},{2,26},{10... | collective-permute-start | bytes 221192 | tf_op jit(solution)/shard_map/ppermute | solution.py:751
  37.5 9.3 %collective-permute-start.15 = (bf16[120,512]{1,0:T(8,128)(2,1)S(1)}, bf16[120,512]{1,0:T(8,128)(2,1)S(1)}, u32[]{:S(2)}, u32[]{:S(2)}) collective-permute-start(bf16[120,512]{1,0:T(8,128)(2,1)S(1)} %shard_map.162.refs_0_), channel_id=1, source_target_pairs={{0,6},{1,7},{2,4},{3,5},{4,2},{5,3},{6,0},{7,1},{8,14},{9,15},{10,... | collective-permute-start | bytes 368648 | tf_op jit(solution)/shard_map/ppermute | solution.py:662
  39.6 7.3 %collective-permute-start.14 = (bf16[120,512]{1,0:T(8,128)(2,1)S(1)}, bf16[120,512]{1,0:T(8,128)(2,1)S(1)}, u32[]{:S(2)}, u32[]{:S(2)}) collective-permute-start(bf16[120,512]{1,0:T(8,128)(2,1)S(1)} %shard_map.162.refs_0_), channel_id=1, source_target_pairs={{0,4},{1,5},{2,6},{3,7},{4,0},{5,1},{6,2},{7,3},{8,12},{9,13},{10,... | collective-permute-start | bytes 368648 | tf_op jit(solution)/shard_map/ppermute | solution.py:662
  40.6 5.4 %collective-permute-start.21 = (bf16[72,512]{1,0:T(8,128)(2,1)S(1)}, bf16[72,512]{1,0:T(8,128)(2,1)S(1)}, u32[]{:S(2)}, u32[]{:S(2)}) collective-permute-start(bf16[72,512]{1,0:T(8,128)(2,1)S(1)} %shard_map.161.kv_ref), channel_id=1, source_target_pairs={{0,16},{8,24},{16,0},{24,8},{1,17},{9,25},{17,1},{25,9},{2,18},{10... | collective-permute-start | bytes 221192 | tf_op jit(solution)/shard_map/ppermute | solution.py:751
  40.6 5.4 %collective-permute-start.20 = (bf16[72,512]{1,0:T(8,128)(2,1)S(1)}, bf16[72,512]{1,0:T(8,128)(2,1)S(1)}, u32[]{:S(2)}, u32[]{:S(2)}) collective-permute-start(bf16[72,512]{1,0:T(8,128)(2,1)S(1)} %shard_map.161.kv_ref), channel_id=1, source_target_pairs={{0,8},{8,0},{16,24},{24,16},{1,9},{9,1},{17,25},{25,17},{2,10},{10... | collective-permute-start | bytes 221192 | tf_op jit(solution)/shard_map/ppermute | solution.py:751
  46.0 1.4 %collective-permute-start.16 = (bf16[120,512]{1,0:T(8,128)(2,1)S(1)}, bf16[120,512]{1,0:T(8,128)(2,1)S(1)}, u32[]{:S(2)}, u32[]{:S(2)}) collective-permute-start(bf16[120,512]{1,0:T(8,128)(2,1)S(1)} %shard_map.162.refs_0_), channel_id=1, source_target_pairs={{0,1},{1,0},{2,3},{3,2},{4,5},{5,4},{6,7},{7,6},{8,9},{9,8},{10,11... | collective-permute-start | bytes 368648 | tf_op jit(solution)/shard_map/ppermute | solution.py:756
  46.0 6.2 %collective-permute-start.13 = (bf16[120,512]{1,0:T(8,128)(2,1)S(1)}, bf16[120,512]{1,0:T(8,128)(2,1)S(1)}, u32[]{:S(2)}, u32[]{:S(2)}) collective-permute-start(bf16[120,512]{1,0:T(8,128)(2,1)S(1)} %shard_map.162.refs_0_), channel_id=1, source_target_pairs={{0,2},{1,3},{2,0},{3,1},{4,6},{5,7},{6,4},{7,5},{8,10},{9,11},{10,... | collective-permute-start | bytes 368648 | tf_op jit(solution)/shard_map/ppermute | solution.py:662
  46.8 6.4 %collective-permute-start.19 = (bf16[120,512]{1,0:T(8,128)(2,1)S(1)}, bf16[120,512]{1,0:T(8,128)(2,1)S(1)}, u32[]{:S(2)}, u32[]{:S(2)}) collective-permute-start(bf16[120,512]{1,0:T(8,128)(2,1)S(1)} %collective-permute-done.15.refs_3_), channel_id=1, source_target_pairs={{0,1},{1,0},{2,3},{3,2},{4,5},{5,4},{6,7},{7,6},{8,9},{9,8},{10,11... | collective-permute-start | bytes 368648 | tf_op jit(solution)/shard_map/ppermute | solution.py:756
  46.8 6.8 %collective-permute-start.18 = (bf16[120,512]{1,0:T(8,128)(2,1)S(1)}, bf16[120,512]{1,0:T(8,128)(2,1)S(1)}, u32[]{:S(2)}, u32[]{:S(2)}) collective-permute-start(bf16[120,512]{1,0:T(8,128)(2,1)S(1)} %collective-permute-done.14.refs_2_), channel_id=1, source_target_pairs={{0,1},{1,0},{2,3},{3,2},{4,5},{5,4},{6,7},{7,6},{8,9},{9,8},{10,11... | collective-permute-start | bytes 368648 | tf_op jit(solution)/shard_map/ppermute | solution.py:756
  47.4 10.0 %collective-permute-start.26 = (bf16[216,512]{1,0:T(8,128)(2,1)S(1)}, bf16[216,512]{1,0:T(8,128)(2,1)S(1)}, u32[]{:S(2)}, u32[]{:S(2)}) collective-permute-start(bf16[216,512]{1,0:T(8,128)(2,1)S(1)} %shard_map.163.refs_8_), channel_id=1, source_target_pairs={{0,6},{1,7},{2,4},{3,5},{4,2},{5,3},{6,0},{7,1},{8,14},{9,15},{10,... | collective-permute-start | bytes 663560 | tf_op jit(solution)/shard_map/ppermute | solution.py:662
  52.2 9.4 %collective-permute-start.25 = (bf16[216,512]{1,0:T(8,128)(2,1)S(1)}, bf16[216,512]{1,0:T(8,128)(2,1)S(1)}, u32[]{:S(2)}, u32[]{:S(2)}) collective-permute-start(bf16[216,512]{1,0:T(8,128)(2,1)S(1)} %shard_map.163.refs_8_), channel_id=1, source_target_pairs={{0,4},{1,5},{2,6},{3,7},{4,0},{5,1},{6,2},{7,3},{8,12},{9,13},{10,... | collective-permute-start | bytes 663560 | tf_op jit(solution)/shard_map/ppermute | solution.py:662
  53.2 8.5 %collective-permute-start.24 = (bf16[216,512]{1,0:T(8,128)(2,1)S(1)}, bf16[216,512]{1,0:T(8,128)(2,1)S(1)}, u32[]{:S(2)}, u32[]{:S(2)}) collective-permute-start(bf16[216,512]{1,0:T(8,128)(2,1)S(1)} %shard_map.163.refs_8_), channel_id=1, source_target_pairs={{0,2},{1,3},{2,0},{3,1},{4,6},{5,7},{6,4},{7,5},{8,10},{9,11},{10,... | collective-permute-start | bytes 663560 | tf_op jit(solution)/shard_map/ppermute | solution.py:662
  53.7 1.3 %collective-permute-start.17 = (bf16[120,512]{1,0:T(8,128)(2,1)S(1)}, bf16[120,512]{1,0:T(8,128)(2,1)S(1)}, u32[]{:S(2)}, u32[]{:S(2)}) collective-permute-start(bf16[120,512]{1,0:T(8,128)(2,1)S(1)} %collective-permute-done.13.refs_1_), channel_id=1, source_target_pairs={{0,1},{1,0},{2,3},{3,2},{4,5},{5,4},{6,7},{7,6},{8,9},{9,8},{10,11... | collective-permute-start | bytes 368648 | tf_op jit(solution)/shard_map/ppermute | solution.py:756
  55.0 9.6 %collective-permute-start.23 = (bf16[216,512]{1,0:T(8,128)(2,1)S(1)}, bf16[216,512]{1,0:T(8,128)(2,1)S(1)}, u32[]{:S(2)}, u32[]{:S(2)}) collective-permute-start(bf16[216,512]{1,0:T(8,128)(2,1)S(1)} %shard_map.163.refs_8_), channel_id=1, source_target_pairs={{0,1},{1,0},{2,3},{3,2},{4,5},{5,4},{6,7},{7,6},{8,9},{9,8},{10,11... | collective-permute-start | bytes 663560 | tf_op jit(solution)/shard_map/ppermute | solution.py:759
  57.4 11.5 %collective-permute-start.29 = (bf16[216,512]{1,0:T(8,128)(2,1)S(1)}, bf16[216,512]{1,0:T(8,128)(2,1)S(1)}, u32[]{:S(2)}, u32[]{:S(2)}) collective-permute-start(bf16[216,512]{1,0:T(8,128)(2,1)S(1)} %collective-permute-done.26.refs_2_), channel_id=1, source_target_pairs={{0,1},{1,0},{2,3},{3,2},{4,5},{5,4},{6,7},{7,6},{8,9},{9,8},{10,11... | collective-permute-start | bytes 663560 | tf_op jit(solution)/shard_map/ppermute | solution.py:759
  61.6 7.3 %collective-permute-start.28 = (bf16[216,512]{1,0:T(8,128)(2,1)S(1)}, bf16[216,512]{1,0:T(8,128)(2,1)S(1)}, u32[]{:S(2)}, u32[]{:S(2)}) collective-permute-start(bf16[216,512]{1,0:T(8,128)(2,1)S(1)} %collective-permute-done.25.refs_1_), channel_id=1, source_target_pairs={{0,1},{1,0},{2,3},{3,2},{4,5},{5,4},{6,7},{7,6},{8,9},{9,8},{10,11... | collective-permute-start | bytes 663560 | tf_op jit(solution)/shard_map/ppermute | solution.py:759
  61.6 7.2 %collective-permute-start.27 = (bf16[216,512]{1,0:T(8,128)(2,1)S(1)}, bf16[216,512]{1,0:T(8,128)(2,1)S(1)}, u32[]{:S(2)}, u32[]{:S(2)}) collective-permute-start(bf16[216,512]{1,0:T(8,128)(2,1)S(1)} %collective-permute-done.24.refs_0_), channel_id=1, source_target_pairs={{0,1},{1,0},{2,3},{3,2},{4,5},{5,4},{6,7},{7,6},{8,9},{9,8},{10,11... | collective-permute-start | bytes 663560 | tf_op jit(solution)/shard_map/ppermute | solution.py:759
  63.8 0.9 copy-start.6
  63.8 1.1 %copy-start.5 = (bf16[512,4,192]{0,2,1:T(8,128)(2,1)S(1)}, bf16[512,4,192]{0,2,1:T(8,128)(2,1)}, u32[]{:S(2)}) copy-start(bf16[512,4,192]{0,2,1:T(8,128)(2,1)} %param.27) | copy-start | bytes 2359300
  73.3 1.8 %collective-permute-start.31 = (bf16[384,512]{1,0:T(8,128)(2,1)S(1)}, bf16[384,512]{1,0:T(8,128)(2,1)S(1)}, u32[]{:S(2)}, u32[]{:S(2)}) collective-permute-start(bf16[384,512]{1,0:T(8,128)(2,1)S(1)} %get-tuple-element.77.heads_ref), channel_id=1, source_target_pairs={{0,1},{1,0},{2,3},{3,2},{4,5},{5,4},{6,7},{7,6},{8,9},{9,8},{10,11... | collective-permute-start | bytes 1179656 | tf_op jit(solution)/shard_map/ppermute | solution.py:811
  74.0 13.4 %copy-start.1 = (bf16[384,256]{1,0:T(8,128)(2,1)S(1)}, bf16[384,256]{1,0:T(8,128)(2,1)}, u32[]{:S(2)}) copy-start(bf16[384,256]{1,0:T(8,128)(2,1)} %latent_ref.1) | copy-start | bytes 589828
  75.7 7.8 %collective-permute-start.32 = (bf16[384,256]{1,0:T(8,128)(2,1)S(1)}, bf16[384,256]{1,0:T(8,128)(2,1)S(1)}, u32[]{:S(2)}, u32[]{:S(2)}) collective-permute-start(bf16[384,256]{1,0:T(8,128)(2,1)S(1)} %get-tuple-element.80), channel_id=1, source_target_pairs={{0,2},{1,3},{2,0},{3,1},{4,6},{5,7},{6,4},{7,5},{8,10},{9,11},{10,... | collective-permute-start | bytes 589832 | tf_op jit(solution)/shard_map/ppermute | solution.py:826
  76.4 7.3 %collective-permute-start.33 = (bf16[384,256]{1,0:T(8,128)(2,1)S(1)}, bf16[384,256]{1,0:T(8,128)(2,1)S(1)}, u32[]{:S(2)}, u32[]{:S(2)}) collective-permute-start(bf16[384,256]{1,0:T(8,128)(2,1)S(1)} %get-tuple-element.81), channel_id=1, source_target_pairs={{0,4},{1,5},{2,6},{3,7},{4,0},{5,1},{6,2},{7,3},{8,12},{9,13},{10,... | collective-permute-start | bytes 589832 | tf_op jit(solution)/shard_map/ppermute | solution.py:826
  77.4 10.0 %collective-permute-start.34 = (bf16[384,256]{1,0:T(8,128)(2,1)S(1)}, bf16[384,256]{1,0:T(8,128)(2,1)S(1)}, u32[]{:S(2)}, u32[]{:S(2)}) collective-permute-start(bf16[384,256]{1,0:T(8,128)(2,1)S(1)} %get-tuple-element.82), channel_id=1, source_target_pairs={{0,6},{1,7},{2,4},{3,5},{4,2},{5,3},{6,0},{7,1},{8,14},{9,15},{10,... | collective-permute-start | bytes 589832 | tf_op jit(solution)/shard_map/ppermute | solution.py:826
